TPU v7x, 256 devices: a whole 4x4x8 slice. The times are simulated.
256 devices in a mesh: sp: 16 (over y, x), tp: 16 (over z, core).
Axes of the slice: x: 4, y: 4, z: 8, core: 2. Of those that a mesh axis runs over, the one named last changes fastest.
Arguments:
- queries: bfloat16 [16384, 1536], P('sp', 'tp'), may hold values from -34 to 34
- latent: bfloat16 [16384, 512], P('sp'), may hold values from -6 to 6
- rot_key: bfloat16 [16384, 32], P('sp'), may hold values from -34 to 34
- latent_gain: float32 [512], replicated, may hold values from 0.1 to 1.9
- key_up: bfloat16 [512, 1024], P(None, 'tp'), may hold values from -0.25 to 0.25
- value_up: bfloat16 [512, 1024], P(None, 'tp'), may hold values from -0.70710678 to 0.70710678
- query_gain: float32 [96], replicated, may hold values from 0.5 to 6
- key_gain: float32 [96], replicated, may hold values from 0.5 to 6
- out_gain: float32 [1024], replicated, may hold values from 0.1 to 1.9
- out_weight: bfloat16 [1024, 2048], replicated, may hold values from -0.1875 to 0.1875
- residual: bfloat16 [16384, 2048], P(('sp', 'tp')), may hold values from -6 to 6
- ffn_gain: float32 [2048], replicated, may hold values from 0.1 to 1.9
- routes: int32 [16384, 2], P(('sp', 'tp')), may hold values from 0 to 15, all different within a row; in each aligned block of 64 rows (0 to 63, 64 to 127, ...) at most 9 rows name the same one
- route_weights: float32 [16384, 2], P(('sp', 'tp')), may hold values from 0.2 to 1
- expert_gate: bfloat16 [16, 2048, 2048], P('sp', None, 'tp'), may hold values from -0.125 to 0.125
- expert_up: bfloat16 [16, 2048, 2048], P('sp', None, 'tp'), may hold values from -0.125 to 0.125
- expert_down: bfloat16 [16, 2048, 2048], P('sp', 'tp'), may hold values from -0.125 to 0.125
Outputs:
- layer_out: bfloat16 [16384, 2048], P(('sp', 'tp'))
Inputs may be any that keep to these rules, and one draw needn't show every extreme that they name: `routes`: the 2 experts of a token differ. Among the 64 rows of one device each expert is named by at most 9 rows, a bound that some block reaches.
All inputs are finite; a program needn't handle non-finite values.
Results may differ from a plain program's by a relative error of at most 0.02.
The roundings to bfloat16 on the way count: a program that leaves them out, or rounds other values in their place, can miss the bound.
Values may be sent and summed in bfloat16 or wider, within the bound.
A program may use at most 128 MiB of HBM per device.

v0:
```python
import jax
import jax.numpy as jnp
from jax import lax
from jax.sharding import PartitionSpec as P

D = 2048
NOPE = 64
ROPE = 32
VH = 64
TOPK = 2
QK = 96


epsilon = 1e-06
rope_base = 10000.0


def rms_scale(values):
    return lax.rsqrt(jnp.mean(values * values, axis=-1, keepdims=True) + epsilon)


def rotate_half(values, angles):
    half_dims = values.shape[-1] // 2
    first_half = values[..., :half_dims]
    second_half = values[..., half_dims:]
    cosine = jnp.cos(angles)
    sine_val = jnp.sin(angles)
    return jnp.concatenate(
        [
            first_half * cosine - second_half * sine_val,
            second_half * cosine + first_half * sine_val,
        ],
        axis=-1,
    )


def head_prepare(raw_rows, gain_vec, angles):
    normed_rows = raw_rows * rms_scale(raw_rows) * gain_vec
    turned_rows = rotate_half(normed_rows[..., NOPE:], angles[:, None, :])
    return jnp.concatenate([normed_rows[..., :NOPE], turned_rows], axis=-1).astype(jnp.bfloat16)


def slot_targets(route_rows, expert_total, slot_cap):
    flat_routes = route_rows.reshape(-1)
    one_hot = (flat_routes[:, None] == jnp.arange(expert_total, dtype=jnp.int32)[None, :]).astype(
        jnp.int32
    )
    earlier = jnp.cumsum(one_hot, axis=0) - one_hot
    rank_in = jnp.sum(earlier * one_hot, axis=1)
    return (flat_routes * slot_cap + rank_in).reshape(route_rows.shape)


def select_matrix(targets, slot_total):
    hits = targets[:, :, None] == jnp.arange(slot_total, dtype=jnp.int32)[None, None, :]
    return jnp.sum(hits.astype(jnp.bfloat16), axis=1)


def shards(
    queries,
    latent,
    rot_key,
    latent_gain,
    key_up,
    value_up,
    query_gain,
    key_gain,
    out_gain,
    out_weight,
    residual,
    ffn_gain,
    routes,
    route_weights,
    expert_gate,
    expert_up,
    expert_down,
):
    shard_len = queries.shape[0]
    local_heads = key_up.shape[1] // NOPE
    sp_count = lax.axis_size("sp")
    tp_count = lax.axis_size("tp")
    my_first = lax.axis_index("sp") * shard_len
    my_last = my_first + shard_len - 1
    positions = my_first + jnp.arange(shard_len, dtype=jnp.int32)
    inverse = rope_base ** (-jnp.arange(0, ROPE, 2, dtype=jnp.float32) / ROPE)
    angles = positions.astype(jnp.float32)[:, None] * inverse[None, :]
    lat_f32 = latent.astype(jnp.float32)
    normed_latent = (lat_f32 * rms_scale(lat_f32) * latent_gain).astype(jnp.bfloat16)
    key_nope = jnp.dot(normed_latent, key_up, preferred_element_type=jnp.float32).astype(
        jnp.bfloat16
    )
    value_rows = jnp.dot(normed_latent, value_up, preferred_element_type=jnp.float32).astype(
        jnp.bfloat16
    )
    shared = rot_key.astype(jnp.float32)[:, None, :]
    raw_keys = jnp.concatenate(
        [key_nope.astype(jnp.float32).reshape(shard_len, local_heads, NOPE), shared], axis=-1
    )
    key_rows = head_prepare(raw_keys, key_gain, angles)
    query_rows = head_prepare(
        queries.astype(jnp.float32).reshape(shard_len, local_heads, QK), query_gain, angles
    )
    query_heads = jnp.transpose(query_rows, (1, 0, 2))
    bundle = jnp.concatenate(
        [
            jnp.transpose(key_rows, (1, 2, 0)),
            jnp.transpose(value_rows.reshape(shard_len, local_heads, VH), (1, 2, 0)),
        ],
        axis=1,
    )
    score_scale = QK ** (-0.5)
    init_state = (
        jnp.full((local_heads, shard_len), -1e30, jnp.float32),
        jnp.zeros((local_heads, shard_len), jnp.float32),
        jnp.zeros((local_heads, shard_len, VH), jnp.float32),
    )
    key_piece = lax.all_gather(bundle, "sp", axis=2, tiled=True)
    block_count = key_piece.shape[2] // shard_len

    def one_block(block_index, running_state):
        first_key = block_index * shard_len

        def compute(inner):
            row_peak, row_total, weighted = inner
            key_part = lax.dynamic_slice_in_dim(key_piece, block_index * shard_len, shard_len, 2)
            scores = (
                jnp.einsum(
                    "hqc,hck->hqk",
                    query_heads,
                    key_part[:, :QK, :],
                    preferred_element_type=jnp.float32,
                )
                * score_scale
            )
            key_pos = first_key + jnp.arange(shard_len, dtype=jnp.int32)
            allowed = key_pos[None, None, :] <= positions[None, :, None]
            scores = jnp.where(allowed, scores, -1e30)
            new_peak = jnp.maximum(row_peak, jnp.max(scores, axis=2))
            exponent = jnp.where(allowed, jnp.exp(scores - new_peak[..., None]), 0.0)
            factor = jnp.exp(row_peak - new_peak)
            new_total = row_total * factor + jnp.sum(exponent, axis=2)
            contrib = jnp.einsum(
                "hqk,hvk->hqv",
                exponent.astype(jnp.bfloat16),
                key_part[:, QK:, :],
                preferred_element_type=jnp.float32,
            )
            return (new_peak, new_total, weighted * factor[..., None] + contrib)

        return lax.cond(first_key <= my_last, compute, lambda inner: inner, running_state)

    row_peak, row_total, weighted = lax.fori_loop(0, block_count, one_block, init_state)
    attended = (weighted / row_total[..., None]).astype(jnp.bfloat16)
    tok_count = residual.shape[0]
    head_major = jnp.transpose(attended, (1, 0, 2)).reshape(shard_len, local_heads * VH)
    token_rows = lax.all_to_all(head_major, "tp", split_axis=0, concat_axis=1, tiled=True).astype(
        jnp.float32
    )
    normed_rows = (token_rows * rms_scale(token_rows) * out_gain).astype(jnp.bfloat16)
    partials = jnp.einsum(
        "tgc,gcd->tgd",
        normed_rows.reshape(tok_count, tp_count, -1),
        out_weight.reshape(tp_count, -1, D),
        preferred_element_type=jnp.float32,
    )
    rounded = lax.optimization_barrier(partials.astype(jnp.bfloat16))
    mixed = jnp.sum(rounded.astype(jnp.float32), axis=1)
    middle = residual.astype(jnp.float32) + mixed
    ffn_input = (middle * rms_scale(middle) * ffn_gain).astype(jnp.bfloat16)
    slot_cap = max(2, 9 * tok_count * TOPK // (8 * sp_count))
    slot_total = sp_count * slot_cap
    targets = slot_targets(routes, sp_count, slot_cap)
    chooser = select_matrix(targets, slot_total)
    outbound = (
        jnp.einsum("ts,td->sd", chooser, ffn_input, preferred_element_type=jnp.float32)
        .astype(jnp.bfloat16)
        .reshape(sp_count, slot_cap, D)
    )
    arrived = lax.all_to_all(outbound, "sp", split_axis=0, concat_axis=0, tiled=True)
    item_count = arrived.shape[1]
    flat_rows = arrived.reshape(sp_count * item_count, D)
    row_block = lax.all_gather(flat_rows, "tp", axis=0, tiled=True)
    gate_pre = jnp.dot(row_block, expert_gate[0], preferred_element_type=jnp.float32)
    up_pre = jnp.dot(row_block, expert_up[0], preferred_element_type=jnp.float32)
    hidden = (jax.nn.silu(gate_pre) * up_pre).astype(jnp.bfloat16)
    served = lax.psum_scatter(
        jnp.dot(hidden, expert_down[0], preferred_element_type=jnp.float32).astype(jnp.bfloat16),
        "tp",
        scatter_dimension=0,
        tiled=True,
    ).reshape(sp_count, item_count, D)
    returned_rows = lax.all_to_all(served, "sp", split_axis=0, concat_axis=0, tiled=True).reshape(
        slot_total, D
    )
    picked = (
        jnp.take(returned_rows, targets.reshape(-1), axis=0)
        .reshape(tok_count, TOPK, D)
        .astype(jnp.float32)
    )
    moe_sum = jnp.sum(picked * route_weights[:, :, None], axis=1)
    return (middle + moe_sum).astype(jnp.bfloat16)


def solution(mesh):
    return jax.shard_map(
        shards,
        mesh=mesh,
        in_specs=(
            P("sp", "tp"),
            P("sp", None),
            P("sp", None),
            P(),
            P(None, "tp"),
            P(None, "tp"),
            P(),
            P(),
            P(),
            P(),
            P(("sp", "tp"), None),
            P(),
            P(("sp", "tp"), None),
            P(("sp", "tp"), None),
            P("sp", None, "tp"),
            P("sp", None, "tp"),
            P("sp", "tp", None),
        ),
        out_specs=P(("sp", "tp"), None),
        check_vma=False,
    )
```

profile of v0, /device:TPU:1, one launch (start us, length us, event | category | flops | bytes accessed | tf_op | source)
XLA Modules:
  0.0 448.4 jit_solution(6509418621641927697)
XLA Ops:
  6.6 0.0 all-gather.3.cloned.1.call-start
  6.6 1.6 fusion.21
  8.3 0.0 copy-start.8
  8.3 0.0 copy-start.6
  8.3 1.8 fusion.29
  10.1 0.9 fusion.40
  11.0 1.0 fusion.42
  12.0 1.0 fusion.41
  13.0 0.6 fusion.30
  13.6 0.1 fusion.44
  13.7 0.3 fusion.74
  14.1 0.7 pad_maximum_fusion
  14.8 0.0 all-gather.3.cloned.1.call-update
  14.9 0.2 copy.34
  15.1 0.1 mul.291
  15.2 0.1 copy.36
  15.2 0.1 reshape.499
  15.4 0.1 fusion.72
  15.5 0.2 reduce_window_sum.11
  15.7 0.2 select_reduce_fusion
  15.8 0.1 reduce_sum.105
  16.0 0.1 copy.37
  16.1 63.8 %all-gather.3.cloned.1.call-done = bf16[1,160,16384]{2,1,0:T(8,128)(2,1)} async-done(((bf16[1,160,1024]{2,1,0:T(8,128)(2,1)}), bf16[1,160,16384]{2,1,0:T(8,128)(2,1)}) %all-gather.3.cloned.1.call-update) | async-done | bytes 5242896 | tf_op jit(solution)/shard_map/all_gather | solution.py:116
  79.9 9.9 %while.18 = (s32[]{:T(128)}, f32[1,1024]{1,0:T(1,128)S(1)}, f32[1,1024]{1,0:T(1,128)S(1)}, f32[1,1024,64]{1,2,0:T(8,128)S(1)}, s32[]{:T(128)}, /*index=5*/bf16[1...) while((s32[]{:T(128)}, f32[1,1024]{1,0:T(1,128)S(1)}, ...), condition=%wide.region_8.9_spmd.clone, body=%wide.region_3.8_spmd.clone.sunk | while | flops 352456704 | bytes 30515560 | solution.py:151
  79.9 9.1 %conditional.3 = ((f32[1,1024]{1,0:T(1,128)S(1)}, f32[1,1024]{1,0:T(1,128)S(1)}, f32[1,1024,64]{1,2,0:T(8,128)S(1)})) conditional(s32[]{:T(128)} %convert_element_type.207, (f32[1,1024]{1,0:T(1,128)S(1)}, f32[1,1024]{1,0:T(1,128)S(1)}, f32[1,1024,64]{1,2,0:T(8,128)S(1)}) %tuple.54, (s32[]{:T(128)}, s32[]{:T(128)}, s32[]{:T(128)}, ...), branch_computations={%region_4.0_spmd, %region_5.7_spmd} | conditional | flops 352456704 | bytes 30511242 | solution.py:149
  79.9 2.0 fusion.2
  82.0 2.0 copy-done.1
  84.0 1.5 fusion.4
  85.6 3.5 fusion.10
  89.8 0.2 copy.41
  90.0 0.9 reshape.512
  90.9 7.9 %all-to-all-start = ((bf16[16,2,2048]{2,1,0:T(2,128)(2,1)}), bf16[16,2,2048]{2,1,0:T(2,128)(2,1)S(1)}, u32[]{:S(2)}, u32[]{:S(2)}) async-start(bf16[16,2,2048]{2,1,0:T(2,128)(2,1)} %reshape.512), calls=%async_computation | async-start | bytes 262144 | tf_op jit(solution)/shard_map/all_to_all | solution.py:155
  98.8 0.0 all-gather.5.cloned.1.call-start
  98.9 0.1 fusion.71
  98.9 8.7 %all-to-all-done = bf16[16,2,2048]{2,1,0:T(2,128)(2,1)S(1)} async-done(((bf16[16,2,2048]{2,1,0:T(2,128)(2,1)}), bf16[16,2,2048]{2,1,0:T(2,128)(2,1)S(1)}, u32[]{:S(2)}, u32[]{:S(2)}) %all-to-all-start) | async-done | bytes 131104 | tf_op jit(solution)/shard_map/all_to_all | solution.py:155
  107.7 0.2 reshape.513
  107.9 0.2 fusion.32
  108.1 3.5 convert_bitcast_fusion
  111.6 0.8 convert_reduce_fusion
  112.4 0.2 copy-done.2
  112.5 0.2 multiply_reduce_fusion.1
  112.7 0.4 convolution_convert_fusion.1
  113.1 0.2 reshape.500
  113.3 157.4 %all_to_all.23 = bf16[16,9,2048]{2,1,0:T(8,128)(2,1)S(1)} all-to-all(bf16[16,9,2048]{2,1,0:T(8,128)(2,1)S(1)} %reshape.500), channel_id=1, replica_groups=mesh['sp'=16,'tp'=16] {'sp'}, dimensions={0} | all-to-all | bytes 1179648 | tf_op jit(solution)/shard_map/all_to_all | solution.py:178
  270.7 1.1 reshape.501
  271.8 0.0 all-gather.5.cloned.1.call-update
  271.8 0.2 reduce-scatter.2.cloned.1.call-start
  272.1 54.8 %all-gather.5.cloned.1.call-done = bf16[2304,2048]{1,0:T(8,128)(2,1)} async-done(((bf16[144,2048]{1,0:T(8,128)(2,1)}), bf16[2304,2048]{1,0:T(8,128)(2,1)}) %all-gather.5.cloned.1.call-update) | async-done | bytes 9437200 | tf_op jit(solution)/shard_map/all_gather | solution.py:181
  326.8 5.3 %fusion.38 = f32[2304,128]{1,0:T(8,128)S(1)} fusion(bf16[2304,2048]{1,0:T(8,128)(2,1)} %all-gather.5.cloned.1.call-done, bf16[1,2048,128]{2,1,0:T(8,128)(2,1)} %param.35), kind=kOutput, calls=%fused_computation.53 | convolution fusion | flops 1207959552 | bytes 11141120 | tf_op jit(solution)/shard_map/dot_general | solution.py:182
  332.2 14.2 %convolution_convert_fusion = bf16[2304,2048]{1,0:T(8,128)(2,1)} fusion(bf16[2304,2048]{1,0:T(8,128)(2,1)} %all-gather.5.cloned.1.call-done, f32[2304,128]{1,0:T(8,128)S(1)} %fusion.38, bf16[1,128,2048]{2,1,0:T(8,128)(2,1)S(1)} %copy-done, bf16[1,2048,128]{2,1,0:T(8,128)(2,1)S(1)} %copy-done.5), kind=kOutput, calls=%fused_computation.23 | convolution fusion | flops 2422407168 | bytes 21102592 | tf_op jit(solution)/shard_map/dot_general | solution.py:186
  346.4 0.0 reduce-scatter.2.cloned.1.call-update
  346.4 68.3 %reduce-scatter.2.cloned.1.call-done = bf16[144,2048]{1,0:T(8,128)(2,1)} async-done(((bf16[2304,2048]{1,0:T(8,128)(2,1)}), bf16[144,2048]{1,0:T(8,128)(2,1)}) %reduce-scatter.2.cloned.1.call-update) | async-done | bytes 589840 | tf_op jit(solution)/shard_map/reduce_scatter | solution.py:185
  414.7 2.3 reshape.502
  417.0 6.5 %all-to-all-start.2 = ((bf16[16,9,2048]{2,1,0:T(8,128)(2,1)}), bf16[16,9,2048]{2,1,0:T(8,128)(2,1)S(1)}, u32[]{:S(2)}, u32[]{:S(2)}) async-start(bf16[16,9,2048]{2,1,0:T(8,128)(2,1)} %reshape.502), calls=%async_computation.3 | async-start | bytes 2097152 | tf_op jit(solution)/shard_map/all_to_all | solution.py:191
  423.5 0.1 copy.39
  423.6 0.1 mul.304
  423.8 0.1 copy.38
  423.9 0.1 copy.40
  424.0 13.2 %all-to-all-done.2 = bf16[16,9,2048]{2,1,0:T(8,128)(2,1)S(1)} async-done(((bf16[16,9,2048]{2,1,0:T(8,128)(2,1)}), bf16[16,9,2048]{2,1,0:T(8,128)(2,1)S(1)}, u32[]{:S(2)}, u32[]{:S(2)}) %all-to-all-start.2) | async-done | bytes 589856 | tf_op jit(solution)/shard_map/all_to_all | solution.py:191
  437.2 0.3 reshape.503
  437.5 0.9 gather_fusion
  438.4 0.3 gather.7
  438.8 2.3 multiply_reduce_fusion
  441.1 0.8 add_convert_fusion
  (76 shorter events, 0.5 us)
Async XLA Ops:
  6.5 325.6 %copy-start = (bf16[1,128,2048]{2,1,0:T(8,128)(2,1)S(1)}, bf16[1,128,2048]{2,1,0:T(8,128)(2,1)}, u32[]{:S(2)}) copy-start(bf16[1,128,2048]{2,1,0:T(8,128)(2,1)} %param.37) | copy-start | bytes 1572868
  6.5 6.5 %copy-start.3 = (bf16[1024,512]{1,0:T(8,128)(2,1)S(1)}, bf16[1024,512]{1,0:T(8,128)(2,1)}, u32[]{:S(2)}) copy-start(bf16[1024,512]{1,0:T(8,128)(2,1)} %param.22) | copy-start | bytes 3145732
  6.5 6.5 %copy-start.12 = (f32[512]{0:T(512)S(1)}, f32[512]{0:T(512)}, u32[]{:S(2)}) copy-start(f32[512]{0:T(512)} %param.24) | copy-start | bytes 6148
  6.5 7.0 %copy-start.4 = (bf16[1024,96]{0,1:T(8,128)(2,1)S(1)}, bf16[1024,96]{0,1:T(8,128)(2,1)}, u32[]{:S(2)}) copy-start(bf16[1024,96]{0,1:T(8,128)(2,1)} %param.21) | copy-start | bytes 589828
  6.5 6.5 %copy-start.11 = (bf16[512,64]{0,1:T(8,128)(2,1)S(1)}, bf16[512,64]{0,1:T(8,128)(2,1)}, u32[]{:S(2)}) copy-start(bf16[512,64]{0,1:T(8,128)(2,1)} %param.26) | copy-start | bytes 196612
  6.5 7.0 %copy-start.10 = (f32[96]{0:T(128)S(1)}, f32[96]{0:T(128)}, u32[]{:S(2)}) copy-start(f32[96]{0:T(128)} %param.27) | copy-start | bytes 1156
  6.6 73.3 %all-gather.3.cloned.1.call-start = ((), (), s32[]{:S(2)}) async-start(), calls=%async_computation.4 | async-start | bytes 5570560 | tf_op jit(solution)/shard_map/all_gather | solution.py:116
  8.3 6.8 %copy-start.8 = (f32[1024]{0:T(1024)S(1)}, f32[1024]{0:T(1024)}, u32[]{:S(2)}) copy-start(f32[1024]{0:T(1024)} %param.29) | copy-start | bytes 12292
  8.3 6.9 %copy-start.6 = (s32[64,2]{0,1:T(2,128)S(1)}, s32[64,2]{0,1:T(2,128)}, u32[]{:S(2)}) copy-start(s32[64,2]{0,1:T(2,128)} %param.33) | copy-start | bytes 1540
  82.0 2.0 copy-start.1
  90.9 16.8 %all-to-all-start = ((bf16[16,2,2048]{2,1,0:T(2,128)(2,1)}), bf16[16,2,2048]{2,1,0:T(2,128)(2,1)S(1)}, u32[]{:S(2)}, u32[]{:S(2)}) async-start(bf16[16,2,2048]{2,1,0:T(2,128)(2,1)} %reshape.512), calls=%async_computation | async-start | bytes 262144 | tf_op jit(solution)/shard_map/all_to_all | solution.py:155
  98.8 228.0 %all-gather.5.cloned.1.call-start = ((), (), s32[]{:S(2)}) async-start(), calls=%async_computation.5 | async-start | bytes 10027008 | tf_op jit(solution)/shard_map/all_gather | solution.py:181
  111.6 1.0 copy-start.2
  111.6 1.1 copy-start.7
  271.8 60.3 %copy-start.5 = (bf16[1,2048,128]{2,1,0:T(8,128)(2,1)S(1)}, bf16[1,2048,128]{2,1,0:T(8,128)(2,1)}, u32[]{:S(2)}) copy-start(bf16[1,2048,128]{2,1,0:T(8,128)(2,1)} %param.36) | copy-start | bytes 1572868
  271.8 142.9 %reduce-scatter.2.cloned.1.call-start = ((), (), s32[]{:S(2)}) async-start(), calls=%async_computation.6 | async-start | bytes 10027008 | tf_op jit(solution)/shard_map/reduce_scatter | solution.py:185
  346.4 77.5 %copy-start.9 = (f32[64,2]{0,1:T(2,128)S(1)}, f32[64,2]{0,1:T(2,128)}, u32[]{:S(2)}) copy-start(f32[64,2]{0,1:T(2,128)} %param.34) | copy-start | bytes 1540
  417.0 20.2 %all-to-all-start.2 = ((bf16[16,9,2048]{2,1,0:T(8,128)(2,1)}), bf16[16,9,2048]{2,1,0:T(8,128)(2,1)S(1)}, u32[]{:S(2)}, u32[]{:S(2)}) async-start(bf16[16,9,2048]{2,1,0:T(8,128)(2,1)} %reshape.502), calls=%async_computation.3 | async-start | bytes 2097152 | tf_op jit(solution)/shard_map/all_to_all | solution.py:191
Sparse Core Ops, SparseCore 0:
  14.9 64.8 all-gather.2
  271.9 54.8 all-gather.4
  346.5 68.1 reduce-scatter.1
where the time goes:
time: 452 us; the launch traced here: 448 us
  waiting for transfers between devices  209 us (46%)
  blocking collectives  157 us (35%)
  matrix products  31.3 us (7%)
  starting transfers between devices  14.7 us (3%)
  between operations  13.5 us (3%)
  other arithmetic  12 us (3%)
  local copies, waits for them, and re-layouts  9.85 us (2%)
    all_to_all x1, blocking collectives, shards(): lax.all_to_all(outbound, 'sp', split_axis=0, concat_axis=0, tiled=True)  157 us
    reduce_scatter x1, waiting for transfers between devices, shards(): lax.psum_scatter(jnp.dot(hidden, expert_down[0], preferred_element_type=j...  68.3 us
    all_gather x1, waiting for transfers between devices, shards(): key_piece = lax.all_gather(bundle, 'sp', axis=2, tiled=True)  63.8 us
    all_gather x1, waiting for transfers between devices, shards(): row_block = lax.all_gather(flat_rows, 'tp', axis=0, tiled=True)  54.8 us
    dot_general x1, matrix products, shards(): jnp.dot(hidden, expert_down[0], preferred_element_type=jnp.float32)  14.2 us
    all_to_all x1, waiting for transfers between devices, shards(): lax.all_to_all(served, 'sp', split_axis=0, concat_axis=0, tiled=True)  13.2 us
  transfers between devices with their start and end apart: 5, of which 5 were waited for; matrix products, arithmetic and copies ran while one was open for 0% of the time, Pallas kernels for 0%

commit v1 on v0

--- a/solution.py
+++ b/solution.py
@@ -1,6 +1,8 @@
 import jax
 import jax.numpy as jnp
 from jax import lax
+from jax.experimental import pallas as pl
+from jax.experimental.pallas import tpu as pltpu
 from jax.sharding import PartitionSpec as P
 
 D = 2048
@@ -53,6 +55,253 @@
 def select_matrix(targets, slot_total):
     hits = targets[:, :, None] == jnp.arange(slot_total, dtype=jnp.int32)[None, None, :]
     return jnp.sum(hits.astype(jnp.bfloat16), axis=1)
+
+
+SCORE_EXP = 1.4426950408889634 * QK ** (-0.5)
+Q_TILE = 256
+
+
+def attend_body(q_ref, kv_ref, out_ref, peak_ref, acc_ref, val_ref, block_count):
+    shard_len = kv_ref.shape[2]
+    half = shard_len // 2
+    mine = lax.axis_index("sp")
+    low = jnp.minimum(mine, block_count - 1 - mine)
+    high = block_count - 1 - low
+    shift = jnp.where(mine < block_count // 2, 0, half)
+    peak_ref[...] = jnp.full_like(peak_ref, -1e30)
+    acc_ref[...] = jnp.zeros_like(acc_ref)
+    lane = lax.broadcasted_iota(jnp.int32, (shard_len, 128), 1)
+    val_ref[...] = jnp.where(lane == VH, 1.0, 0.0).astype(jnp.bfloat16)
+
+    def one_block(block, parts):
+        keys = kv_ref[block, :QK, :]
+        val_ref[:, :VH] = kv_ref[block, QK:, :].T
+        values = val_ref[...]
+        for start, masked in parts:
+            for first in range(start, start + half, Q_TILE):
+                rows = pl.ds(first, Q_TILE)
+                scores = jnp.dot(q_ref[rows, :], keys, preferred_element_type=jnp.float32)
+                if masked:
+                    row = lax.broadcasted_iota(jnp.int32, scores.shape, 0)
+                    col = lax.broadcasted_iota(jnp.int32, scores.shape, 1)
+                    scores = jnp.where(col - row <= shift + (first - start), scores, -1e30)
+                old = peak_ref[rows, :]
+                new = jnp.maximum(old, jnp.max(scores, axis=1, keepdims=True))
+                weights = jnp.exp2((scores - new[:, :1]) * SCORE_EXP).astype(jnp.bfloat16)
+                factor = jnp.exp2((old - new) * SCORE_EXP)
+                peak_ref[rows, :] = new
+                acc_ref[rows, :] = acc_ref[rows, :] * factor + jnp.dot(
+                    weights, values, preferred_element_type=jnp.float32
+                )
+
+    lax.fori_loop(0, low, lambda j, _: one_block(j, ((0, False), (half, False))), None)
+    one_block(low, ((0, True), (half, False)))
+    lax.fori_loop(low + 1, high, lambda j, _: one_block(j, ((half, False),)), None)
+    one_block(high, ((half, True),))
+    total = acc_ref[:, VH : VH + 1]
+    out_ref[...] = (acc_ref[:, :VH] / total).astype(jnp.bfloat16)
+
+
+def flash_attention(query_pair, key_blocks, block_count):
+    shard_len = query_pair.shape[0]
+
+    def kernel(q_ref, kv_ref, out_ref, peak_ref, acc_ref, val_ref):
+        attend_body(q_ref, kv_ref, out_ref, peak_ref, acc_ref, val_ref, block_count)
+
+    return pl.pallas_call(
+        kernel,
+        out_shape=jax.ShapeDtypeStruct((shard_len, VH), jnp.bfloat16),
+        in_specs=[pl.BlockSpec(memory_space=pltpu.VMEM)] * 2,
+        out_specs=pl.BlockSpec(memory_space=pltpu.VMEM),
+        scratch_shapes=[
+            pltpu.VMEM((shard_len, 128), jnp.float32),
+            pltpu.VMEM((shard_len, 128), jnp.float32),
+            pltpu.VMEM((shard_len, 128), jnp.bfloat16),
+        ],
+        compiler_params=pltpu.CompilerParams(vmem_limit_bytes=40 * 1024 * 1024),
+        cost_estimate=pl.CostEstimate(
+            flops=9 * shard_len * shard_len * 320, bytes_accessed=6 << 20, transcendentals=9 << 20
+        ),
+    )(query_pair, key_blocks)
+
+
+ROW_CUT = 80
+
+
+def expert_ring(rows, gate, up, down):
+    count, width = rows.shape
+    hidden = gate.shape[1]
+    chips = lax.axis_size("tp") // 2
+    both = 2 * count
+
+    def kernel(
+        x_ref, gate_ref, up_ref, down_ref, out_ref,
+        both_ref, seen, own_part, far_part, near_part, run_in, run_out,
+        fwd_send, fwd_recv, back_send, back_recv, twin_send, twin_recv,
+        part_send, part_recv, sum_fwd_send, sum_fwd_recv, sum_back_send, sum_back_recv,
+    ):
+        place = lax.axis_index("tp")
+        chip, core = place // 2, place % 2
+        toward = jnp.where(core == 0, 1, chips - 1)
+        ahead = ((chip + toward) % chips) * 2 + core
+        behind = ((chip + chips - toward) % chips) * 2 + core
+        twin = chip * 2 + 1 - core
+
+        barrier = pltpu.get_barrier_semaphore()
+        for other in (ahead, behind, twin):
+            pl.semaphore_signal(
+                barrier, inc=1, device_id={"tp": other}, device_id_type=pl.DeviceIdType.MESH
+            )
+        pl.semaphore_wait(barrier, 3)
+
+        def remote(source, target, send, recv, other):
+            return pltpu.make_async_remote_copy(
+                src_ref=source,
+                dst_ref=target,
+                send_sem=send,
+                recv_sem=recv,
+                device_id={"tp": other},
+                device_id_type=pl.DeviceIdType.MESH,
+            )
+
+        first, second = pl.ds(0, ROW_CUT), pl.ds(ROW_CUT, count - ROW_CUT)
+        front, rear = pl.ds(0, count), pl.ds(count, count)
+
+        def forward(step):
+            return (
+                remote(seen.at[step, first], seen.at[step + 1, first],
+                       fwd_send.at[step], fwd_recv.at[step + 1], ahead),
+                remote(seen.at[step, second], seen.at[step + 1, second],
+                       back_send.at[step], back_recv.at[step + 1], behind),
+            )
+
+        def forward_own():
+            return (
+                remote(x_ref.at[first], seen.at[1, first], fwd_send.at[0], fwd_recv.at[1], ahead),
+                remote(x_ref.at[second], seen.at[1, second],
+                       back_send.at[0], back_recv.at[1], behind),
+            )
+
+        def share(step):
+            return remote(seen.at[step, front], seen.at[step, rear],
+                          twin_send.at[step], twin_recv.at[step], twin)
+
+        def share_own():
+            return remote(x_ref, seen.at[0, rear], twin_send.at[0], twin_recv.at[0], twin)
+
+        def hand_over(step):
+            return remote(far_part.at[step], near_part.at[step],
+                          part_send.at[step], part_recv.at[step], twin)
+
+        def pass_sum(step):
+            return (
+                remote(run_out.at[step, first], run_in.at[step + 1, first],
+                       sum_fwd_send.at[step], sum_fwd_recv.at[step + 1], ahead),
+                remote(run_out.at[step, second], run_in.at[step + 1, second],
+                       sum_back_send.at[step], sum_back_recv.at[step + 1], behind),
+            )
+
+        def experts(step):
+            tokens = seen[step]
+            pre = jnp.dot(tokens, both_ref[...], preferred_element_type=jnp.float32)
+            inner = (jax.nn.silu(pre[:, :hidden]) * pre[:, hidden:]).astype(jnp.bfloat16)
+            part = jnp.dot(inner, down_ref[...], preferred_element_type=jnp.float32).astype(
+                jnp.bfloat16
+            )
+            own_part[step] = part[:count]
+            far_part[step] = part[count:]
+
+        for copy in (*forward_own(), share_own()):
+            copy.start()
+        both_ref[:, :hidden] = gate_ref[...]
+        both_ref[:, hidden:] = up_ref[...]
+        seen[0, front, :] = x_ref[...]
+        share_own().wait_recv()
+        experts(0)
+        hand_over(0).start()
+
+        def step_of(step, _):
+            arrived = forward(step - 1)
+            arrived[0].wait_recv()
+            arrived[1].wait_recv()
+
+            @pl.when(step < chips - 1)
+            def _():
+                for copy in forward(step):
+                    copy.start()
+
+            share(step).start()
+            share(step).wait_recv()
+            experts(step)
+            hand_over(step).start()
+            hand_over(step).wait_recv()
+
+            @pl.when(step > 1)
+            def _():
+                for copy in pass_sum(step - 1):
+                    copy.wait_recv()
+                run_out[step] = (
+                    run_in[step].astype(jnp.float32)
+                    + own_part[step].astype(jnp.float32)
+                    + near_part[step].astype(jnp.float32)
+                ).astype(jnp.bfloat16)
+
+            @pl.when(step == 1)
+            def _():
+                run_out[step] = (
+                    own_part[step].astype(jnp.float32) + near_part[step].astype(jnp.float32)
+                ).astype(jnp.bfloat16)
+
+            for copy in pass_sum(step):
+                copy.start()
+
+        lax.fori_loop(1, chips, step_of, None)
+        hand_over(0).wait_recv()
+        for copy in pass_sum(chips - 1):
+            copy.wait_recv()
+        out_ref[...] = (
+            run_in[chips].astype(jnp.float32)
+            + own_part[0].astype(jnp.float32)
+            + near_part[0].astype(jnp.float32)
+        ).astype(jnp.bfloat16)
+
+        for copy in (*forward_own(), share_own(), hand_over(0)):
+            copy.wait_send()
+
+        def drain(step, _):
+            @pl.when(step < chips - 1)
+            def _():
+                for copy in forward(step):
+                    copy.wait_send()
+
+            share(step).wait_send()
+            hand_over(step).wait_send()
+            for copy in pass_sum(step):
+                copy.wait_send()
+
+        lax.fori_loop(1, chips, drain, None)
+
+    block = (count, width)
+    sems = [pltpu.SemaphoreType.DMA((chips + 1,)) for _ in range(12)]
+    return pl.pallas_call(
+        kernel,
+        out_shape=jax.ShapeDtypeStruct(block, jnp.bfloat16),
+        in_specs=[pl.BlockSpec(memory_space=pltpu.VMEM)] * 4,
+        out_specs=pl.BlockSpec(memory_space=pltpu.VMEM),
+        scratch_shapes=[
+            pltpu.VMEM((width, 2 * hidden), jnp.bfloat16),
+            pltpu.VMEM((chips, both, width), jnp.bfloat16),
+            pltpu.VMEM((chips, *block), jnp.bfloat16),
+            pltpu.VMEM((chips, *block), jnp.bfloat16),
+            pltpu.VMEM((chips, *block), jnp.bfloat16),
+            pltpu.VMEM((chips + 1, *block), jnp.bfloat16),
+            pltpu.VMEM((chips, *block), jnp.bfloat16),
+            *sems,
+        ],
+        compiler_params=pltpu.CompilerParams(
+            collective_id=3, has_side_effects=True, vmem_limit_bytes=50 * 1024 * 1024
+        ),
+    )(rows, gate, up, down)
 
 
 def shards(
@@ -79,7 +328,6 @@
     sp_count = lax.axis_size("sp")
     tp_count = lax.axis_size("tp")
     my_first = lax.axis_index("sp") * shard_len
-    my_last = my_first + shard_len - 1
     positions = my_first + jnp.arange(shard_len, dtype=jnp.int32)
     inverse = rope_base ** (-jnp.arange(0, ROPE, 2, dtype=jnp.float32) / ROPE)
     angles = positions.astype(jnp.float32)[:, None] * inverse[None, :]
@@ -99,59 +347,26 @@
     query_rows = head_prepare(
         queries.astype(jnp.float32).reshape(shard_len, local_heads, QK), query_gain, angles
     )
-    query_heads = jnp.transpose(query_rows, (1, 0, 2))
-    bundle = jnp.concatenate(
-        [
-            jnp.transpose(key_rows, (1, 2, 0)),
-            jnp.transpose(value_rows.reshape(shard_len, local_heads, VH), (1, 2, 0)),
-        ],
-        axis=1,
-    )
-    score_scale = QK ** (-0.5)
-    init_state = (
-        jnp.full((local_heads, shard_len), -1e30, jnp.float32),
-        jnp.zeros((local_heads, shard_len), jnp.float32),
-        jnp.zeros((local_heads, shard_len, VH), jnp.float32),
-    )
-    key_piece = lax.all_gather(bundle, "sp", axis=2, tiled=True)
-    block_count = key_piece.shape[2] // shard_len
-
-    def one_block(block_index, running_state):
-        first_key = block_index * shard_len
-
-        def compute(inner):
-            row_peak, row_total, weighted = inner
-            key_part = lax.dynamic_slice_in_dim(key_piece, block_index * shard_len, shard_len, 2)
-            scores = (
-                jnp.einsum(
-                    "hqc,hck->hqk",
-                    query_heads,
-                    key_part[:, :QK, :],
-                    preferred_element_type=jnp.float32,
-                )
-                * score_scale
-            )
-            key_pos = first_key + jnp.arange(shard_len, dtype=jnp.int32)
-            allowed = key_pos[None, None, :] <= positions[None, :, None]
-            scores = jnp.where(allowed, scores, -1e30)
-            new_peak = jnp.maximum(row_peak, jnp.max(scores, axis=2))
-            exponent = jnp.where(allowed, jnp.exp(scores - new_peak[..., None]), 0.0)
-            factor = jnp.exp(row_peak - new_peak)
-            new_total = row_total * factor + jnp.sum(exponent, axis=2)
-            contrib = jnp.einsum(
-                "hqk,hvk->hqv",
-                exponent.astype(jnp.bfloat16),
-                key_part[:, QK:, :],
-                preferred_element_type=jnp.float32,
-            )
-            return (new_peak, new_total, weighted * factor[..., None] + contrib)
-
-        return lax.cond(first_key <= my_last, compute, lambda inner: inner, running_state)
-
-    row_peak, row_total, weighted = lax.fori_loop(0, block_count, one_block, init_state)
-    attended = (weighted / row_total[..., None]).astype(jnp.bfloat16)
+    bundle = jnp.concatenate([key_rows.reshape(shard_len, QK).T, value_rows.T], axis=0)
+    key_blocks = lax.all_gather(bundle, "sp", axis=0, tiled=False)
+    low_side = lax.axis_index("sp") < sp_count // 2
+    half = shard_len // 2
+    query_rows = query_rows.reshape(shard_len, QK)
+    mirror = [(place, sp_count - 1 - place) for place in range(sp_count)]
+    kept = jnp.where(low_side, query_rows[:half], query_rows[half:])
+    sent = jnp.where(low_side, query_rows[half:], query_rows[:half])
+    traded = lax.ppermute(sent, "sp", mirror)
+    query_pair = jnp.where(
+        low_side, jnp.concatenate([kept, traded]), jnp.concatenate([traded, kept])
+    )
+    pair_out = flash_attention(query_pair, key_blocks, sp_count)
+    own_out = jnp.where(low_side, pair_out[:half], pair_out[half:])
+    other_out = jnp.where(low_side, pair_out[half:], pair_out[:half])
+    traded_out = lax.ppermute(other_out, "sp", mirror)
+    head_major = jnp.where(
+        low_side, jnp.concatenate([own_out, traded_out]), jnp.concatenate([traded_out, own_out])
+    )
     tok_count = residual.shape[0]
-    head_major = jnp.transpose(attended, (1, 0, 2)).reshape(shard_len, local_heads * VH)
     token_rows = lax.all_to_all(head_major, "tp", split_axis=0, concat_axis=1, tiled=True).astype(
         jnp.float32
     )
@@ -178,16 +393,9 @@
     arrived = lax.all_to_all(outbound, "sp", split_axis=0, concat_axis=0, tiled=True)
     item_count = arrived.shape[1]
     flat_rows = arrived.reshape(sp_count * item_count, D)
-    row_block = lax.all_gather(flat_rows, "tp", axis=0, tiled=True)
-    gate_pre = jnp.dot(row_block, expert_gate[0], preferred_element_type=jnp.float32)
-    up_pre = jnp.dot(row_block, expert_up[0], preferred_element_type=jnp.float32)
-    hidden = (jax.nn.silu(gate_pre) * up_pre).astype(jnp.bfloat16)
-    served = lax.psum_scatter(
-        jnp.dot(hidden, expert_down[0], preferred_element_type=jnp.float32).astype(jnp.bfloat16),
-        "tp",
-        scatter_dimension=0,
-        tiled=True,
-    ).reshape(sp_count, item_count, D)
+    served = expert_ring(flat_rows, expert_gate[0], expert_up[0], expert_down[0]).reshape(
+        sp_count, item_count, D
+    )
     returned_rows = lax.all_to_all(served, "sp", split_axis=0, concat_axis=0, tiled=True).reshape(
         slot_total, D
     )

time: 452 us -> 291 us (0.64)
  blocking collectives: 157 us -> 20.9 us
  waiting for transfers between devices: 209 us -> 85.6 us
  Pallas kernels: 0 us -> 118 us
  matrix products: 31.3 us -> 6.21 us
  starting transfers between devices: 14.7 us -> 21.2 us
    all_to_all x1, blocking collectives: 157 us -> 20.9 us  [shards(): lax.all_to_all(outbound, 'sp', split_axis=0, concat_axis=0, tiled=True)]
    pallas_call x0 -> x2, Pallas kernels: none -> 118 us  [the longest x1 95.1 us: expert_ring(): pl.pallas_call(kernel, out_shape=jax.ShapeDtypeStruct(block, jnp.bfloat16...]
    reduce_scatter x1 -> x0, waiting for transfers between devices: 68.3 us -> none  [shards(): lax.psum_scatter(jnp.dot(hidden, expert_down[0], preferred_element_type=j...]
    all_gather x2 -> x1, waiting for transfers between devices: 119 us -> 56.4 us  [shards(): key_blocks = lax.all_gather(bundle, 'sp', axis=0, tiled=False)]
    dot_general x4 -> x0, matrix products: 25.1 us -> none  [the longest x1 14.2 us: shards(): jnp.dot(hidden, expert_down[0], preferred_element_type=jnp.float32)]
    ppermute x0 -> x2, starting transfers between devices: none -> 8.62 us  [the longest x1 5.84 us: shards(): traded = lax.ppermute(sent, 'sp', mirror)]
    ppermute x0 -> x2, waiting for transfers between devices: none -> 6.21 us  [the longest x1 4.44 us: shards(): traded_out = lax.ppermute(other_out, 'sp', mirror)]
  transfers between devices with their start and end apart: 5 -> 5, of which waited for: 5 -> 5; matrix products, arithmetic and copies ran while one was open for 0% -> 1% of each run, Pallas kernels for 0% -> 0%
where the time goes in v1:
time: 291 us; the launch traced here: 288 us
  Pallas kernels  118 us (41%)
  waiting for transfers between devices  85.6 us (29%)
  starting transfers between devices  21.2 us (7%)
  blocking collectives  20.9 us (7%)
  between operations  13.9 us (5%)
  local copies, waits for them, and re-layouts  11.6 us (4%)
  other arithmetic  10.9 us (4%)
  matrix products  6.21 us (2%)
    pallas_call x1, Pallas kernels, expert_ring(): pl.pallas_call(kernel, out_shape=jax.ShapeDtypeStruct(block, jnp.bfloat16...  95.1 us
    all_gather x1, waiting for transfers between devices, shards(): key_blocks = lax.all_gather(bundle, 'sp', axis=0, tiled=False)  56.4 us
    pallas_call x1, Pallas kernels, flash_attention(): pl.pallas_call(kernel, out_shape=jax.ShapeDtypeStruct((shard_len, VH), jn...  22.8 us
    all_to_all x1, blocking collectives, shards(): lax.all_to_all(outbound, 'sp', split_axis=0, concat_axis=0, tiled=True)  20.9 us
    all_to_all x1, waiting for transfers between devices, shards(): lax.all_to_all(served, 'sp', split_axis=0, concat_axis=0, tiled=True)  14.2 us
    all_to_all x1, waiting for transfers between devices, shards(): lax.all_to_all(head_major, 'tp', split_axis=0, concat_axis=1, tiled=True)  8.78 us
    all_to_all x1, starting transfers between devices, shards(): lax.all_to_all(head_major, 'tp', split_axis=0, concat_axis=1, tiled=True)  8.74 us
    ppermute x1, starting transfers between devices, shards(): traded = lax.ppermute(sent, 'sp', mirror)  5.84 us
  transfers between devices with their start and end apart: 5, of which 5 were waited for; matrix products, arithmetic and copies ran while one was open for 1% of the time, Pallas kernels for 0%

profile of v1, /device:TPU:1, one launch (start us, length us, event | category | flops | bytes accessed | tf_op | source)
XLA Modules:
  0.0 288.2 jit_solution(16687816683631749083)
XLA Ops:
  6.6 1.5 fusion
  8.1 0.0 copy-start.13
  8.1 1.0 copy.54
  9.2 0.0 copy-start.7
  9.2 0.0 copy-start.15
  9.2 1.8 fusion.3
  11.0 0.3 fusion.15
  11.3 0.2 copy.51
  11.5 0.0 copy-start.14
  11.5 0.2 fusion.12
  11.8 0.3 fusion.16
  12.1 0.6 convolution_convert_fusion.2
  12.7 0.2 copy.55
  12.9 0.2 fusion.14
  13.1 2.5 fusion.38
  15.6 0.3 maximum_bitcast_fusion
  15.9 0.2 pad_maximum_fusion
  16.1 0.9 copy.56
  17.0 0.0 all-gather.3.cloned.1.call-update
  17.1 0.3 pad_maximum_fusion.1
  17.4 5.8 %collective-permute-start = (bf16[512,96]{1,0:T(8,128)(2,1)S(1)}, bf16[512,96]{1,0:T(8,128)(2,1)S(1)}, u32[]{:S(2)}, u32[]{:S(2)}) collective-permute-start(bf16[512,96]{1,0:T(8,128)(2,1)S(1)} %get-tuple-element.14), channel_id=1, source_target_pairs={{0,240},{16,224},{32,208},{48,192},{64,176},{80,160},{96,144},{112... | collective-permute-start | bytes 294920 | tf_op jit(solution)/shard_map/ppermute | solution.py:358
  23.2 0.1 copy.57
  23.3 0.1 reshape.427
  23.5 0.1 fusion.41
  23.6 0.1 mul.254
  23.7 0.2 reduce_window_sum.11
  23.8 1.8 collective-permute-done
  25.6 0.1 maximum_select_fusion.q_ref
  25.7 56.4 %all-gather.3.cloned.1.call-done = bf16[2560,1024]{1,0:T(8,128)(2,1)} async-done(((bf16[160,1024]{1,0:T(8,128)(2,1)}), bf16[2560,1024]{1,0:T(8,128)(2,1)}) %all-gather.3.cloned.1.call-update) | async-done | bytes 5242896 | tf_op jit(solution)/shard_map/all_gather | solution.py:351
  82.1 2.5 copy-done.4
  84.6 22.8 %shard_map.163 = bf16[1024,64]{1,0:T(8,128)(2,1)S(1)} custom-call(bf16[1024,96]{1,0:T(8,128)(2,1)S(1)} %maximum_select_fusion.q_ref, bf16[16,160,1024]{2,1,0:T(8,128)(2,1)S(1)} %bitcast.42), custom_call_target="tpu_custom_call" | custom-call | flops 3019898880 | bytes 6291456 | tf_op jit(solution)/shard_map/pallas_call | solution.py:111
  107.4 2.8 collective-permute-start.1
  110.1 0.2 select_reduce_fusion
  110.3 0.1 reduce_sum.94
  110.5 0.1 copy.58
  110.5 4.4 %collective-permute-done.1 = bf16[512,64]{1,0:T(8,128)(2,1)S(1)} collective-permute-done((bf16[512,64]{1,0:T(8,128)(2,1)S(1)}, bf16[512,64]{1,0:T(8,128)(2,1)S(1)}, u32[]{:S(2)}, u32[]{:S(2)}) %collective-permute-start.1) | collective-permute-done | bytes 65568 | tf_op jit(solution)/shard_map/ppermute | solution.py:365
  115.0 0.1 maximum_select_fusion.1
  115.1 0.9 reshape.441
  116.0 8.7 %all-to-all-start = ((bf16[16,2,2048]{2,1,0:T(2,128)(2,1)}), bf16[16,2,2048]{2,1,0:T(2,128)(2,1)S(1)}, u32[]{:S(2)}, u32[]{:S(2)}) async-start(bf16[16,2,2048]{2,1,0:T(2,128)(2,1)} %reshape.441), calls=%async_computation | async-start | bytes 262144 | tf_op jit(solution)/shard_map/all_to_all | solution.py:370
  124.7 0.1 fusion.40
  124.8 8.8 %all-to-all-done = bf16[16,2,2048]{2,1,0:T(2,128)(2,1)S(1)} async-done(((bf16[16,2,2048]{2,1,0:T(2,128)(2,1)}), bf16[16,2,2048]{2,1,0:T(2,128)(2,1)S(1)}, u32[]{:S(2)}, u32[]{:S(2)}) %all-to-all-start) | async-done | bytes 131104 | tf_op jit(solution)/shard_map/all_to_all | solution.py:370
  133.6 0.2 reshape.442
  133.8 0.2 fusion.17
  134.0 3.5 %convert_bitcast_fusion = bf16[64,16,2048]{2,0,1:T(8,128)(2,1)S(1)} fusion(bf16[16,64,2048]{2,1,0:T(8,128)(2,1)} %bitcast.43, bf16[16,64,64]{2,1,0:T(8,128)(2,1)S(1)} %reshape.442, f32[16,64]{1,0:T(8,128)S(1)} %mul.254, f32[64]{0:T(128)S(1)} %add_rsqrt_fusion.4), kind=kOutput, calls=%fused_computation.2 | convolution fusion | flops 270794752 | bytes 8524032 | tf_op jit(solution)/shard_map/tgc,gcd->tgd/dot_general | solution.py:374
  137.5 0.8 convert_reduce_fusion
  138.3 0.2 copy-done.5
  138.4 0.2 multiply_reduce_fusion.1
  138.6 0.4 convolution_convert_fusion
  139.0 0.2 reshape.428
  139.3 20.9 %all_to_all.20 = bf16[16,9,2048]{2,1,0:T(8,128)(2,1)} all-to-all(bf16[16,9,2048]{2,1,0:T(8,128)(2,1)S(1)} %reshape.428), channel_id=1, replica_groups=mesh['sp'=16,'tp'=16] {'sp'}, dimensions={0} | all-to-all | bytes 1179648 | tf_op jit(solution)/shard_map/all_to_all | solution.py:393
  160.2 1.5 reshape.429.x_ref
  161.7 95.1 %shard_map.164 = bf16[144,2048]{1,0:T(8,128)(2,1)S(1)} custom-call(bf16[144,2048]{1,0:T(8,128)(2,1)S(1)} %reshape.429.x_ref, bf16[2048,128]{1,0:T(8,128)(2,1)S(1)} %bitcast.39, bf16[2048,128]{1,0:T(8,128)(2,1)S(1)} %bitcast.40, bf16[128,2048]{1,0:T(8,128)(2,1)S(1)} %bitcast.41), custom_call_target="tpu_custom_call" | custom-call | tf_op jit(solution)/shard_map/pallas_call | solution.py:286
  256.9 1.2 reshape.430
  258.1 3.9 %all-to-all-start.2 = ((bf16[16,9,2048]{2,1,0:T(8,128)(2,1)}), bf16[16,9,2048]{2,1,0:T(8,128)(2,1)S(1)}, u32[]{:S(2)}, u32[]{:S(2)}) async-start(bf16[16,9,2048]{2,1,0:T(8,128)(2,1)} %reshape.430), calls=%async_computation.2 | async-start | bytes 2097152 | tf_op jit(solution)/shard_map/all_to_all | solution.py:399
  262.0 0.1 copy.60
  262.1 0.1 mul.265
  262.2 0.1 copy.59
  262.3 0.1 copy.61
  262.5 14.2 %all-to-all-done.2 = bf16[16,9,2048]{2,1,0:T(8,128)(2,1)S(1)} async-done(((bf16[16,9,2048]{2,1,0:T(8,128)(2,1)}), bf16[16,9,2048]{2,1,0:T(8,128)(2,1)S(1)}, u32[]{:S(2)}, u32[]{:S(2)}) %all-to-all-start.2) | async-done | bytes 589856 | tf_op jit(solution)/shard_map/all_to_all | solution.py:399
  276.7 0.3 reshape.431
  276.9 0.9 gather_fusion
  277.9 0.3 gather.7
  278.2 2.3 multiply_reduce_fusion
  280.6 0.8 add_convert_fusion
  (44 shorter events, 0.3 us)
Async XLA Ops:
  6.5 2.6 copy-start
  6.5 4.8 %copy-start.8 = (bf16[1024,96]{0,1:T(8,128)(2,1)S(1)}, bf16[1024,96]{0,1:T(8,128)(2,1)}, u32[]{:S(2)}) copy-start(bf16[1024,96]{0,1:T(8,128)(2,1)} %param.17) | copy-start | bytes 589828
  6.5 75.5 %all-gather.3.cloned.1.call-start = ((), (), s32[]{:S(2)}) async-start(), calls=%async_computation.3 | async-start | bytes 5570560 | tf_op jit(solution)/shard_map/all_gather | solution.py:351
  8.1 3.7 %copy-start.13 = (f32[96]{0:T(128)S(1)}, f32[96]{0:T(128)}, u32[]{:S(2)}) copy-start(f32[96]{0:T(128)} %param.24) | copy-start | bytes 1156
  9.2 2.9 %copy-start.7 = (bf16[1024,512]{1,0:T(8,128)(2,1)S(1)}, bf16[1024,512]{1,0:T(8,128)(2,1)}, u32[]{:S(2)}) copy-start(bf16[1024,512]{1,0:T(8,128)(2,1)} %param.18) | copy-start | bytes 3145732
  9.2 2.9 %copy-start.15 = (bf16[512,64]{0,1:T(8,128)(2,1)S(1)}, bf16[512,64]{0,1:T(8,128)(2,1)}, u32[]{:S(2)}) copy-start(bf16[512,64]{0,1:T(8,128)(2,1)} %param.22) | copy-start | bytes 196612
  9.2 2.9 %copy-start.16 = (f32[512]{0:T(512)S(1)}, f32[512]{0:T(512)}, u32[]{:S(2)}) copy-start(f32[512]{0:T(512)} %param.20) | copy-start | bytes 6148
  11.5 1.3 copy-start.14
  15.9 7.4 %copy-start.9 = (s32[64,2]{0,1:T(2,128)S(1)}, s32[64,2]{0,1:T(2,128)}, u32[]{:S(2)}) copy-start(s32[64,2]{0,1:T(2,128)} %param.29) | copy-start | bytes 1540
  15.9 7.7 %copy-start.11 = (f32[1024]{0:T(1024)S(1)}, f32[1024]{0:T(1024)}, u32[]{:S(2)}) copy-start(f32[1024]{0:T(1024)} %param.25) | copy-start | bytes 12292
  17.4 8.2 %collective-permute-start = (bf16[512,96]{1,0:T(8,128)(2,1)S(1)}, bf16[512,96]{1,0:T(8,128)(2,1)S(1)}, u32[]{:S(2)}, u32[]{:S(2)}) collective-permute-start(bf16[512,96]{1,0:T(8,128)(2,1)S(1)} %get-tuple-element.14), channel_id=1, source_target_pairs={{0,240},{16,224},{32,208},{48,192},{64,176},{80,160},{96,144},{112... | collective-permute-start | bytes 294920 | tf_op jit(solution)/shard_map/ppermute | solution.py:358
  82.1 2.5 copy-start.4
  107.4 7.6 %collective-permute-start.1 = (bf16[512,64]{1,0:T(8,128)(2,1)S(1)}, bf16[512,64]{1,0:T(8,128)(2,1)S(1)}, u32[]{:S(2)}, u32[]{:S(2)}) collective-permute-start(bf16[512,64]{1,0:T(8,128)(2,1)S(1)} %get-tuple-element.12), channel_id=1, source_target_pairs={{0,240},{16,224},{32,208},{48,192},{64,176},{80,160},{96,144},{112... | collective-permute-start | bytes 196616 | tf_op jit(solution)/shard_map/ppermute | solution.py:365
  116.0 17.6 %all-to-all-start = ((bf16[16,2,2048]{2,1,0:T(2,128)(2,1)}), bf16[16,2,2048]{2,1,0:T(2,128)(2,1)S(1)}, u32[]{:S(2)}, u32[]{:S(2)}) async-start(bf16[16,2,2048]{2,1,0:T(2,128)(2,1)} %reshape.441), calls=%async_computation | async-start | bytes 262144 | tf_op jit(solution)/shard_map/all_to_all | solution.py:370
  137.5 1.0 copy-start.5
  137.5 1.1 copy-start.10
  139.3 22.5 %copy-start.1 = (bf16[1,2048,128]{2,1,0:T(8,128)(2,1)S(1)}, bf16[1,2048,128]{2,1,0:T(8,128)(2,1)}, u32[]{:S(2)}) copy-start(bf16[1,2048,128]{2,1,0:T(8,128)(2,1)} %param.31) | copy-start | bytes 1572868
  139.3 22.5 %copy-start.2 = (bf16[1,2048,128]{2,1,0:T(8,128)(2,1)S(1)}, bf16[1,2048,128]{2,1,0:T(8,128)(2,1)}, u32[]{:S(2)}) copy-start(bf16[1,2048,128]{2,1,0:T(8,128)(2,1)} %param.32) | copy-start | bytes 1572868
  139.3 22.5 %copy-start.3 = (bf16[1,128,2048]{2,1,0:T(8,128)(2,1)S(1)}, bf16[1,128,2048]{2,1,0:T(8,128)(2,1)}, u32[]{:S(2)}) copy-start(bf16[1,128,2048]{2,1,0:T(8,128)(2,1)} %param.33) | copy-start | bytes 1572868
  256.9 5.5 %copy-start.12 = (f32[64,2]{0,1:T(2,128)S(1)}, f32[64,2]{0,1:T(2,128)}, u32[]{:S(2)}) copy-start(f32[64,2]{0,1:T(2,128)} %param.30) | copy-start | bytes 1540
  258.1 18.6 %all-to-all-start.2 = ((bf16[16,9,2048]{2,1,0:T(8,128)(2,1)}), bf16[16,9,2048]{2,1,0:T(8,128)(2,1)S(1)}, u32[]{:S(2)}, u32[]{:S(2)}) async-start(bf16[16,9,2048]{2,1,0:T(8,128)(2,1)} %reshape.430), calls=%async_computation.2 | async-start | bytes 2097152 | tf_op jit(solution)/shard_map/all_to_all | solution.py:399
  277.9 2.7 copy-start.6
Sparse Core Ops, SparseCore 0:
  17.2 64.8 all-gather.2

commit v2 on v1

--- a/solution.py
+++ b/solution.py
@@ -59,70 +59,291 @@
 
 SCORE_EXP = 1.4426950408889634 * QK ** (-0.5)
 Q_TILE = 256
-
-
-def attend_body(q_ref, kv_ref, out_ref, peak_ref, acc_ref, val_ref, block_count):
-    shard_len = kv_ref.shape[2]
+SIDE = 4
+VISITS = (
+    (0, 0), (1, 0), (3, 0), (0, 1), (0, 3), (1, 1), (1, 3), (3, 1),
+    (3, 3), (2, 0), (0, 2), (2, 1), (2, 3), (1, 2), (3, 2), (2, 2),
+)
+
+
+def attention(query_rows, bundle):
+    shard_len = query_rows.shape[0]
     half = shard_len // 2
-    mine = lax.axis_index("sp")
-    low = jnp.minimum(mine, block_count - 1 - mine)
-    high = block_count - 1 - low
-    shift = jnp.where(mine < block_count // 2, 0, half)
-    peak_ref[...] = jnp.full_like(peak_ref, -1e30)
-    acc_ref[...] = jnp.zeros_like(acc_ref)
-    lane = lax.broadcasted_iota(jnp.int32, (shard_len, 128), 1)
-    val_ref[...] = jnp.where(lane == VH, 1.0, 0.0).astype(jnp.bfloat16)
-
-    def one_block(block, parts):
-        keys = kv_ref[block, :QK, :]
-        val_ref[:, :VH] = kv_ref[block, QK:, :].T
-        values = val_ref[...]
-        for start, masked in parts:
-            for first in range(start, start + half, Q_TILE):
-                rows = pl.ds(first, Q_TILE)
-                scores = jnp.dot(q_ref[rows, :], keys, preferred_element_type=jnp.float32)
-                if masked:
-                    row = lax.broadcasted_iota(jnp.int32, scores.shape, 0)
-                    col = lax.broadcasted_iota(jnp.int32, scores.shape, 1)
-                    scores = jnp.where(col - row <= shift + (first - start), scores, -1e30)
-                old = peak_ref[rows, :]
-                new = jnp.maximum(old, jnp.max(scores, axis=1, keepdims=True))
-                weights = jnp.exp2((scores - new[:, :1]) * SCORE_EXP).astype(jnp.bfloat16)
-                factor = jnp.exp2((old - new) * SCORE_EXP)
-                peak_ref[rows, :] = new
-                acc_ref[rows, :] = acc_ref[rows, :] * factor + jnp.dot(
-                    weights, values, preferred_element_type=jnp.float32
-                )
-
-    lax.fori_loop(0, low, lambda j, _: one_block(j, ((0, False), (half, False))), None)
-    one_block(low, ((0, True), (half, False)))
-    lax.fori_loop(low + 1, high, lambda j, _: one_block(j, ((half, False),)), None)
-    one_block(high, ((half, True),))
-    total = acc_ref[:, VH : VH + 1]
-    out_ref[...] = (acc_ref[:, :VH] / total).astype(jnp.bfloat16)
-
-
-def flash_attention(query_pair, key_blocks, block_count):
-    shard_len = query_pair.shape[0]
-
-    def kernel(q_ref, kv_ref, out_ref, peak_ref, acc_ref, val_ref):
-        attend_body(q_ref, kv_ref, out_ref, peak_ref, acc_ref, val_ref, block_count)
+    block_count = lax.axis_size("sp")
+    tp_count = lax.axis_size("tp")
+    tok = shard_len // tp_count
+    bundle_rows = bundle.shape[0]
+    part_rows = bundle_rows // 2
+
+    def kernel(
+        q_ref, own_ref, out_ref,
+        kv_ref, pair_ref, peak_ref, acc_ref, val_ref, done_ref, tok_ref,
+        kv_send, kv_recv, q_send, q_recv, out_send, out_recv,
+    ):
+        mine = lax.axis_index("sp")
+        head = lax.axis_index("tp")
+        mirror = block_count - 1 - mine
+        low = jnp.minimum(mine, mirror)
+        high = jnp.maximum(mine, mirror)
+        shift = pl.multiple_of(jnp.where(mine < block_count // 2, 0, half), half)
+        rest = pl.multiple_of(half - shift, half)
+        row, col = mine // SIDE, mine % SIDE
+
+        def block_at(dx, dy):
+            return ((row + dy) % SIDE) * SIDE + (col + dx) % SIDE
+
+        barrier = pltpu.get_barrier_semaphore()
+
+        def greet(place, lane):
+            pl.semaphore_signal(
+                barrier,
+                inc=1,
+                device_id={"sp": place, "tp": lane},
+                device_id_type=pl.DeviceIdType.MESH,
+            )
+
+        for dx, dy in ((1, 0), (3, 0), (0, 1), (0, 3)):
+            greet(block_at(dx, dy), head)
+        for other in range(tp_count):
+            greet(mirror, other)
+
+            @pl.when(other != head)
+            def _():
+                greet(mine, other)
+
+        pl.semaphore_wait(barrier, 4 + 2 * tp_count - 1)
+
+        def remote(source, target, send, recv, place, lane):
+            return pltpu.make_async_remote_copy(
+                src_ref=source,
+                dst_ref=target,
+                send_sem=send,
+                recv_sem=recv,
+                device_id={"sp": place, "tp": lane},
+                device_id_type=pl.DeviceIdType.MESH,
+            )
+
+        def trade():
+            return remote(q_ref.at[pl.ds(rest, half)], pair_ref.at[pl.ds(shift, half)],
+                          q_send.at[0], q_recv.at[0], mirror, head)
+
+        def traded():
+            return remote(q_ref.at[pl.ds(rest, half)], pair_ref.at[pl.ds(rest, half)],
+                          q_send.at[0], q_recv.at[0], mirror, head)
+
+        def at(part, along, across):
+            return (along, across) if part == 0 else (across, along)
+
+        def piece(part, where, way, own=False, side=None):
+            block = block_at(*where)
+            rows = pl.ds(part * part_rows, part_rows)
+            cols = slice(None) if side is None else pl.ds(side * half, half)
+            index = (part * block_count + block) * 2
+            source = own_ref.at[rows] if own else kv_ref.at[block, rows, cols]
+            compass = ((1, 0), (3, 0), (0, 1), (0, 3)).index(way)
+            return remote(source, kv_ref.at[block, rows, cols],
+                          kv_send.at[index * 2 + compass],
+                          kv_recv.at[index + (0 if side is None else side)],
+                          block_at(*way), head)
+
+        def landed(part, where, side=None):
+            piece(part, where, (1, 0), side=side).wait_recv()
+
+        sent = []
+
+        def push(part, where, way, own=False, side=None):
+            piece(part, where, way, own, side).start()
+            sent.append((part, where, way, own, side))
+
+        def spread(part, where):
+            push(part, where, at(part, 0, 1))
+            push(part, where, at(part, 0, 3))
+
+        def neighbours_first():
+            for part in (0, 1):
+                for along, side, way in ((3, 0, 1), (1, 1, 3)):
+                    landed(part, at(part, along, 0))
+                    push(part, at(part, along, 0), at(part, way, 0), side=side)
+                    spread(part, at(part, along, 0))
+
+        def pass_across(alongs):
+            for part in (0, 1):
+                for along in alongs:
+                    for across, side, way in ((3, 0, 1), (1, 1, 3)):
+                        landed(part, at(part, along, across))
+                        push(part, at(part, along, across), at(part, 0, way), side=side)
+
+        def far_first():
+            for part in (0, 1):
+                landed(part, at(part, 2, 0), 0)
+                landed(part, at(part, 2, 0), 1)
+                spread(part, at(part, 2, 0))
+
+        def far_across(alongs):
+            for part in (0, 1):
+                for along in alongs:
+                    landed(part, at(part, along, 2), 0)
+                    landed(part, at(part, along, 2), 1)
+
+        trade().start()
+        for part in (0, 1):
+            push(part, (0, 0), at(part, 1, 0), own=True)
+            push(part, (0, 0), at(part, 3, 0), own=True)
+        for part in (0, 1):
+            push(part, (0, 0), at(part, 0, 1), own=True)
+            push(part, (0, 0), at(part, 0, 3), own=True)
+        kv_ref[mine] = own_ref[...]
+        pair_ref[pl.ds(shift, half), :] = q_ref[pl.ds(shift, half), :]
+        peak_ref[...] = jnp.full_like(peak_ref, -1e30)
+        acc_ref[...] = jnp.zeros_like(acc_ref)
+        lane = lax.broadcasted_iota(jnp.int32, (shard_len, 128), 1)
+        val_ref[...] = jnp.where(lane == VH, 1.0, 0.0).astype(jnp.bfloat16)
+
+        def attend(block, parts):
+            keys = kv_ref[block, :QK, :]
+            val_ref[:, :VH] = kv_ref[block, QK:, :].T
+            values = val_ref[...]
+            for start, masked in parts:
+                for first in range(start, start + half, Q_TILE):
+                    rows = pl.ds(first, Q_TILE)
+                    scores = jnp.dot(pair_ref[rows, :], keys, preferred_element_type=jnp.float32)
+                    if masked:
+                        q_pos = lax.broadcasted_iota(jnp.int32, scores.shape, 0)
+                        k_pos = lax.broadcasted_iota(jnp.int32, scores.shape, 1)
+                        scores = jnp.where(
+                            k_pos - q_pos <= shift + (first - start), scores, -1e30
+                        )
+                    old = peak_ref[rows, :]
+                    new = jnp.maximum(old, jnp.max(scores, axis=1, keepdims=True))
+                    weights = jnp.exp2((scores - new[:, :1]) * SCORE_EXP).astype(jnp.bfloat16)
+                    factor = jnp.exp2((old - new) * SCORE_EXP)
+                    peak_ref[rows, :] = new
+                    acc_ref[rows, :] = acc_ref[rows, :] * factor + jnp.dot(
+                        weights, values, preferred_element_type=jnp.float32
+                    )
+
+        def visit(step, _):
+            @pl.when(step == 0)
+            def _():
+                neighbours_first()
+                traded().wait_recv()
+
+            @pl.when(step == 1)
+            def _():
+                pass_across((0,))
+
+            @pl.when(step == 2)
+            def _():
+                far_first()
+
+            @pl.when(step == 5)
+            def _():
+                pass_across((1, 3))
+
+            @pl.when(step == 9)
+            def _():
+                far_across((0,))
+                pass_across((2,))
+
+            @pl.when(step == 11)
+            def _():
+                far_across((1, 3))
+
+            @pl.when(step == 15)
+            def _():
+                far_across((2,))
+
+            dx = sum(jnp.where(step == k, v[0], 0) for k, v in enumerate(VISITS) if v[0])
+            dy = sum(jnp.where(step == k, v[1], 0) for k, v in enumerate(VISITS) if v[1])
+            block = block_at(dx, dy)
+
+            @pl.when(block < low)
+            def _():
+                attend(block, ((0, False), (half, False)))
+
+            @pl.when(block == low)
+            def _():
+                attend(block, ((0, True), (half, False)))
+
+            @pl.when((block > low) & (block < high))
+            def _():
+                attend(block, ((half, False),))
+
+            @pl.when(block == high)
+            def _():
+                attend(block, ((half, True),))
+
+        lax.fori_loop(0, block_count, visit, None)
+        done_ref[...] = (acc_ref[:, :VH] / acc_ref[:, VH : VH + 1]).astype(jnp.bfloat16)
+
+        first_lane = shift // tok
+
+        def result(index):
+            side, order = index // (tp_count // 2), index % (tp_count // 2)
+            own_side = jnp.where(side == 0, shift, rest)
+            start = pl.multiple_of(own_side + order * tok, tok)
+            return remote(done_ref.at[pl.ds(start, tok)], tok_ref.at[head],
+                          out_send.at[index], out_recv.at[head],
+                          jnp.where(side == 0, mine, mirror), first_lane + order)
+
+        here = (head >= first_lane) & (head < first_lane + tp_count // 2)
+        self_index = jnp.where(here, head - first_lane, tp_count)
+
+        def send_result(index, _):
+            @pl.when(index != self_index)
+            def _():
+                result(index).start()
+
+        lax.fori_loop(0, tp_count, send_result, None)
+
+        @pl.when(here)
+        def _():
+            tok_ref[head] = done_ref[pl.ds(pl.multiple_of(head * tok, tok), tok), :]
+
+        def take_result(index, _):
+            @pl.when(jnp.logical_not(here & (index == head)))
+            def _():
+                remote(done_ref.at[pl.ds(0, tok)], tok_ref.at[index],
+                       out_send.at[index], out_recv.at[index], mirror, head).wait_recv()
+
+        lax.fori_loop(0, tp_count, take_result, None)
+        out_ref[...] = tok_ref[...]
+
+        trade().wait_send()
+        for message in sent:
+            piece(*message).wait_send()
+
+        def drain(index, _):
+            @pl.when(index != self_index)
+            def _():
+                result(index).wait_send()
+
+        lax.fori_loop(0, tp_count, drain, None)
 
     return pl.pallas_call(
         kernel,
-        out_shape=jax.ShapeDtypeStruct((shard_len, VH), jnp.bfloat16),
+        out_shape=jax.ShapeDtypeStruct((tp_count, tok, VH), jnp.bfloat16),
         in_specs=[pl.BlockSpec(memory_space=pltpu.VMEM)] * 2,
         out_specs=pl.BlockSpec(memory_space=pltpu.VMEM),
         scratch_shapes=[
+            pltpu.VMEM((block_count, bundle_rows, shard_len), jnp.bfloat16),
+            pltpu.VMEM((shard_len, QK), jnp.bfloat16),
             pltpu.VMEM((shard_len, 128), jnp.float32),
             pltpu.VMEM((shard_len, 128), jnp.float32),
             pltpu.VMEM((shard_len, 128), jnp.bfloat16),
+            pltpu.VMEM((shard_len, VH), jnp.bfloat16),
+            pltpu.VMEM((tp_count, tok, VH), jnp.bfloat16),
+            pltpu.SemaphoreType.DMA((block_count * 8,)),
+            pltpu.SemaphoreType.DMA((block_count * 4,)),
+            pltpu.SemaphoreType.DMA((1,)),
+            pltpu.SemaphoreType.DMA((1,)),
+            pltpu.SemaphoreType.DMA((tp_count,)),
+            pltpu.SemaphoreType.DMA((tp_count,)),
         ],
-        compiler_params=pltpu.CompilerParams(vmem_limit_bytes=40 * 1024 * 1024),
-        cost_estimate=pl.CostEstimate(
-            flops=9 * shard_len * shard_len * 320, bytes_accessed=6 << 20, transcendentals=9 << 20
+        compiler_params=pltpu.CompilerParams(
+            collective_id=4, has_side_effects=True, vmem_limit_bytes=40 * 1024 * 1024
         ),
-    )(query_pair, key_blocks)
+    )(query_rows, bundle)
 
 
 ROW_CUT = 80
@@ -348,28 +569,9 @@
         queries.astype(jnp.float32).reshape(shard_len, local_heads, QK), query_gain, angles
     )
     bundle = jnp.concatenate([key_rows.reshape(shard_len, QK).T, value_rows.T], axis=0)
-    key_blocks = lax.all_gather(bundle, "sp", axis=0, tiled=False)
-    low_side = lax.axis_index("sp") < sp_count // 2
-    half = shard_len // 2
-    query_rows = query_rows.reshape(shard_len, QK)
-    mirror = [(place, sp_count - 1 - place) for place in range(sp_count)]
-    kept = jnp.where(low_side, query_rows[:half], query_rows[half:])
-    sent = jnp.where(low_side, query_rows[half:], query_rows[:half])
-    traded = lax.ppermute(sent, "sp", mirror)
-    query_pair = jnp.where(
-        low_side, jnp.concatenate([kept, traded]), jnp.concatenate([traded, kept])
-    )
-    pair_out = flash_attention(query_pair, key_blocks, sp_count)
-    own_out = jnp.where(low_side, pair_out[:half], pair_out[half:])
-    other_out = jnp.where(low_side, pair_out[half:], pair_out[:half])
-    traded_out = lax.ppermute(other_out, "sp", mirror)
-    head_major = jnp.where(
-        low_side, jnp.concatenate([own_out, traded_out]), jnp.concatenate([traded_out, own_out])
-    )
     tok_count = residual.shape[0]
-    token_rows = lax.all_to_all(head_major, "tp", split_axis=0, concat_axis=1, tiled=True).astype(
-        jnp.float32
-    )
+    by_head = attention(query_rows.reshape(shard_len, QK), bundle)
+    token_rows = jnp.transpose(by_head, (1, 0, 2)).reshape(tok_count, -1).astype(jnp.float32)
     normed_rows = (token_rows * rms_scale(token_rows) * out_gain).astype(jnp.bfloat16)
     partials = jnp.einsum(
         "tgc,gcd->tgd",

time: 291 us -> 232 us (0.80)
  waiting for transfers between devices: 85.6 us -> 15.4 us
  Pallas kernels: 118 us -> 165 us
  starting transfers between devices: 21.2 us -> 4.43 us
  between operations: 13.9 us -> 0.47 us
  local copies, waits for them, and re-layouts: 11.6 us -> 5.88 us
  other arithmetic: 10.9 us -> 7.09 us
  blocking collectives: 20.9 us -> 24.3 us
    all_gather x1 -> x0, waiting for transfers between devices: 56.4 us -> none  [shards(): key_blocks = lax.all_gather(bundle, 'sp', axis=0, tiled=False)]
    pallas_call x1, Pallas kernels: 22.8 us -> 65.6 us  [attention(): pl.pallas_call(kernel, out_shape=jax.ShapeDtypeStruct((tp_count, tok, VH)...]
    all_to_all x1 -> x0, waiting for transfers between devices: 8.78 us -> none  [shards(): lax.all_to_all(head_major, 'tp', split_axis=0, concat_axis=1, tiled=True)]
    all_to_all x1 -> x0, starting transfers between devices: 8.74 us -> none  [shards(): lax.all_to_all(head_major, 'tp', split_axis=0, concat_axis=1, tiled=True)]
    ppermute x2 -> x0, starting transfers between devices: 8.62 us -> none  [the longest x1 5.84 us: shards(): traded = lax.ppermute(sent, 'sp', mirror)]
    ppermute x2 -> x0, waiting for transfers between devices: 6.21 us -> none  [the longest x1 4.44 us: shards(): traded_out = lax.ppermute(other_out, 'sp', mirror)]
    unnamed x40 -> x36, local copies, waits for them, and re-layouts: 5.21 us -> 0.43 us
    pallas_call x1, Pallas kernels: 95.1 us -> 99.5 us  [expert_ring(): pl.pallas_call(kernel, out_shape=jax.ShapeDtypeStruct(block, jnp.bfloat16...]
  transfers between devices with their start and end apart: 5 -> 1, of which waited for: 5 -> 1; matrix products, arithmetic and copies ran while one was open for 1% -> 0% of each run, Pallas kernels for 0% -> 0%
where the time goes in v2:
time: 232 us; the launch traced here: 229 us
  Pallas kernels  165 us (71%)
  blocking collectives  24.3 us (10%)
  waiting for transfers between devices  15.4 us (7%)
  other arithmetic  7.09 us (3%)
  matrix products  6.26 us (3%)
  local copies, waits for them, and re-layouts  5.88 us (3%)
  starting transfers between devices  4.43 us (2%)
    pallas_call x1, Pallas kernels, expert_ring(): pl.pallas_call(kernel, out_shape=jax.ShapeDtypeStruct(block, jnp.bfloat16...  99.5 us
    pallas_call x1, Pallas kernels, attention(): pl.pallas_call(kernel, out_shape=jax.ShapeDtypeStruct((tp_count, tok, VH)...  65.6 us
    all_to_all x1, blocking collectives, shards(): lax.all_to_all(outbound, 'sp', split_axis=0, concat_axis=0, tiled=True)  24.3 us
    all_to_all x1, waiting for transfers between devices, shards(): lax.all_to_all(served, 'sp', split_axis=0, concat_axis=0, tiled=True)  15.4 us
  transfers between devices with their start and end apart: 1, of which 1 were waited for; matrix products, arithmetic and copies ran while one was open for 0% of the time, Pallas kernels for 0%

profile of v2, /device:TPU:1, one launch (start us, length us, event | category | flops | bytes accessed | tf_op | source)
XLA Modules:
  0.0 229.0 jit_solution(9106896216346068480)
XLA Ops:
  0.0 0.0 copy-start
  0.0 0.0 copy-start.13
  0.0 0.0 copy-start.14
  0.1 1.6 fusion
  1.6 0.0 copy-start.6
  1.6 0.0 copy-start.15
  1.7 0.0 copy-start.16
  1.7 0.0 copy-done
  1.7 1.9 fusion.3
  3.5 0.0 copy-done.8
  3.6 0.1 fusion.11
  3.6 0.0 copy-done.7
  3.6 0.1 fusion.8
  3.7 0.0 copy-done.13
  3.7 0.1 fusion.12
  3.9 0.1 fusion.10
  4.0 0.5 fusion.4
  4.6 0.0 copy-start.11
  4.6 0.3 fusion.43
  5.0 0.2 copy.31.q_ref
  5.2 65.6 %shard_map.163 = bf16[16,64,64]{2,1,0:T(8,128)(2,1)S(1)} custom-call(bf16[1024,96]{1,0:T(8,128)(2,1)S(1)} %copy.31.q_ref, bf16[160,1024]{1,0:T(8,128)(2,1)S(1)} %pad_maximum_fusion.own_ref), custom_call_target="tpu_custom_call" | custom-call | tf_op jit(solution)/shard_map/pallas_call | solution.py:323
  70.8 0.2 fusion.5
  70.9 0.1 mul.254
  71.0 3.5 %convert_bitcast_fusion = bf16[64,16,2048]{2,0,1:T(8,128)(2,1)S(1)} fusion(bf16[16,64,2048]{2,1,0:T(8,128)(2,1)} %bitcast.43, bf16[16,64,64]{2,1,0:T(8,128)(2,1)S(1)} %shard_map.163, f32[16,64]{1,0:T(8,128)S(1)} %mul.254, f32[64]{0:T(128)S(1)} %add_rsqrt_fusion.4), kind=kOutput, calls=%fused_computation.2 | convolution fusion | flops 270794752 | bytes 8524032 | tf_op jit(solution)/shard_map/tgc,gcd->tgd/dot_general | solution.py:576
  74.5 0.0 copy-start.4
  74.5 0.0 copy-start.9
  74.5 0.0 copy-start.10
  74.5 0.8 convert_reduce_fusion
  75.3 0.1 copy-done.4
  75.5 0.2 multiply_reduce_fusion.1
  75.7 0.1 copy.32
  75.8 0.1 reshape.394
  75.9 0.1 fusion.41
  76.0 0.2 reduce_window_sum.11
  76.2 0.2 select_reduce_fusion
  76.3 0.1 reduce_sum.94
  76.5 0.1 copy.33
  76.6 0.1 fusion.40
  76.7 0.4 convolution_convert_fusion
  77.1 0.2 reshape.395
  77.3 0.0 copy-start.1
  77.3 0.0 copy-start.2
  77.3 0.0 copy-start.3
  77.3 24.3 %all_to_all.10 = bf16[16,9,2048]{2,1,0:T(8,128)(2,1)} all-to-all(bf16[16,9,2048]{2,1,0:T(8,128)(2,1)S(1)} %reshape.395), channel_id=1, replica_groups=mesh['sp'=16,'tp'=16] {'sp'}, dimensions={0} | all-to-all | bytes 1179648 | tf_op jit(solution)/shard_map/all_to_all | solution.py:595
  101.7 1.5 reshape.396.x_ref
  103.2 0.0 copy-done.1
  103.2 0.0 copy-done.2
  103.2 0.0 copy-done.3
  103.2 99.5 %shard_map.164 = bf16[144,2048]{1,0:T(8,128)(2,1)S(1)} custom-call(bf16[144,2048]{1,0:T(8,128)(2,1)S(1)} %reshape.396.x_ref, bf16[2048,128]{1,0:T(8,128)(2,1)S(1)} %bitcast.40, bf16[2048,128]{1,0:T(8,128)(2,1)S(1)} %bitcast.41, bf16[128,2048]{1,0:T(8,128)(2,1)S(1)} %bitcast.42), custom_call_target="tpu_custom_call" | custom-call | tf_op jit(solution)/shard_map/pallas_call | solution.py:507
  202.7 0.0 copy-start.12
  202.7 1.2 reshape.397
  204.0 4.4 %all-to-all-start.1 = ((bf16[16,9,2048]{2,1,0:T(8,128)(2,1)}), bf16[16,9,2048]{2,1,0:T(8,128)(2,1)S(1)}, u32[]{:S(2)}, u32[]{:S(2)}) async-start(bf16[16,9,2048]{2,1,0:T(8,128)(2,1)} %reshape.397), calls=%async_computation.1 | async-start | bytes 2097152 | tf_op jit(solution)/shard_map/all_to_all | solution.py:601
  208.4 0.1 copy.35
  208.5 0.1 mul.265
  208.7 0.1 copy.34
  208.8 0.1 copy.36
  208.9 15.4 %all-to-all-done.1 = bf16[16,9,2048]{2,1,0:T(8,128)(2,1)S(1)} async-done(((bf16[16,9,2048]{2,1,0:T(8,128)(2,1)}), bf16[16,9,2048]{2,1,0:T(8,128)(2,1)S(1)}, u32[]{:S(2)}, u32[]{:S(2)}) %all-to-all-start.1) | async-done | bytes 589856 | tf_op jit(solution)/shard_map/all_to_all | solution.py:601
  224.3 0.3 reshape.398
  224.6 0.9 gather_fusion
  225.5 0.0 copy-start.5
  225.5 0.3 gather.7
  225.9 2.3 %multiply_reduce_fusion = f32[64,2048]{1,0:T(8,128)S(1)} fusion(bf16[64,2,2048]{2,1,0:T(2,128)(2,1)S(1)} %gather.7, pred[64,2]{1,0:T(8,128)(4,1)S(1)} %copy.34, f32[64,2]{1,0:T(8,128)S(1)} %copy.36), kind=kLoop, calls=%fused_computation.13 | loop fusion | flops 917504 | bytes 1049216 | tf_op jit(solution)/shard_map/reduce_sum | solution.py:609
  228.2 0.0 copy-done.5
  228.2 0.8 add_convert_fusion
  (25 shorter events, 0.2 us)
Async XLA Ops:
  0.0 1.7 copy-start
  0.0 3.5 %copy-start.8 = (bf16[1024,32]{0,1:T(8,128)(2,1)S(1)}, bf16[1024,32]{0,1:T(8,128)(2,1)}, u32[]{:S(2)}) copy-start(bf16[1024,32]{0,1:T(8,128)(2,1)} %param.19) | copy-start | bytes 196612
  0.0 3.6 %copy-start.7 = (bf16[1024,96]{0,1:T(8,128)(2,1)S(1)}, bf16[1024,96]{0,1:T(8,128)(2,1)}, u32[]{:S(2)}) copy-start(bf16[1024,96]{0,1:T(8,128)(2,1)} %param.17) | copy-start | bytes 589828
  0.0 3.7 %copy-start.13 = (f32[96]{0:T(128)S(1)}, f32[96]{0:T(128)}, u32[]{:S(2)}) copy-start(f32[96]{0:T(128)} %param.24) | copy-start | bytes 1156
  0.0 3.8 %copy-start.14 = (f32[96]{0:T(128)S(1)}, f32[96]{0:T(128)}, u32[]{:S(2)}) copy-start(f32[96]{0:T(128)} %param.23) | copy-start | bytes 1156
  1.6 2.4 %copy-start.6 = (bf16[1024,512]{1,0:T(8,128)(2,1)S(1)}, bf16[1024,512]{1,0:T(8,128)(2,1)}, u32[]{:S(2)}) copy-start(bf16[1024,512]{1,0:T(8,128)(2,1)} %param.18) | copy-start | bytes 3145732
  1.6 2.4 %copy-start.15 = (bf16[512,64]{0,1:T(8,128)(2,1)S(1)}, bf16[512,64]{0,1:T(8,128)(2,1)}, u32[]{:S(2)}) copy-start(bf16[512,64]{0,1:T(8,128)(2,1)} %param.22) | copy-start | bytes 196612
  1.7 2.4 %copy-start.16 = (f32[512]{0:T(512)S(1)}, f32[512]{0:T(512)}, u32[]{:S(2)}) copy-start(f32[512]{0:T(512)} %param.20) | copy-start | bytes 6148
  4.6 66.4 %copy-start.11 = (f32[1024]{0:T(1024)S(1)}, f32[1024]{0:T(1024)}, u32[]{:S(2)}) copy-start(f32[1024]{0:T(1024)} %param.25) | copy-start | bytes 12292
  74.5 1.0 copy-start.4
  74.5 1.1 copy-start.9
  74.5 2.1 copy-start.10
  77.3 25.9 %copy-start.1 = (bf16[1,2048,128]{2,1,0:T(8,128)(2,1)S(1)}, bf16[1,2048,128]{2,1,0:T(8,128)(2,1)}, u32[]{:S(2)}) copy-start(bf16[1,2048,128]{2,1,0:T(8,128)(2,1)} %param.31) | copy-start | bytes 1572868
  77.3 25.8 %copy-start.2 = (bf16[1,2048,128]{2,1,0:T(8,128)(2,1)S(1)}, bf16[1,2048,128]{2,1,0:T(8,128)(2,1)}, u32[]{:S(2)}) copy-start(bf16[1,2048,128]{2,1,0:T(8,128)(2,1)} %param.32) | copy-start | bytes 1572868
  77.3 25.8 %copy-start.3 = (bf16[1,128,2048]{2,1,0:T(8,128)(2,1)S(1)}, bf16[1,128,2048]{2,1,0:T(8,128)(2,1)}, u32[]{:S(2)}) copy-start(bf16[1,128,2048]{2,1,0:T(8,128)(2,1)} %param.33) | copy-start | bytes 1572868
  202.7 6.0 %copy-start.12 = (f32[64,2]{0,1:T(2,128)S(1)}, f32[64,2]{0,1:T(2,128)}, u32[]{:S(2)}) copy-start(f32[64,2]{0,1:T(2,128)} %param.30) | copy-start | bytes 1540
  204.0 20.4 %all-to-all-start.1 = ((bf16[16,9,2048]{2,1,0:T(8,128)(2,1)}), bf16[16,9,2048]{2,1,0:T(8,128)(2,1)S(1)}, u32[]{:S(2)}, u32[]{:S(2)}) async-start(bf16[16,9,2048]{2,1,0:T(8,128)(2,1)} %reshape.397), calls=%async_computation.1 | async-start | bytes 2097152 | tf_op jit(solution)/shard_map/all_to_all | solution.py:601
  225.5 2.7 %copy-start.5 = (bf16[64,2048]{1,0:T(8,128)(2,1)S(1)}, bf16[64,2048]{1,0:T(8,128)(2,1)}, u32[]{:S(2)}) copy-start(bf16[64,2048]{1,0:T(8,128)(2,1)} %param.27) | copy-start | bytes 786436

commit v3 on v2

--- a/solution.py
+++ b/solution.py
@@ -52,11 +52,6 @@
     return (flat_routes * slot_cap + rank_in).reshape(route_rows.shape)
 
 
-def select_matrix(targets, slot_total):
-    hits = targets[:, :, None] == jnp.arange(slot_total, dtype=jnp.int32)[None, None, :]
-    return jnp.sum(hits.astype(jnp.bfloat16), axis=1)
-
-
 SCORE_EXP = 1.4426950408889634 * QK ** (-0.5)
 Q_TILE = 256
 SIDE = 4
@@ -206,7 +201,9 @@
             for start, masked in parts:
                 for first in range(start, start + half, Q_TILE):
                     rows = pl.ds(first, Q_TILE)
-                    scores = jnp.dot(pair_ref[rows, :], keys, preferred_element_type=jnp.float32)
+                    scores = jnp.dot(
+                        pair_ref[rows, :QK], keys, preferred_element_type=jnp.float32
+                    )
                     if masked:
                         q_pos = lax.broadcasted_iota(jnp.int32, scores.shape, 0)
                         k_pos = lax.broadcasted_iota(jnp.int32, scores.shape, 1)
@@ -274,7 +271,7 @@
                 attend(block, ((half, True),))
 
         lax.fori_loop(0, block_count, visit, None)
-        done_ref[...] = (acc_ref[:, :VH] / acc_ref[:, VH : VH + 1]).astype(jnp.bfloat16)
+        done_ref[...] = (acc_ref[...] / acc_ref[:, VH : VH + 1]).astype(jnp.bfloat16)
 
         first_lane = shift // tok
 
@@ -307,7 +304,7 @@
                        out_send.at[index], out_recv.at[index], mirror, head).wait_recv()
 
         lax.fori_loop(0, tp_count, take_result, None)
-        out_ref[...] = tok_ref[...]
+        out_ref[...] = tok_ref[:, :, :VH]
 
         trade().wait_send()
         for message in sent:
@@ -327,12 +324,12 @@
         out_specs=pl.BlockSpec(memory_space=pltpu.VMEM),
         scratch_shapes=[
             pltpu.VMEM((block_count, bundle_rows, shard_len), jnp.bfloat16),
-            pltpu.VMEM((shard_len, QK), jnp.bfloat16),
+            pltpu.VMEM((shard_len, 128), jnp.bfloat16),
             pltpu.VMEM((shard_len, 128), jnp.float32),
             pltpu.VMEM((shard_len, 128), jnp.float32),
             pltpu.VMEM((shard_len, 128), jnp.bfloat16),
-            pltpu.VMEM((shard_len, VH), jnp.bfloat16),
-            pltpu.VMEM((tp_count, tok, VH), jnp.bfloat16),
+            pltpu.VMEM((shard_len, 128), jnp.bfloat16),
+            pltpu.VMEM((tp_count, tok, 128), jnp.bfloat16),
             pltpu.SemaphoreType.DMA((block_count * 8,)),
             pltpu.SemaphoreType.DMA((block_count * 4,)),
             pltpu.SemaphoreType.DMA((1,)),
@@ -349,15 +346,22 @@
 ROW_CUT = 80
 
 
-def expert_ring(rows, gate, up, down):
-    count, width = rows.shape
+def expert_ring(chooser, ffn_input, gate, up, down, near_weights, middle):
+    count = chooser.shape[0]
+    width = ffn_input.shape[1]
+    places = lax.axis_size("sp")
+    slots = count // places
+    chunks = width // 128
+    slab = slots * chunks
     hidden = gate.shape[1]
     chips = lax.axis_size("tp") // 2
     both = 2 * count
 
     def kernel(
-        x_ref, gate_ref, up_ref, down_ref, out_ref,
-        both_ref, seen, own_part, far_part, near_part, run_in, run_out,
+        choose_ref, token_ref, gate_ref, up_ref, down_hbm, mix_ref, middle_ref, out_ref,
+        wide_ref, load_sem, away_ref, got_ref, home_ref, back_ref, ret_ref, x_ref,
+        away_send, away_recv, home_send, home_recv,
+        both_ref, down_ref, seen, own_part, far_part, near_part, run_in, run_out,
         fwd_send, fwd_recv, back_send, back_recv, twin_send, twin_recv,
         part_send, part_recv, sum_fwd_send, sum_fwd_recv, sum_back_send, sum_back_recv,
     ):
@@ -373,7 +377,66 @@
             pl.semaphore_signal(
                 barrier, inc=1, device_id={"tp": other}, device_id_type=pl.DeviceIdType.MESH
             )
-        pl.semaphore_wait(barrier, 3)
+        mine = lax.axis_index("sp")
+
+        def peer(turn):
+            return (mine + turn) % places
+
+        def greet(turn, _):
+            pl.semaphore_signal(
+                barrier, inc=1, device_id={"sp": peer(turn)}, device_id_type=pl.DeviceIdType.MESH
+            )
+
+        lax.fori_loop(1, places, greet, None)
+        loads = (
+            pltpu.make_async_copy(gate_ref, both_ref.at[:, pl.ds(0, hidden)], load_sem.at[0]),
+            pltpu.make_async_copy(up_ref, both_ref.at[:, pl.ds(hidden, hidden)], load_sem.at[1]),
+            pltpu.make_async_copy(down_hbm, down_ref, load_sem.at[2]),
+        )
+        for load in loads:
+            load.start()
+        chosen = jnp.dot(choose_ref[...], token_ref[...], preferred_element_type=jnp.float32)
+        for chunk in range(chunks):
+            wide_ref[pl.ds(chunk, count, stride=chunks), :] = chosen[
+                :, chunk * 128 : (chunk + 1) * 128
+            ]
+        away_ref[...] = wide_ref[...].astype(jnp.bfloat16)
+        pl.semaphore_wait(barrier, 3 + places - 1)
+
+        def slab_of(place):
+            return pl.ds(pl.multiple_of(place * slab, slab), slab)
+
+        def swap(source, target, send, recv, turn):
+            return pltpu.make_async_remote_copy(
+                src_ref=source.at[slab_of(peer(turn))],
+                dst_ref=target.at[slab_of(mine)],
+                send_sem=send.at[turn],
+                recv_sem=recv.at[turn],
+                device_id={"sp": peer(turn)},
+                device_id_type=pl.DeviceIdType.MESH,
+            )
+
+        def exchange(source, target, send, recv):
+            def start(turn, _):
+                swap(source, target, send, recv, turn).start()
+
+            lax.fori_loop(1, places, start, None)
+            target[slab_of(mine), :] = source[slab_of(mine), :]
+
+            def finish(turn, _):
+                swap(source, target, send, recv, turn).wait_recv()
+
+            lax.fori_loop(1, places, finish, None)
+
+        def narrow(target):
+            for chunk in range(chunks):
+                target[:, pl.ds(chunk * 128, 128)] = wide_ref[
+                    pl.ds(chunk, count, stride=chunks), :
+                ].astype(jnp.bfloat16)
+
+        exchange(away_ref, got_ref, away_send, away_recv)
+        wide_ref[...] = got_ref[...].astype(jnp.float32)
+        narrow(x_ref)
 
         def remote(source, target, send, recv, other):
             return pltpu.make_async_remote_copy(
@@ -434,8 +497,8 @@
 
         for copy in (*forward_own(), share_own()):
             copy.start()
-        both_ref[:, :hidden] = gate_ref[...]
-        both_ref[:, hidden:] = up_ref[...]
+        for load in loads:
+            load.wait()
         seen[0, front, :] = x_ref[...]
         share_own().wait_recv()
         experts(0)
@@ -480,11 +543,32 @@
         hand_over(0).wait_recv()
         for copy in pass_sum(chips - 1):
             copy.wait_recv()
-        out_ref[...] = (
+        served = (
             run_in[chips].astype(jnp.float32)
             + own_part[0].astype(jnp.float32)
             + near_part[0].astype(jnp.float32)
+        )
+        for chunk in range(chunks):
+            wide_ref[pl.ds(chunk, count, stride=chunks), :] = served[
+                :, chunk * 128 : (chunk + 1) * 128
+            ]
+        home_ref[...] = wide_ref[...].astype(jnp.bfloat16)
+        exchange(home_ref, back_ref, home_send, home_recv)
+        wide_ref[...] = back_ref[...].astype(jnp.float32)
+        narrow(ret_ref)
+        returned = ret_ref[...]
+        out_ref[...] = (
+            middle_ref[...]
+            + jnp.dot(mix_ref[0], returned, preferred_element_type=jnp.float32)
+            + jnp.dot(mix_ref[1], returned, preferred_element_type=jnp.float32)
+            + jnp.dot(mix_ref[2], returned, preferred_element_type=jnp.float32)
         ).astype(jnp.bfloat16)
+
+        def settle(turn, _):
+            swap(away_ref, got_ref, away_send, away_recv, turn).wait_send()
+            swap(home_ref, back_ref, home_send, home_recv, turn).wait_send()
+
+        lax.fori_loop(1, places, settle, None)
 
         for copy in (*forward_own(), share_own(), hand_over(0)):
             copy.wait_send()
@@ -506,11 +590,20 @@
     sems = [pltpu.SemaphoreType.DMA((chips + 1,)) for _ in range(12)]
     return pl.pallas_call(
         kernel,
-        out_shape=jax.ShapeDtypeStruct(block, jnp.bfloat16),
-        in_specs=[pl.BlockSpec(memory_space=pltpu.VMEM)] * 4,
+        out_shape=jax.ShapeDtypeStruct(middle.shape, jnp.bfloat16),
+        in_specs=[pl.BlockSpec(memory_space=pltpu.VMEM)] * 2
+        + [pl.BlockSpec(memory_space=pltpu.HBM)] * 3
+        + [pl.BlockSpec(memory_space=pltpu.VMEM)] * 2,
         out_specs=pl.BlockSpec(memory_space=pltpu.VMEM),
         scratch_shapes=[
+            pltpu.VMEM((count * chunks, 128), jnp.float32),
+            pltpu.SemaphoreType.DMA((3,)),
+            *[pltpu.VMEM((count * chunks, 128), jnp.bfloat16) for _ in range(4)],
+            pltpu.VMEM(block, jnp.bfloat16),
+            pltpu.VMEM(block, jnp.bfloat16),
+            *[pltpu.SemaphoreType.DMA((places,)) for _ in range(4)],
             pltpu.VMEM((width, 2 * hidden), jnp.bfloat16),
+            pltpu.VMEM((hidden, width), jnp.bfloat16),
             pltpu.VMEM((chips, both, width), jnp.bfloat16),
             pltpu.VMEM((chips, *block), jnp.bfloat16),
             pltpu.VMEM((chips, *block), jnp.bfloat16),
@@ -522,7 +615,7 @@
         compiler_params=pltpu.CompilerParams(
             collective_id=3, has_side_effects=True, vmem_limit_bytes=50 * 1024 * 1024
         ),
-    )(rows, gate, up, down)
+    )(chooser, ffn_input, gate, up, down, near_weights, middle)
 
 
 def shards(
@@ -547,7 +640,6 @@
     shard_len = queries.shape[0]
     local_heads = key_up.shape[1] // NOPE
     sp_count = lax.axis_size("sp")
-    tp_count = lax.axis_size("tp")
     my_first = lax.axis_index("sp") * shard_len
     positions = my_first + jnp.arange(shard_len, dtype=jnp.int32)
     inverse = rope_base ** (-jnp.arange(0, ROPE, 2, dtype=jnp.float32) / ROPE)
@@ -570,44 +662,26 @@
     )
     bundle = jnp.concatenate([key_rows.reshape(shard_len, QK).T, value_rows.T], axis=0)
     tok_count = residual.shape[0]
-    by_head = attention(query_rows.reshape(shard_len, QK), bundle)
+    by_head = attention(jnp.pad(query_rows.reshape(shard_len, QK), ((0, 0), (0, 128 - QK))), bundle)
     token_rows = jnp.transpose(by_head, (1, 0, 2)).reshape(tok_count, -1).astype(jnp.float32)
     normed_rows = (token_rows * rms_scale(token_rows) * out_gain).astype(jnp.bfloat16)
-    partials = jnp.einsum(
-        "tgc,gcd->tgd",
-        normed_rows.reshape(tok_count, tp_count, -1),
-        out_weight.reshape(tp_count, -1, D),
-        preferred_element_type=jnp.float32,
-    )
-    rounded = lax.optimization_barrier(partials.astype(jnp.bfloat16))
-    mixed = jnp.sum(rounded.astype(jnp.float32), axis=1)
+    mixed = jnp.dot(normed_rows, out_weight, preferred_element_type=jnp.float32)
     middle = residual.astype(jnp.float32) + mixed
     ffn_input = (middle * rms_scale(middle) * ffn_gain).astype(jnp.bfloat16)
     slot_cap = max(2, 9 * tok_count * TOPK // (8 * sp_count))
     slot_total = sp_count * slot_cap
     targets = slot_targets(routes, sp_count, slot_cap)
-    chooser = select_matrix(targets, slot_total)
-    outbound = (
-        jnp.einsum("ts,td->sd", chooser, ffn_input, preferred_element_type=jnp.float32)
-        .astype(jnp.bfloat16)
-        .reshape(sp_count, slot_cap, D)
+    slot_ids = jnp.arange(slot_total, dtype=jnp.int32)
+    hits = targets[:, :, None] == slot_ids[None, None, :]
+    chooser = jnp.any(slot_ids[:, None, None] == targets[None, :, :], axis=2).astype(jnp.bfloat16)
+    mix = jnp.sum(jnp.where(hits, route_weights[:, :, None], 0.0), axis=1)
+    mix_high = lax.reduce_precision(mix, 8, 7)
+    mix_mid = lax.reduce_precision(mix - mix_high, 8, 7)
+    mix_low = mix - mix_high - mix_mid
+    mix_parts = jnp.stack([mix_high, mix_mid, mix_low]).astype(jnp.bfloat16)
+    return expert_ring(
+        chooser, ffn_input, expert_gate[0], expert_up[0], expert_down[0], mix_parts, middle
     )
-    arrived = lax.all_to_all(outbound, "sp", split_axis=0, concat_axis=0, tiled=True)
-    item_count = arrived.shape[1]
-    flat_rows = arrived.reshape(sp_count * item_count, D)
-    served = expert_ring(flat_rows, expert_gate[0], expert_up[0], expert_down[0]).reshape(
-        sp_count, item_count, D
-    )
-    returned_rows = lax.all_to_all(served, "sp", split_axis=0, concat_axis=0, tiled=True).reshape(
-        slot_total, D
-    )
-    picked = (
-        jnp.take(returned_rows, targets.reshape(-1), axis=0)
-        .reshape(tok_count, TOPK, D)
-        .astype(jnp.float32)
-    )
-    moe_sum = jnp.sum(picked * route_weights[:, :, None], axis=1)
-    return (middle + moe_sum).astype(jnp.bfloat16)
 
 
 def solution(mesh):

time: 232 us -> 204 us (0.88)
  Pallas kernels: 165 us -> 191 us
  blocking collectives: 24.3 us -> 0 us
  waiting for transfers between devices: 15.4 us -> 0 us
  starting transfers between devices: 4.43 us -> 0 us
  other arithmetic: 7.09 us -> 3.32 us
  local copies, waits for them, and re-layouts: 5.88 us -> 2.43 us
    pallas_call x1, Pallas kernels: 99.5 us -> 125 us  [expert_ring(): pl.pallas_call(kernel, out_shape=jax.ShapeDtypeStruct(middle.shape, jnp.b...]
    all_to_all x1 -> x0, blocking collectives: 24.3 us -> none  [shards(): lax.all_to_all(outbound, 'sp', split_axis=0, concat_axis=0, tiled=True)]
    all_to_all x1 -> x0, waiting for transfers between devices: 15.4 us -> none  [shards(): lax.all_to_all(served, 'sp', split_axis=0, concat_axis=0, tiled=True)]
    all_to_all x1 -> x0, starting transfers between devices: 4.43 us -> none  [shards(): lax.all_to_all(served, 'sp', split_axis=0, concat_axis=0, tiled=True)]
    reshape x5 -> x0, local copies, waits for them, and re-layouts: 3.34 us -> none  [the longest x1 1.48 us: shards(): flat_rows = arrived.reshape(sp_count * item_count, D)]
    reduce_sum x3 -> x1, other arithmetic: 3.18 us -> 0.12 us  [shards(): mix = jnp.sum(jnp.where(hits, route_weights[:, :, None], 0.0), axis=1)]
  transfers between devices with their start and end apart: 1 -> 0, of which waited for: 1 -> 0; matrix products, arithmetic and copies ran while one was open for 0% -> 0% of each run, Pallas kernels for 0% -> 0%
where the time goes in v3:
time: 204 us; the launch traced here: 202 us
  Pallas kernels  191 us (94%)
  matrix products  5.54 us (3%)
  other arithmetic  3.32 us (2%)
  local copies, waits for them, and re-layouts  2.43 us (1%)
    pallas_call x1, Pallas kernels, expert_ring(): pl.pallas_call(kernel, out_shape=jax.ShapeDtypeStruct(middle.shape, jnp.b...  125 us
    pallas_call x1, Pallas kernels, attention(): pl.pallas_call(kernel, out_shape=jax.ShapeDtypeStruct((tp_count, tok, VH)...  65.6 us

profile of v3, /device:TPU:1, one launch (start us, length us, event | category | flops | bytes accessed | tf_op | source)
XLA Modules:
  0.0 202.2 jit_solution(5645268437679845197)
XLA Ops:
  0.0 0.0 copy-start
  0.0 0.0 copy-start.7
  0.0 0.0 copy-start.12
  0.0 0.0 copy-start.5
  0.0 0.0 copy-start.13
  0.0 1.6 fusion
  1.6 0.0 copy-done
  1.6 1.8 fusion.3
  3.4 0.0 copy-start.4
  3.4 0.0 copy-start.14
  3.4 0.0 copy-start.15
  3.4 0.0 copy-done.7
  3.4 0.1 fusion.9
  3.5 0.0 copy-done.12
  3.5 0.1 fusion.10
  3.6 0.0 copy-done.5
  3.6 0.1 fusion.6
  3.7 0.0 copy-done.13
  3.7 0.1 fusion.8
  3.8 0.3 fusion.37
  4.3 0.4 copy-done.4
  4.6 0.0 copy-done.14
  4.6 0.0 copy-done.15
  4.6 0.6 fusion.4
  5.2 0.2 copy.42
  5.4 0.0 copy-start.6
  5.4 0.0 copy-start.9
  5.4 0.1 pad.4.clone.q_ref
  5.5 65.6 %shard_map.163 = bf16[16,64,64]{2,1,0:T(8,128)(2,1)S(1)} custom-call(bf16[1024,128]{1,0:T(8,128)(2,1)S(1)} %pad.4.clone.q_ref, bf16[160,1024]{1,0:T(8,128)(2,1)S(1)} %pad_maximum_fusion.own_ref), custom_call_target="tpu_custom_call" | custom-call | tf_op jit(solution)/shard_map/pallas_call | solution.py:320
  71.1 0.3 copy.40
  71.4 0.2 reshape.355
  71.6 0.2 fusion.5
  71.8 0.0 copy-done.6
  71.8 0.0 copy-done.9
  71.8 0.0 copy-start.8
  71.8 0.0 copy-start.10
  71.8 0.0 copy-start.11
  71.9 3.2 %multiply_reduce_fusion = (f32[64]{0:T(128)S(1)}, f32[64,2048]{1,0:T(8,128)S(1)}) fusion(bf16[1024,2048]{1,0:T(8,128)(2,1)} %param.26, f32[64,1024]{1,0:T(8,128)S(1)} %reshape.355, f32[1024]{0:T(1024)S(1)} %copy-done.9, f32[64]{0:T(128)S(1)} %add_rsqrt_fusion.4, bf16[64,2048]{1,0:T(8,128)(2,1)S(1)} %copy-done.6), kind=kOutput, calls=%fused_computation.14 | convolution fusion | flops 269156288 | bytes 5247488 | tf_op jit(solution)/shard_map/dot_general | solution.py:668
  75.1 0.0 copy-start.1
  75.1 0.0 copy-start.2
  75.1 0.0 copy-start.3
  75.1 0.0 copy-done.8
  75.1 0.1 multiply_convert_fusion.token_ref
  75.3 0.0 copy-done.10
  75.3 0.1 copy.37
  75.4 0.1 eq.42
  75.5 0.1 fusion.35
  75.6 0.2 reduce_window_sum.11
  75.8 0.2 select_reduce_fusion.1
  75.9 0.1 reduce_sum.68
  76.1 0.1 copy.38
  76.2 0.0 copy-done.11
  76.2 0.1 select_reduce_fusion
  76.4 0.1 fusion.17
  76.5 0.1 copy.41.choose_ref
  76.6 0.0 copy-done.1
  76.6 0.0 copy-done.2
  76.6 0.0 copy-done.3
  76.6 124.9 %shard_map.164 = bf16[64,2048]{1,0:T(8,128)(2,1)S(1)} custom-call(bf16[144,64]{1,0:T(8,128)(2,1)S(1)} %copy.41.choose_ref, bf16[64,2048]{1,0:T(8,128)(2,1)S(1)} %multiply_convert_fusion.token_ref, bf16[2048,128]{1,0:T(8,128)(2,1)S(1)} %bitcast.36, bf16[2048,128]{1,0:T(8,128)(2,1)S(1)} %bitcast.37, bf16[128,2048]{1,0:T(8,128)(2,1)S(1)} %bitcast.38, ...), custom_call_target="tpu_custom_call" | custom-call | tf_op jit(solution)/shard_map/pallas_call | solution.py:591
  201.5 0.7 copy.44
  (16 shorter events, 0.2 us)
Async XLA Ops:
  0.0 1.6 copy-start
  0.0 3.4 %copy-start.7 = (bf16[1024,32]{0,1:T(8,128)(2,1)S(1)}, bf16[1024,32]{0,1:T(8,128)(2,1)}, u32[]{:S(2)}) copy-start(bf16[1024,32]{0,1:T(8,128)(2,1)} %param.19) | copy-start | bytes 196612
  0.0 3.5 %copy-start.12 = (f32[96]{0:T(128)S(1)}, f32[96]{0:T(128)}, u32[]{:S(2)}) copy-start(f32[96]{0:T(128)} %param.24) | copy-start | bytes 1156
  0.0 3.6 %copy-start.5 = (bf16[1024,96]{0,1:T(8,128)(2,1)S(1)}, bf16[1024,96]{0,1:T(8,128)(2,1)}, u32[]{:S(2)}) copy-start(bf16[1024,96]{0,1:T(8,128)(2,1)} %param.17) | copy-start | bytes 589828
  0.0 3.7 %copy-start.13 = (f32[96]{0:T(128)S(1)}, f32[96]{0:T(128)}, u32[]{:S(2)}) copy-start(f32[96]{0:T(128)} %param.23) | copy-start | bytes 1156
  3.4 1.2 copy-start.4
  3.4 1.2 copy-start.14
  3.4 1.2 copy-start.15
  5.4 66.4 %copy-start.6 = (bf16[64,2048]{1,0:T(8,128)(2,1)S(1)}, bf16[64,2048]{1,0:T(8,128)(2,1)}, u32[]{:S(2)}) copy-start(bf16[64,2048]{1,0:T(8,128)(2,1)} %param.27) | copy-start | bytes 786436
  5.4 66.4 %copy-start.9 = (f32[1024]{0:T(1024)S(1)}, f32[1024]{0:T(1024)}, u32[]{:S(2)}) copy-start(f32[1024]{0:T(1024)} %param.25) | copy-start | bytes 12292
  71.8 3.3 %copy-start.8 = (f32[2048]{0:T(1024)S(1)}, f32[2048]{0:T(1024)}, u32[]{:S(2)}) copy-start(f32[2048]{0:T(1024)} %param.28) | copy-start | bytes 24580
  71.8 3.4 %copy-start.10 = (s32[64,2]{0,1:T(2,128)S(1)}, s32[64,2]{0,1:T(2,128)}, u32[]{:S(2)}) copy-start(s32[64,2]{0,1:T(2,128)} %param.29) | copy-start | bytes 1540
  71.8 4.3 %copy-start.11 = (f32[64,2]{0,1:T(2,128)S(1)}, f32[64,2]{0,1:T(2,128)}, u32[]{:S(2)}) copy-start(f32[64,2]{0,1:T(2,128)} %param.30) | copy-start | bytes 1540
  75.1 1.5 copy-start.1
  75.1 1.5 copy-start.2
  75.1 1.5 copy-start.3

commit v4 on v3

--- a/solution.py
+++ b/solution.py
@@ -61,27 +61,37 @@
 )
 
 
-def attention(query_rows, bundle):
+def attention(query_rows, bundle, down):
     shard_len = query_rows.shape[0]
     half = shard_len // 2
     block_count = lax.axis_size("sp")
     tp_count = lax.axis_size("tp")
     tok = shard_len // tp_count
+    chips = tp_count // 2
+    pack = tok // 2
+    groups = tp_count // 4
+    hidden, width = down.shape
+    share_rows = hidden // 2
     bundle_rows = bundle.shape[0]
     part_rows = bundle_rows // 2
 
     def kernel(
-        q_ref, own_ref, out_ref,
+        q_ref, own_ref, down_ref, out_ref, all_ref,
         kv_ref, pair_ref, peak_ref, acc_ref, val_ref, done_ref, tok_ref,
         kv_send, kv_recv, q_send, q_recv, out_send, out_recv,
+        w_send, w_recv, twin_send, twin_recv,
     ):
         mine = lax.axis_index("sp")
         head = lax.axis_index("tp")
         mirror = block_count - 1 - mine
         low = jnp.minimum(mine, mirror)
         high = jnp.maximum(mine, mirror)
-        shift = pl.multiple_of(jnp.where(mine < block_count // 2, 0, half), half)
-        rest = pl.multiple_of(half - shift, half)
+        early = mine < block_count // 2
+        shift = pl.multiple_of(jnp.where(early, 0, 2 * tok), 2 * tok)
+        own_slot = pl.multiple_of(jnp.where(early, 0, half), half)
+        far_slot = pl.multiple_of(half - own_slot, half)
+        chip, core = head // 2, head % 2
+        twin = chip * 2 + 1 - core
         row, col = mine // SIDE, mine % SIDE
 
         def block_at(dx, dy):
@@ -118,13 +128,45 @@
                 device_id_type=pl.DeviceIdType.MESH,
             )
 
-        def trade():
-            return remote(q_ref.at[pl.ds(rest, half)], pair_ref.at[pl.ds(shift, half)],
-                          q_send.at[0], q_recv.at[0], mirror, head)
-
-        def traded():
-            return remote(q_ref.at[pl.ds(rest, half)], pair_ref.at[pl.ds(rest, half)],
-                          q_send.at[0], q_recv.at[0], mirror, head)
+        def queries_of(group, offset):
+            return q_ref.at[pl.ds(pl.multiple_of(group * 4 * tok + offset, 2 * tok), 2 * tok)]
+
+        def trade(group, slot):
+            target = pair_ref.at[pl.ds(pl.multiple_of(slot + group * 2 * tok, 2 * tok), 2 * tok)]
+            return remote(queries_of(group, 2 * tok - shift), target,
+                          q_send.at[group], q_recv.at[group], mirror, head)
+
+        def lane_of(way, distance):
+            return ((chip + (chips - distance if way == 0 else distance)) % chips) * 2 + core
+
+        def wanted(way, distance, part):
+            far = chips // 2
+            return distance < far or (distance == far and part == way)
+
+        def weight(way, distance, part):
+            lane = lane_of(way, distance - 1)
+            rows = pl.ds(part * share_rows, share_rows)
+            source = down_ref.at[rows] if distance == 1 else all_ref.at[lane, rows]
+            index = (way * chips + distance) * 2 + part
+            return remote(source, all_ref.at[lane, rows], w_send.at[index], w_recv.at[index],
+                          mine, ((chip + (1 if way == 0 else chips - 1)) % chips) * 2 + core)
+
+        def share(way, distance, part):
+            lane = lane_of(way, distance)
+            rows = pl.ds(part * share_rows, share_rows)
+            source = down_ref.at[rows] if distance == 0 else all_ref.at[lane, rows]
+            index = (way * chips + distance) * 2 + part
+            return remote(source, all_ref.at[lane, rows],
+                          twin_send.at[index], twin_recv.at[index], mine, twin)
+
+        def weights_arrive(distance, parts):
+            for part in parts:
+                for way in (0, 1):
+                    if wanted(way, distance, part):
+                        weight(way, distance, part).wait_recv()
+                        if wanted(way, distance + 1, part):
+                            weight(way, distance + 1, part).start()
+                        share(way, distance, part).start()
 
         def at(part, along, across):
             return (along, across) if part == 0 else (across, along)
@@ -180,7 +222,12 @@
                     landed(part, at(part, along, 2), 0)
                     landed(part, at(part, along, 2), 1)
 
-        trade().start()
+        for group in range(groups):
+            trade(group, own_slot).start()
+        for part in (0, 1):
+            for way in (0, 1):
+                weight(way, 1, part).start()
+            share(0, 0, part).start()
         for part in (0, 1):
             push(part, (0, 0), at(part, 1, 0), own=True)
             push(part, (0, 0), at(part, 3, 0), own=True)
@@ -188,7 +235,9 @@
             push(part, (0, 0), at(part, 0, 1), own=True)
             push(part, (0, 0), at(part, 0, 3), own=True)
         kv_ref[mine] = own_ref[...]
-        pair_ref[pl.ds(shift, half), :] = q_ref[pl.ds(shift, half), :]
+        for group in range(groups):
+            target = pl.ds(pl.multiple_of(own_slot + group * 2 * tok, 2 * tok), 2 * tok)
+            pair_ref[target, :] = queries_of(group, shift)[...]
         peak_ref[...] = jnp.full_like(peak_ref, -1e30)
         acc_ref[...] = jnp.zeros_like(acc_ref)
         lane = lax.broadcasted_iota(jnp.int32, (shard_len, 128), 1)
@@ -207,9 +256,9 @@
                     if masked:
                         q_pos = lax.broadcasted_iota(jnp.int32, scores.shape, 0)
                         k_pos = lax.broadcasted_iota(jnp.int32, scores.shape, 1)
-                        scores = jnp.where(
-                            k_pos - q_pos <= shift + (first - start), scores, -1e30
-                        )
+                        q_pos = q_pos + (first - start)
+                        q_pos = q_pos + (q_pos // (2 * tok)) * (2 * tok)
+                        scores = jnp.where(k_pos - q_pos <= shift, scores, -1e30)
                     old = peak_ref[rows, :]
                     new = jnp.maximum(old, jnp.max(scores, axis=1, keepdims=True))
                     weights = jnp.exp2((scores - new[:, :1]) * SCORE_EXP).astype(jnp.bfloat16)
@@ -223,11 +272,33 @@
             @pl.when(step == 0)
             def _():
                 neighbours_first()
-                traded().wait_recv()
+                for group in range(groups):
+                    trade(group, far_slot).wait_recv()
 
             @pl.when(step == 1)
             def _():
                 pass_across((0,))
+                weights_arrive(1, (0,))
+
+            @pl.when(step == 3)
+            def _():
+                weights_arrive(1, (1,))
+
+            @pl.when(step == 6)
+            def _():
+                weights_arrive(2, (0,))
+
+            @pl.when(step == 8)
+            def _():
+                weights_arrive(2, (1,))
+
+            @pl.when(step == 10)
+            def _():
+                weights_arrive(3, (0,))
+
+            @pl.when(step == 13)
+            def _():
+                weights_arrive(3, (1,))
 
             @pl.when(step == 2)
             def _():
@@ -271,20 +342,30 @@
                 attend(block, ((half, True),))
 
         lax.fori_loop(0, block_count, visit, None)
-        done_ref[...] = (acc_ref[...] / acc_ref[:, VH : VH + 1]).astype(jnp.bfloat16)
-
-        first_lane = shift // tok
+        shares = (acc_ref[...] / acc_ref[:, VH : VH + 1]).reshape(tp_count, 2, pack, 128)
+        lanes = lax.broadcasted_iota(jnp.int32, (tp_count, pack, 128), 2)
+        done_ref[...] = (
+            jnp.where(lanes < VH, shares[:, 0], pltpu.roll(shares[:, 1], VH, 2))
+            .reshape(tp_count * pack, 128)
+            .astype(jnp.bfloat16)
+        )
+
+        per_slot = tp_count // 2
+
+        def piece_of(slot, order):
+            return pl.ds(pl.multiple_of((slot // tok + order) * pack, pack), pack)
 
         def result(index):
-            side, order = index // (tp_count // 2), index % (tp_count // 2)
-            own_side = jnp.where(side == 0, shift, rest)
-            start = pl.multiple_of(own_side + order * tok, tok)
-            return remote(done_ref.at[pl.ds(start, tok)], tok_ref.at[head],
+            side, order = index // per_slot, index % per_slot
+            slot = jnp.where(side == 0, own_slot, far_slot)
+            return remote(done_ref.at[piece_of(slot, order)], tok_ref.at[head],
                           out_send.at[index], out_recv.at[head],
-                          jnp.where(side == 0, mine, mirror), first_lane + order)
-
-        here = (head >= first_lane) & (head < first_lane + tp_count // 2)
-        self_index = jnp.where(here, head - first_lane, tp_count)
+                          jnp.where(side == 0, mine, mirror),
+                          (order // 2) * 4 + shift // tok + order % 2)
+
+        here = (chip % 2) * 2 * tok == shift
+        self_order = (head // 4) * 2 + core
+        self_index = jnp.where(here, self_order, tp_count)
 
         def send_result(index, _):
             @pl.when(index != self_index)
@@ -295,18 +376,28 @@
 
         @pl.when(here)
         def _():
-            tok_ref[head] = done_ref[pl.ds(pl.multiple_of(head * tok, tok), tok), :]
+            tok_ref[head] = done_ref[piece_of(own_slot, self_order), :]
 
         def take_result(index, _):
             @pl.when(jnp.logical_not(here & (index == head)))
             def _():
-                remote(done_ref.at[pl.ds(0, tok)], tok_ref.at[index],
+                remote(done_ref.at[pl.ds(0, pack)], tok_ref.at[index],
                        out_send.at[index], out_recv.at[index], mirror, head).wait_recv()
 
         lax.fori_loop(0, tp_count, take_result, None)
-        out_ref[...] = tok_ref[:, :, :VH]
-
-        trade().wait_send()
+        out_ref[...] = tok_ref[...]
+
+        far = chips // 2
+        weights_arrive(far, (0, 1))
+        for part in (0, 1):
+            share(0, 0, part).wait()
+            for distance in range(1, far + 1):
+                for way in (0, 1):
+                    if wanted(way, distance, part):
+                        weight(way, distance, part).wait_send()
+                        share(way, distance, part).wait()
+        for group in range(groups):
+            trade(group, own_slot).wait_send()
         for message in sent:
             piece(*message).wait_send()
 
@@ -319,34 +410,42 @@
 
     return pl.pallas_call(
         kernel,
-        out_shape=jax.ShapeDtypeStruct((tp_count, tok, VH), jnp.bfloat16),
-        in_specs=[pl.BlockSpec(memory_space=pltpu.VMEM)] * 2,
-        out_specs=pl.BlockSpec(memory_space=pltpu.VMEM),
+        out_shape=(
+            jax.ShapeDtypeStruct((tp_count, pack, 128), jnp.bfloat16),
+            jax.ShapeDtypeStruct((tp_count, hidden, width), jnp.bfloat16),
+        ),
+        in_specs=[pl.BlockSpec(memory_space=pltpu.VMEM)] * 2
+        + [pl.BlockSpec(memory_space=pltpu.HBM)],
+        out_specs=(
+            pl.BlockSpec(memory_space=pltpu.VMEM),
+            pl.BlockSpec(memory_space=pltpu.HBM),
+        ),
         scratch_shapes=[
             pltpu.VMEM((block_count, bundle_rows, shard_len), jnp.bfloat16),
             pltpu.VMEM((shard_len, 128), jnp.bfloat16),
             pltpu.VMEM((shard_len, 128), jnp.float32),
             pltpu.VMEM((shard_len, 128), jnp.float32),
             pltpu.VMEM((shard_len, 128), jnp.bfloat16),
-            pltpu.VMEM((shard_len, 128), jnp.bfloat16),
-            pltpu.VMEM((tp_count, tok, 128), jnp.bfloat16),
+            pltpu.VMEM((tp_count * pack, 128), jnp.bfloat16),
+            pltpu.VMEM((tp_count, pack, 128), jnp.bfloat16),
             pltpu.SemaphoreType.DMA((block_count * 8,)),
             pltpu.SemaphoreType.DMA((block_count * 4,)),
-            pltpu.SemaphoreType.DMA((1,)),
-            pltpu.SemaphoreType.DMA((1,)),
+            pltpu.SemaphoreType.DMA((groups,)),
+            pltpu.SemaphoreType.DMA((groups,)),
             pltpu.SemaphoreType.DMA((tp_count,)),
             pltpu.SemaphoreType.DMA((tp_count,)),
+            *[pltpu.SemaphoreType.DMA((4 * chips,)) for _ in range(4)],
         ],
         compiler_params=pltpu.CompilerParams(
             collective_id=4, has_side_effects=True, vmem_limit_bytes=40 * 1024 * 1024
         ),
-    )(query_rows, bundle)
+    )(query_rows, bundle, down)
 
 
 ROW_CUT = 80
 
 
-def expert_ring(chooser, ffn_input, gate, up, down, near_weights, middle):
+def expert_ring(chooser, ffn_input, gate, up, down, all_down, near_weights, middle):
     count = chooser.shape[0]
     width = ffn_input.shape[1]
     places = lax.axis_size("sp")
@@ -358,12 +457,11 @@
     both = 2 * count
 
     def kernel(
-        choose_ref, token_ref, gate_ref, up_ref, down_hbm, mix_ref, middle_ref, out_ref,
+        choose_ref, token_ref, gate_ref, up_ref, down_hbm, all_hbm, mix_ref, middle_ref, out_ref,
         wide_ref, load_sem, away_ref, got_ref, home_ref, back_ref, ret_ref, x_ref,
         away_send, away_recv, home_send, home_recv,
-        both_ref, down_ref, seen, own_part, far_part, near_part, run_in, run_out,
-        fwd_send, fwd_recv, back_send, back_recv, twin_send, twin_recv,
-        part_send, part_recv, sum_fwd_send, sum_fwd_recv, sum_back_send, sum_back_recv,
+        both_ref, down_ref, down_sem, seen, inner_ref, hid_ref, served_ref,
+        fwd_send, fwd_recv, back_send, back_recv, twin_send, twin_recv, hid_send, hid_recv,
     ):
         place = lax.axis_index("tp")
         chip, core = place // 2, place % 2
@@ -391,10 +489,29 @@
         loads = (
             pltpu.make_async_copy(gate_ref, both_ref.at[:, pl.ds(0, hidden)], load_sem.at[0]),
             pltpu.make_async_copy(up_ref, both_ref.at[:, pl.ds(hidden, hidden)], load_sem.at[1]),
-            pltpu.make_async_copy(down_hbm, down_ref, load_sem.at[2]),
         )
         for load in loads:
             load.start()
+
+        def lane_rows(lane):
+            return pl.ds(pl.multiple_of(lane * hidden, hidden), hidden)
+
+        def load_down(lane):
+            return pltpu.make_async_copy(
+                all_hbm.at[lane], down_ref.at[lane_rows(lane)], down_sem.at[lane]
+            )
+
+        own_down = pltpu.make_async_copy(
+            down_hbm, down_ref.at[lane_rows(place)], down_sem.at[place]
+        )
+        own_down.start()
+
+        def fetch(lane, _):
+            @pl.when(lane != place)
+            def _():
+                load_down(lane).start()
+
+        lax.fori_loop(0, 2 * chips, fetch, None)
         chosen = jnp.dot(choose_ref[...], token_ref[...], preferred_element_type=jnp.float32)
         for chunk in range(chunks):
             wide_ref[pl.ds(chunk, count, stride=chunks), :] = chosen[
@@ -473,27 +590,37 @@
         def share_own():
             return remote(x_ref, seen.at[0, rear], twin_send.at[0], twin_recv.at[0], twin)
 
-        def hand_over(step):
-            return remote(far_part.at[step], near_part.at[step],
-                          part_send.at[step], part_recv.at[step], twin)
-
-        def pass_sum(step):
-            return (
-                remote(run_out.at[step, first], run_in.at[step + 1, first],
-                       sum_fwd_send.at[step], sum_fwd_recv.at[step + 1], ahead),
-                remote(run_out.at[step, second], run_in.at[step + 1, second],
-                       sum_back_send.at[step], sum_back_recv.at[step + 1], behind),
-            )
+        def chip_at(distance):
+            return (chip + chips + distance) % chips
+
+        def tell(step):
+            away, near = toward * step, (chips - toward) * step
+            parts = (
+                (first, 0, chip_at(near) * 2 + core, 0),
+                (second, ROW_CUT, chip_at(away) * 2 + core, 1),
+                (first, count, chip_at(away) * 2 + 1 - core, 0),
+                (second, count + ROW_CUT, chip_at(near) * 2 + 1 - core, 1),
+            )
+            columns = pl.ds(pl.multiple_of(place * hidden, hidden), hidden)
+            return [
+                remote(inner_ref.at[step, pl.ds(start, rows.size)], hid_ref.at[rows, columns],
+                       hid_send.at[step * 4 + order], hid_recv.at[place * 2 + half], owner)
+                for order, (rows, start, owner, half) in enumerate(parts)
+            ]
+
+        def hear(lane):
+            columns = pl.ds(pl.multiple_of(lane * hidden, hidden), hidden)
+            return [
+                remote(inner_ref.at[0, pl.ds(0, rows.size)], hid_ref.at[rows, columns],
+                       hid_send.at[half], hid_recv.at[lane * 2 + half], twin)
+                for half, rows in enumerate((first, second))
+            ]
 
         def experts(step):
-            tokens = seen[step]
-            pre = jnp.dot(tokens, both_ref[...], preferred_element_type=jnp.float32)
-            inner = (jax.nn.silu(pre[:, :hidden]) * pre[:, hidden:]).astype(jnp.bfloat16)
-            part = jnp.dot(inner, down_ref[...], preferred_element_type=jnp.float32).astype(
+            pre = jnp.dot(seen[step], both_ref[...], preferred_element_type=jnp.float32)
+            inner_ref[step] = (jax.nn.silu(pre[:, :hidden]) * pre[:, hidden:]).astype(
                 jnp.bfloat16
             )
-            own_part[step] = part[:count]
-            far_part[step] = part[count:]
 
         for copy in (*forward_own(), share_own()):
             copy.start()
@@ -502,12 +629,13 @@
         seen[0, front, :] = x_ref[...]
         share_own().wait_recv()
         experts(0)
-        hand_over(0).start()
+        hid_ref[:, pl.ds(pl.multiple_of(place * hidden, hidden), hidden)] = inner_ref[0, front, :]
+        for copy in tell(0)[2:]:
+            copy.start()
 
         def step_of(step, _):
-            arrived = forward(step - 1)
-            arrived[0].wait_recv()
-            arrived[1].wait_recv()
+            for copy in forward(step - 1):
+                copy.wait_recv()
 
             @pl.when(step < chips - 1)
             def _():
@@ -517,39 +645,30 @@
             share(step).start()
             share(step).wait_recv()
             experts(step)
-            hand_over(step).start()
-            hand_over(step).wait_recv()
-
-            @pl.when(step > 1)
-            def _():
-                for copy in pass_sum(step - 1):
+            for copy in tell(step):
+                copy.start()
+
+        lax.fori_loop(1, chips, step_of, None)
+
+        def gathered(lane, _):
+            @pl.when(lane != place)
+            def _():
+                load_down(lane).wait()
+                for copy in hear(lane):
                     copy.wait_recv()
-                run_out[step] = (
-                    run_in[step].astype(jnp.float32)
-                    + own_part[step].astype(jnp.float32)
-                    + near_part[step].astype(jnp.float32)
-                ).astype(jnp.bfloat16)
-
-            @pl.when(step == 1)
-            def _():
-                run_out[step] = (
-                    own_part[step].astype(jnp.float32) + near_part[step].astype(jnp.float32)
-                ).astype(jnp.bfloat16)
-
-            for copy in pass_sum(step):
-                copy.start()
-
-        lax.fori_loop(1, chips, step_of, None)
-        hand_over(0).wait_recv()
-        for copy in pass_sum(chips - 1):
-            copy.wait_recv()
-        served = (
-            run_in[chips].astype(jnp.float32)
-            + own_part[0].astype(jnp.float32)
-            + near_part[0].astype(jnp.float32)
-        )
+
+        lax.fori_loop(0, 2 * chips, gathered, None)
+        own_down.wait()
+
+        def project(index, _):
+            columns = pl.ds(pl.multiple_of(index * 512, 512), 512)
+            served_ref[:, columns] = jnp.dot(
+                hid_ref[...], down_ref[:, columns], preferred_element_type=jnp.float32
+            )
+
+        lax.fori_loop(0, width // 512, project, None)
         for chunk in range(chunks):
-            wide_ref[pl.ds(chunk, count, stride=chunks), :] = served[
+            wide_ref[pl.ds(chunk, count, stride=chunks), :] = served_ref[
                 :, chunk * 128 : (chunk + 1) * 128
             ]
         home_ref[...] = wide_ref[...].astype(jnp.bfloat16)
@@ -570,7 +689,7 @@
 
         lax.fori_loop(1, places, settle, None)
 
-        for copy in (*forward_own(), share_own(), hand_over(0)):
+        for copy in (*forward_own(), share_own(), *tell(0)[2:]):
             copy.wait_send()
 
         def drain(step, _):
@@ -580,42 +699,41 @@
                     copy.wait_send()
 
             share(step).wait_send()
-            hand_over(step).wait_send()
-            for copy in pass_sum(step):
+            for copy in tell(step):
                 copy.wait_send()
 
         lax.fori_loop(1, chips, drain, None)
 
     block = (count, width)
-    sems = [pltpu.SemaphoreType.DMA((chips + 1,)) for _ in range(12)]
+    sems = [pltpu.SemaphoreType.DMA((chips + 1,)) for _ in range(6)]
+    sems += [pltpu.SemaphoreType.DMA((4 * chips,)) for _ in range(2)]
     return pl.pallas_call(
         kernel,
         out_shape=jax.ShapeDtypeStruct(middle.shape, jnp.bfloat16),
         in_specs=[pl.BlockSpec(memory_space=pltpu.VMEM)] * 2
-        + [pl.BlockSpec(memory_space=pltpu.HBM)] * 3
+        + [pl.BlockSpec(memory_space=pltpu.HBM)] * 4
         + [pl.BlockSpec(memory_space=pltpu.VMEM)] * 2,
         out_specs=pl.BlockSpec(memory_space=pltpu.VMEM),
         scratch_shapes=[
             pltpu.VMEM((count * chunks, 128), jnp.float32),
-            pltpu.SemaphoreType.DMA((3,)),
+            pltpu.SemaphoreType.DMA((2,)),
             *[pltpu.VMEM((count * chunks, 128), jnp.bfloat16) for _ in range(4)],
             pltpu.VMEM(block, jnp.bfloat16),
             pltpu.VMEM(block, jnp.bfloat16),
             *[pltpu.SemaphoreType.DMA((places,)) for _ in range(4)],
             pltpu.VMEM((width, 2 * hidden), jnp.bfloat16),
-            pltpu.VMEM((hidden, width), jnp.bfloat16),
+            pltpu.VMEM((2 * chips * hidden, width), jnp.bfloat16),
+            pltpu.SemaphoreType.DMA((2 * chips,)),
             pltpu.VMEM((chips, both, width), jnp.bfloat16),
-            pltpu.VMEM((chips, *block), jnp.bfloat16),
-            pltpu.VMEM((chips, *block), jnp.bfloat16),
-            pltpu.VMEM((chips, *block), jnp.bfloat16),
-            pltpu.VMEM((chips + 1, *block), jnp.bfloat16),
-            pltpu.VMEM((chips, *block), jnp.bfloat16),
+            pltpu.VMEM((chips, both, hidden), jnp.bfloat16),
+            pltpu.VMEM((count, 2 * chips * hidden), jnp.bfloat16),
+            pltpu.VMEM(block, jnp.float32),
             *sems,
         ],
         compiler_params=pltpu.CompilerParams(
             collective_id=3, has_side_effects=True, vmem_limit_bytes=50 * 1024 * 1024
         ),
-    )(chooser, ffn_input, gate, up, down, near_weights, middle)
+    )(chooser, ffn_input, gate, up, down, all_down, near_weights, middle)
 
 
 def shards(
@@ -662,8 +780,14 @@
     )
     bundle = jnp.concatenate([key_rows.reshape(shard_len, QK).T, value_rows.T], axis=0)
     tok_count = residual.shape[0]
-    by_head = attention(jnp.pad(query_rows.reshape(shard_len, QK), ((0, 0), (0, 128 - QK))), bundle)
-    token_rows = jnp.transpose(by_head, (1, 0, 2)).reshape(tok_count, -1).astype(jnp.float32)
+    by_head, all_down = attention(
+        jnp.pad(query_rows.reshape(shard_len, QK), ((0, 0), (0, 128 - QK))), bundle, expert_down[0]
+    )
+    token_rows = (
+        jnp.transpose(by_head.reshape(*by_head.shape[:2], 2, VH), (2, 1, 0, 3))
+        .reshape(tok_count, -1)
+        .astype(jnp.float32)
+    )
     normed_rows = (token_rows * rms_scale(token_rows) * out_gain).astype(jnp.bfloat16)
     mixed = jnp.dot(normed_rows, out_weight, preferred_element_type=jnp.float32)
     middle = residual.astype(jnp.float32) + mixed
@@ -680,7 +804,8 @@
     mix_low = mix - mix_high - mix_mid
     mix_parts = jnp.stack([mix_high, mix_mid, mix_low]).astype(jnp.bfloat16)
     return expert_ring(
-        chooser, ffn_input, expert_gate[0], expert_up[0], expert_down[0], mix_parts, middle
+        chooser, ffn_input, expert_gate[0], expert_up[0], expert_down[0], all_down, mix_parts,
+        middle,
     )
 
 

time: 204 us -> 186 us (0.912)
  Pallas kernels: 191 us -> 169 us
  local copies, waits for them, and re-layouts: 2.43 us -> 6.19 us
    pallas_call x1, Pallas kernels: 125 us -> 100 us  [expert_ring(): pl.pallas_call(kernel, out_shape=jax.ShapeDtypeStruct(middle.shape, jnp.b...]
    pallas_call x1, Pallas kernels: 65.6 us -> 69 us  [attention(): pl.pallas_call(kernel, out_shape=(jax.ShapeDtypeStruct((tp_count, pack, 1...]
    unnamed x35 -> x38, local copies, waits for them, and re-layouts: 1.41 us -> 4.68 us
where the time goes in v4:
time: 186 us; the launch traced here: 185 us
  Pallas kernels  169 us (91%)
  local copies, waits for them, and re-layouts  6.19 us (3%)
  matrix products  5.56 us (3%)
  other arithmetic  3.24 us (2%)
    pallas_call x1, Pallas kernels, expert_ring(): pl.pallas_call(kernel, out_shape=jax.ShapeDtypeStruct(middle.shape, jnp.b...  100 us
    pallas_call x1, Pallas kernels, attention(): pl.pallas_call(kernel, out_shape=(jax.ShapeDtypeStruct((tp_count, pack, 1...  69 us
    unnamed x38, local copies, waits for them, and re-layouts  4.68 us

profile of v4, /device:TPU:1, one launch (start us, length us, event | category | flops | bytes accessed | tf_op | source)
XLA Modules:
  0.0 184.7 jit_solution(4049194745485630528)
XLA Ops:
  0.0 0.0 copy-start
  0.0 0.0 copy-start.8
  0.0 0.0 copy-start.6
  0.0 0.0 copy-start.14
  0.0 1.6 fusion
  1.6 0.0 copy-done
  1.6 1.8 fusion.3
  3.4 0.0 copy-start.5
  3.4 0.0 copy-start.15
  3.4 0.0 copy-start.16
  3.4 0.0 copy-done.8
  3.4 0.1 fusion.8
  3.5 0.0 copy-done.13
  3.5 0.1 fusion.9
  3.6 0.0 copy-done.6
  3.6 0.1 fusion.5
  3.7 0.0 copy-done.14
  3.7 0.1 fusion.7
  3.8 0.3 fusion.36
  4.2 0.0 copy-start.2
  4.3 0.3 copy-done.5
  4.6 0.0 copy-done.15
  4.6 0.0 copy-done.16
  4.6 0.6 fusion.4
  5.2 0.2 copy.53
  5.4 0.0 copy-start.7
  5.4 0.0 copy-start.10
  5.4 0.1 pad.4.clone.q_ref
  5.5 0.0 copy-done.2
  5.5 69.0 %shard_map.163 = (bf16[16,32,128]{2,1,0:T(8,128)(2,1)S(1)}, bf16[16,128,2048]{2,1,0:T(8,128)(2,1)S(1)}) custom-call(bf16[1024,128]{1,0:T(8,128)(2,1)S(1)} %pad.4.clone.q_ref, bf16[160,1024]{1,0:T(8,128)(2,1)S(1)} %pad_maximum_fusion.own_ref, bf16[128,2048]{1,0:T(8,128)(2,1)S(1)} %bitcast.40), custom_call_target="tpu_custom_call" | custom-call | tf_op jit(solution)/shard_map/pallas_call | solution.py:411
  74.5 0.0 copy-start.1
  74.5 3.2 %copy-done.1 = bf16[16,128,2048]{2,1,0:T(8,128)(2,1)} copy-done((bf16[16,128,2048]{2,1,0:T(8,128)(2,1)}, bf16[16,128,2048]{2,1,0:T(8,128)(2,1)S(1)}, u32[]{:S(2)}) %copy-start.1) | copy-done | bytes 8388632
  77.7 0.3 reshape.371
  78.0 0.3 copy.56
  78.3 0.2 reshape.370
  78.6 0.1 reduce_sum.80
  78.6 0.1 reduce_sum.81
  78.8 0.1 copy.54
  78.9 0.1 rsqrt.47
  78.9 0.0 copy-done.7
  78.9 0.0 copy-done.10
  78.9 0.0 copy-start.11
  79.0 0.0 copy-start.12
  79.0 3.2 %multiply_reduce_fusion = (f32[64]{0:T(128)S(1)}, f32[64,2048]{1,0:T(8,128)S(1)}) fusion(bf16[1024,2048]{1,0:T(8,128)(2,1)} %param.26, f32[64,1024]{1,0:T(8,128)S(1)} %reshape.370, f32[1024]{0:T(1024)S(1)} %copy-done.10, f32[64]{0:T(128)S(1)} %rsqrt.47, bf16[64,2048]{1,0:T(8,128)(2,1)S(1)} %copy-done.7), kind=kOutput, calls=%fused_computation.12 | convolution fusion | flops 269156288 | bytes 5247488 | tf_op jit(solution)/shard_map/dot_general | solution.py:792
  82.2 0.0 copy-start.3
  82.2 0.0 copy-start.4
  82.2 0.0 copy-done.9
  82.2 0.1 multiply_convert_fusion.token_ref
  82.4 0.0 copy-done.11
  82.4 0.1 copy.46
  82.5 0.1 eq.42
  82.6 0.1 fusion.34
  82.7 0.2 reduce_window_sum.11
  82.9 0.2 select_reduce_fusion.1
  83.1 0.1 reduce_sum.75
  83.2 0.1 copy.47
  83.3 0.0 copy-done.12
  83.3 0.1 select_reduce_fusion
  83.5 0.1 fusion.16
  83.6 0.1 copy.51.choose_ref
  83.7 0.0 copy-done.3
  83.7 0.0 copy-done.4
  83.7 100.3 %shard_map.164 = bf16[64,2048]{1,0:T(8,128)(2,1)S(1)} custom-call(bf16[144,64]{1,0:T(8,128)(2,1)S(1)} %copy.51.choose_ref, bf16[64,2048]{1,0:T(8,128)(2,1)S(1)} %multiply_convert_fusion.token_ref, bf16[2048,128]{1,0:T(8,128)(2,1)S(1)} %bitcast.42, bf16[2048,128]{1,0:T(8,128)(2,1)S(1)} %bitcast.43, bf16[128,2048]{1,0:T(8,128)(2,1)S(1)} %bitcast.41, ...), custom_call_target="tpu_custom_call" | custom-call | tf_op jit(solution)/shard_map/pallas_call | solution.py:710
  184.0 0.7 copy.58
  (18 shorter events, 0.2 us)
Async XLA Ops:
  0.0 1.6 copy-start
  0.0 3.4 %copy-start.8 = (bf16[1024,32]{0,1:T(8,128)(2,1)S(1)}, bf16[1024,32]{0,1:T(8,128)(2,1)}, u32[]{:S(2)}) copy-start(bf16[1024,32]{0,1:T(8,128)(2,1)} %param.19) | copy-start | bytes 196612
  0.0 3.5 %copy-start.13 = (f32[96]{0:T(128)S(1)}, f32[96]{0:T(128)}, u32[]{:S(2)}) copy-start(f32[96]{0:T(128)} %param.24) | copy-start | bytes 1156
  0.0 3.6 %copy-start.6 = (bf16[1024,96]{0,1:T(8,128)(2,1)S(1)}, bf16[1024,96]{0,1:T(8,128)(2,1)}, u32[]{:S(2)}) copy-start(bf16[1024,96]{0,1:T(8,128)(2,1)} %param.17) | copy-start | bytes 589828
  0.0 3.7 %copy-start.14 = (f32[96]{0:T(128)S(1)}, f32[96]{0:T(128)}, u32[]{:S(2)}) copy-start(f32[96]{0:T(128)} %param.23) | copy-start | bytes 1156
  3.4 1.2 copy-start.5
  3.4 1.2 copy-start.15
  3.4 1.2 copy-start.16
  4.2 1.2 copy-start.2
  5.4 73.5 %copy-start.7 = (bf16[64,2048]{1,0:T(8,128)(2,1)S(1)}, bf16[64,2048]{1,0:T(8,128)(2,1)}, u32[]{:S(2)}) copy-start(bf16[64,2048]{1,0:T(8,128)(2,1)} %param.27) | copy-start | bytes 786436
  5.4 73.5 %copy-start.10 = (f32[1024]{0:T(1024)S(1)}, f32[1024]{0:T(1024)}, u32[]{:S(2)}) copy-start(f32[1024]{0:T(1024)} %param.25) | copy-start | bytes 12292
  74.5 3.2 %copy-start.1 = (bf16[16,128,2048]{2,1,0:T(8,128)(2,1)}, bf16[16,128,2048]{2,1,0:T(8,128)(2,1)S(1)}, u32[]{:S(2)}) copy-start(bf16[16,128,2048]{2,1,0:T(8,128)(2,1)S(1)} %get-tuple-element.8.all_hbm) | copy-start | bytes 25165828
  78.9 3.3 %copy-start.9 = (f32[2048]{0:T(1024)S(1)}, f32[2048]{0:T(1024)}, u32[]{:S(2)}) copy-start(f32[2048]{0:T(1024)} %param.28) | copy-start | bytes 24580
  78.9 3.4 %copy-start.11 = (s32[64,2]{0,1:T(2,128)S(1)}, s32[64,2]{0,1:T(2,128)}, u32[]{:S(2)}) copy-start(s32[64,2]{0,1:T(2,128)} %param.29) | copy-start | bytes 1540
  79.0 4.3 %copy-start.12 = (f32[64,2]{0,1:T(2,128)S(1)}, f32[64,2]{0,1:T(2,128)}, u32[]{:S(2)}) copy-start(f32[64,2]{0,1:T(2,128)} %param.30) | copy-start | bytes 1540
  82.2 1.5 copy-start.3
  82.2 1.5 copy-start.4

commit v5 on v4

--- a/solution.py
+++ b/solution.py
@@ -59,6 +59,14 @@
     (0, 0), (1, 0), (3, 0), (0, 1), (0, 3), (1, 1), (1, 3), (3, 1),
     (3, 3), (2, 0), (0, 2), (2, 1), (2, 3), (1, 2), (3, 2), (2, 2),
 )
+
+
+EARLY = 5
+
+
+def chunk_order(chips):
+    far = chips // 2
+    return [(1 + n // 2, n % 2) for n in range(2 * far - 1)]
 
 
 def attention(query_rows, bundle, down):
@@ -139,9 +147,7 @@
         def lane_of(way, distance):
             return ((chip + (chips - distance if way == 0 else distance)) % chips) * 2 + core
 
-        def wanted(way, distance, part):
-            far = chips // 2
-            return distance < far or (distance == far and part == way)
+        early_chunks = chunk_order(chips)[:EARLY]
 
         def weight(way, distance, part):
             lane = lane_of(way, distance - 1)
@@ -159,14 +165,13 @@
             return remote(source, all_ref.at[lane, rows],
                           twin_send.at[index], twin_recv.at[index], mine, twin)
 
-        def weights_arrive(distance, parts):
-            for part in parts:
-                for way in (0, 1):
-                    if wanted(way, distance, part):
-                        weight(way, distance, part).wait_recv()
-                        if wanted(way, distance + 1, part):
-                            weight(way, distance + 1, part).start()
-                        share(way, distance, part).start()
+        def weights_arrive(distance, turn):
+            for way in (0, 1):
+                part = turn ^ way
+                weight(way, distance, part).wait_recv()
+                if (distance + 1, turn) in early_chunks:
+                    weight(way, distance + 1, part).start()
+                share(way, distance, part).start()
 
         def at(part, along, across):
             return (along, across) if part == 0 else (across, along)
@@ -226,7 +231,7 @@
             trade(group, own_slot).start()
         for part in (0, 1):
             for way in (0, 1):
-                weight(way, 1, part).start()
+                weight(way, 1, part ^ way).start()
             share(0, 0, part).start()
         for part in (0, 1):
             push(part, (0, 0), at(part, 1, 0), own=True)
@@ -278,27 +283,23 @@
             @pl.when(step == 1)
             def _():
                 pass_across((0,))
-                weights_arrive(1, (0,))
+                weights_arrive(1, 0)
 
             @pl.when(step == 3)
             def _():
-                weights_arrive(1, (1,))
+                weights_arrive(1, 1)
 
             @pl.when(step == 6)
             def _():
-                weights_arrive(2, (0,))
+                weights_arrive(2, 0)
 
             @pl.when(step == 8)
             def _():
-                weights_arrive(2, (1,))
-
-            @pl.when(step == 10)
-            def _():
-                weights_arrive(3, (0,))
-
-            @pl.when(step == 13)
-            def _():
-                weights_arrive(3, (1,))
+                weights_arrive(2, 1)
+
+            @pl.when(step == 11)
+            def _():
+                weights_arrive(3, 0)
 
             @pl.when(step == 2)
             def _():
@@ -387,15 +388,12 @@
         lax.fori_loop(0, tp_count, take_result, None)
         out_ref[...] = tok_ref[...]
 
-        far = chips // 2
-        weights_arrive(far, (0, 1))
         for part in (0, 1):
             share(0, 0, part).wait()
-            for distance in range(1, far + 1):
-                for way in (0, 1):
-                    if wanted(way, distance, part):
-                        weight(way, distance, part).wait_send()
-                        share(way, distance, part).wait()
+        for distance, turn in early_chunks:
+            for way in (0, 1):
+                weight(way, distance, turn ^ way).wait_send()
+                share(way, distance, turn ^ way).wait()
         for group in range(groups):
             trade(group, own_slot).wait_send()
         for message in sent:
@@ -437,7 +435,7 @@
             *[pltpu.SemaphoreType.DMA((4 * chips,)) for _ in range(4)],
         ],
         compiler_params=pltpu.CompilerParams(
-            collective_id=4, has_side_effects=True, vmem_limit_bytes=40 * 1024 * 1024
+            collective_id=4, has_side_effects=True, vmem_limit_bytes=60 * 1024 * 1024
         ),
     )(query_rows, bundle, down)
 
@@ -460,8 +458,8 @@
         choose_ref, token_ref, gate_ref, up_ref, down_hbm, all_hbm, mix_ref, middle_ref, out_ref,
         wide_ref, load_sem, away_ref, got_ref, home_ref, back_ref, ret_ref, x_ref,
         away_send, away_recv, home_send, home_recv,
-        both_ref, down_ref, down_sem, seen, inner_ref, hid_ref, served_ref,
-        fwd_send, fwd_recv, back_send, back_recv, twin_send, twin_recv, hid_send, hid_recv,
+        both_ref, down_ref, down_sem, late_send, late_recv, pair_send, pair_recv, seen, inner_ref, hid_ref, served_ref,
+        hop_send, hop_recv, twin_send, twin_recv, hid_send, hid_recv,
     ):
         place = lax.axis_index("tp")
         chip, core = place // 2, place % 2
@@ -493,25 +491,77 @@
         for load in loads:
             load.start()
 
-        def lane_rows(lane):
-            return pl.ds(pl.multiple_of(lane * hidden, hidden), hidden)
-
-        def load_down(lane):
+        share_rows = hidden // 2
+        chunks_in_order = chunk_order(chips)
+
+        def weight_rows(lane, part):
+            return pl.ds(
+                pl.multiple_of(lane * hidden + part * share_rows, share_rows), share_rows
+            )
+
+        def lane_of(way, distance, side):
+            far = (chip + (chips - distance if way == 0 else distance)) % chips
+            return far * 2 + side
+
+        def load_down(lane, part, index, own=False):
+            rows = pl.ds(part * share_rows, share_rows)
+            source = down_hbm.at[rows] if own else all_hbm.at[lane, rows]
             return pltpu.make_async_copy(
-                all_hbm.at[lane], down_ref.at[lane_rows(lane)], down_sem.at[lane]
-            )
-
-        own_down = pltpu.make_async_copy(
-            down_hbm, down_ref.at[lane_rows(place)], down_sem.at[place]
-        )
-        own_down.start()
-
-        def fetch(lane, _):
-            @pl.when(lane != place)
-            def _():
-                load_down(lane).start()
-
-        lax.fori_loop(0, 2 * chips, fetch, None)
+                source, down_ref.at[weight_rows(lane, part)], down_sem.at[index]
+            )
+
+        def down_loads():
+            loads = []
+            for part in (0, 1):
+                loads.append(load_down(place, part, len(loads), own=True))
+                loads.append(load_down(twin, part, len(loads)))
+            for distance, turn in chunks_in_order[:EARLY]:
+                for way in (0, 1):
+                    for side in (0, 1):
+                        lane = lane_of(way, distance, side)
+                        loads.append(load_down(lane, turn ^ way, len(loads)))
+            return loads
+
+        for load in down_loads():
+            load.start()
+
+        def late_copy(source, target, sems, index, other):
+            return pltpu.make_async_remote_copy(
+                src_ref=source,
+                dst_ref=target,
+                send_sem=sems[0].at[index],
+                recv_sem=sems[1].at[index],
+                device_id={"tp": other},
+                device_id_type=pl.DeviceIdType.MESH,
+            )
+
+        def late_weights():
+            copies = []
+            for distance, turn in chunks_in_order[EARLY:]:
+                for way in (0, 1):
+                    part = turn ^ way
+                    lane = lane_of(way, distance - 1, core)
+                    following = ((chip + (1 if way == 0 else chips - 1)) % chips) * 2 + core
+                    copies.append(
+                        late_copy(
+                            all_hbm.at[lane, pl.ds(part * share_rows, share_rows)],
+                            down_ref.at[weight_rows(lane, part)],
+                            (late_send, late_recv), len(copies), following,
+                        )
+                    )
+            return copies
+
+        def late_shares():
+            copies = []
+            for distance, turn in chunks_in_order[EARLY:]:
+                for way in (0, 1):
+                    rows = weight_rows(lane_of(way, distance, core), turn ^ way)
+                    copies.append(
+                        late_copy(down_ref.at[rows], down_ref.at[rows],
+                                  (pair_send, pair_recv), len(copies), twin)
+                    )
+            return copies
+
         chosen = jnp.dot(choose_ref[...], token_ref[...], preferred_element_type=jnp.float32)
         for chunk in range(chunks):
             wide_ref[pl.ds(chunk, count, stride=chunks), :] = chosen[
@@ -519,6 +569,8 @@
             ]
         away_ref[...] = wide_ref[...].astype(jnp.bfloat16)
         pl.semaphore_wait(barrier, 3 + places - 1)
+        for copy in late_weights():
+            copy.start()
 
         def slab_of(place):
             return pl.ds(pl.multiple_of(place * slab, slab), slab)
@@ -568,20 +620,22 @@
         first, second = pl.ds(0, ROW_CUT), pl.ds(ROW_CUT, count - ROW_CUT)
         front, rear = pl.ds(0, count), pl.ds(count, count)
 
-        def forward(step):
-            return (
-                remote(seen.at[step, first], seen.at[step + 1, first],
-                       fwd_send.at[step], fwd_recv.at[step + 1], ahead),
-                remote(seen.at[step, second], seen.at[step + 1, second],
-                       back_send.at[step], back_recv.at[step + 1], behind),
-            )
-
-        def forward_own():
-            return (
-                remote(x_ref.at[first], seen.at[1, first], fwd_send.at[0], fwd_recv.at[1], ahead),
-                remote(x_ref.at[second], seen.at[1, second],
-                       back_send.at[0], back_recv.at[1], behind),
-            )
+        cuts = ((0, 48), (80, 32), (48, 32), (112, 32))
+
+        def forward(step, source=None):
+            copies = []
+            for index, (start, size) in enumerate(cuts):
+                rows = pl.ds(start, size)
+                copies.append(
+                    remote(
+                        seen.at[step, rows] if source is None else source.at[rows],
+                        seen.at[step + 1, rows],
+                        hop_send.at[step * 4 + index],
+                        hop_recv.at[step * 4 + index],
+                        ahead if start < ROW_CUT else behind,
+                    )
+                )
+            return copies
 
         def share(step):
             return remote(seen.at[step, front], seen.at[step, rear],
@@ -622,7 +676,7 @@
                 jnp.bfloat16
             )
 
-        for copy in (*forward_own(), share_own()):
+        for copy in (*forward(0, x_ref), share_own()):
             copy.start()
         for load in loads:
             load.wait()
@@ -633,32 +687,48 @@
         for copy in tell(0)[2:]:
             copy.start()
 
-        def step_of(step, _):
-            for copy in forward(step - 1):
-                copy.wait_recv()
-
-            @pl.when(step < chips - 1)
-            def _():
-                for copy in forward(step):
-                    copy.start()
-
-            share(step).start()
+        def finish_step(step):
             share(step).wait_recv()
             experts(step)
             for copy in tell(step):
                 copy.start()
 
+        def step_of(step, _):
+            for arrived, onward in zip(forward(step - 1), forward(step)):
+                arrived.wait_recv()
+
+                @pl.when(step < chips - 1)
+                def _():
+                    onward.start()
+
+            share(step).start()
+
+            @pl.when(step == 2)
+            def _():
+                for copy, onward in zip(late_weights(), late_shares()):
+                    copy.wait_recv()
+                    onward.start()
+
+            @pl.when(step > 1)
+            def _():
+                finish_step(step - 1)
+
         lax.fori_loop(1, chips, step_of, None)
+        finish_step(chips - 1)
 
         def gathered(lane, _):
             @pl.when(lane != place)
             def _():
-                load_down(lane).wait()
                 for copy in hear(lane):
                     copy.wait_recv()
 
         lax.fori_loop(0, 2 * chips, gathered, None)
-        own_down.wait()
+        for load in down_loads():
+            load.wait()
+        for copy in late_shares():
+            copy.wait()
+        for copy in late_weights():
+            copy.wait_send()
 
         def project(index, _):
             columns = pl.ds(pl.multiple_of(index * 512, 512), 512)
@@ -689,7 +759,7 @@
 
         lax.fori_loop(1, places, settle, None)
 
-        for copy in (*forward_own(), share_own(), *tell(0)[2:]):
+        for copy in (*forward(0, x_ref), share_own(), *tell(0)[2:]):
             copy.wait_send()
 
         def drain(step, _):
@@ -705,8 +775,7 @@
         lax.fori_loop(1, chips, drain, None)
 
     block = (count, width)
-    sems = [pltpu.SemaphoreType.DMA((chips + 1,)) for _ in range(6)]
-    sems += [pltpu.SemaphoreType.DMA((4 * chips,)) for _ in range(2)]
+    sems = [pltpu.SemaphoreType.DMA((4 * chips,)) for _ in range(6)]
     return pl.pallas_call(
         kernel,
         out_shape=jax.ShapeDtypeStruct(middle.shape, jnp.bfloat16),
@@ -723,7 +792,8 @@
             *[pltpu.SemaphoreType.DMA((places,)) for _ in range(4)],
             pltpu.VMEM((width, 2 * hidden), jnp.bfloat16),
             pltpu.VMEM((2 * chips * hidden, width), jnp.bfloat16),
-            pltpu.SemaphoreType.DMA((2 * chips,)),
+            pltpu.SemaphoreType.DMA((4 + 4 * EARLY,)),
+            *[pltpu.SemaphoreType.DMA((2 * chips,)) for _ in range(4)],
             pltpu.VMEM((chips, both, width), jnp.bfloat16),
             pltpu.VMEM((chips, both, hidden), jnp.bfloat16),
             pltpu.VMEM((count, 2 * chips * hidden), jnp.bfloat16),
@@ -731,7 +801,7 @@
             *sems,
         ],
         compiler_params=pltpu.CompilerParams(
-            collective_id=3, has_side_effects=True, vmem_limit_bytes=50 * 1024 * 1024
+            collective_id=3, has_side_effects=True, vmem_limit_bytes=60 * 1024 * 1024
         ),
     )(chooser, ffn_input, gate, up, down, all_down, near_weights, middle)
 

time: 186 us -> 183 us (0.984)
  Pallas kernels: 169 us -> 166 us
  other arithmetic: 3.24 us -> 5.37 us
    pallas_call x1, Pallas kernels: 69 us -> 65.7 us  [attention(): pl.pallas_call(kernel, out_shape=(jax.ShapeDtypeStruct((tp_count, pack, 1...]
    unnamed x38 -> x34, local copies, waits for them, and re-layouts: 4.68 us -> 2.43 us
where the time goes in v5:
time: 183 us
  Pallas kernels  166 us (91%)
  local copies, waits for them, and re-layouts  6.22 us (3%)
  matrix products  5.56 us (3%)
  other arithmetic  5.37 us (3%)
    pallas_call x1, Pallas kernels, expert_ring(): pl.pallas_call(kernel, out_shape=jax.ShapeDtypeStruct(middle.shape, jnp.b...  99.9 us
    pallas_call x1, Pallas kernels, attention(): pl.pallas_call(kernel, out_shape=(jax.ShapeDtypeStruct((tp_count, pack, 1...  65.7 us

profile of v5, /device:TPU:1, one launch (start us, length us, event | category | flops | bytes accessed | tf_op | source)
XLA Modules:
  0.0 183.1 jit_solution(14526150938604061307)
XLA Ops:
  0.0 0.0 copy-start
  0.0 0.0 copy-start.6
  0.0 0.0 copy-start.11
  0.0 0.0 copy-start.3
  0.0 0.0 copy-start.12
  0.0 1.6 fusion
  1.6 0.0 copy-done
  1.6 1.8 fusion.3
  3.4 0.0 copy-start.2
  3.4 0.0 copy-start.13
  3.4 0.0 copy-start.14
  3.4 0.0 copy-done.6
  3.4 0.1 fusion.8
  3.5 0.0 copy-done.11
  3.5 0.1 fusion.9
  3.6 0.0 copy-done.3
  3.6 0.1 fusion.5
  3.7 0.0 copy-done.12
  3.7 0.1 fusion.7
  3.8 0.3 fusion.36
  4.3 0.4 copy-done.2
  4.6 0.0 copy-done.13
  4.6 0.0 copy-done.14
  4.6 0.6 fusion.4
  5.2 0.8 pad_maximum_fusion.own_ref
  6.0 0.2 copy.53
  6.1 0.0 copy-start.5
  6.2 0.0 copy-start.8
  6.2 0.8 pad.4.clone.q_ref
  6.9 65.7 %shard_map.163 = (bf16[16,32,128]{2,1,0:T(8,128)(2,1)}, bf16[16,128,2048]{2,1,0:T(8,128)(2,1)}) custom-call(bf16[1024,128]{1,0:T(8,128)(2,1)} %pad.4.clone.q_ref, bf16[160,1024]{1,0:T(8,128)(2,1)} %pad_maximum_fusion.own_ref, bf16[128,2048]{1,0:T(8,128)(2,1)} %bitcast.40), custom_call_target="tpu_custom_call" | custom-call | tf_op jit(solution)/shard_map/pallas_call | solution.py:409
  72.7 0.0 copy-start.4
  72.7 1.3 reshape.371
  74.0 0.3 copy.56
  74.3 0.2 reshape.370
  74.5 0.0 copy-done.4
  74.5 0.1 reduce_sum.80
  74.6 0.1 reduce_sum.81
  74.7 0.1 copy.54
  74.8 0.1 rsqrt.47
  74.9 0.0 copy-done.5
  74.9 0.0 copy-done.8
  74.9 0.0 copy-start.7
  74.9 0.0 copy-start.9
  74.9 0.0 copy-start.10
  74.9 3.2 %multiply_reduce_fusion = (f32[64]{0:T(128)S(1)}, f32[64,2048]{1,0:T(8,128)S(1)}) fusion(bf16[1024,2048]{1,0:T(8,128)(2,1)} %param.26, f32[64,1024]{1,0:T(8,128)S(1)} %reshape.370, f32[1024]{0:T(1024)S(1)} %copy-done.8, f32[64]{0:T(128)S(1)} %rsqrt.47, bf16[64,2048]{1,0:T(8,128)(2,1)S(1)} %copy-done.5), kind=kOutput, calls=%fused_computation.12 | convolution fusion | flops 269156288 | bytes 5247488 | tf_op jit(solution)/shard_map/dot_general | solution.py:862
  78.1 0.0 copy-start.1
  78.2 0.0 copy-done.7
  78.2 0.9 multiply_convert_fusion.token_ref
  79.0 0.0 copy-done.9
  79.0 0.1 copy.46
  79.1 0.1 eq.42
  79.3 0.1 fusion.34
  79.4 0.2 reduce_window_sum.11
  79.5 0.2 select_reduce_fusion.1
  79.7 0.1 reduce_sum.75
  79.9 0.1 copy.47
  79.9 0.0 copy-done.10
  79.9 0.1 select_reduce_fusion
  80.1 0.7 pad_maximum_fusion.3.mix_ref
  80.8 0.1 fusion.16
  80.9 0.7 copy.51.choose_ref
  81.6 0.0 copy-done.1
  81.6 99.9 %shard_map.164 = bf16[64,2048]{1,0:T(8,128)(2,1)} custom-call(bf16[144,64]{1,0:T(8,128)(2,1)} %copy.51.choose_ref, bf16[64,2048]{1,0:T(8,128)(2,1)} %multiply_convert_fusion.token_ref, bf16[2048,128]{1,0:T(8,128)(2,1)} %bitcast.43, bf16[2048,128]{1,0:T(8,128)(2,1)} %bitcast.44, bf16[128,2048]{1,0:T(8,128)(2,1)} %bitcast.41, ...), custom_call_target="tpu_custom_call" | custom-call | tf_op jit(solution)/shard_map/pallas_call | solution.py:779
  181.4 1.7 copy.58
  (14 shorter events, 0.2 us)
Async XLA Ops:
  0.0 1.6 copy-start
  0.0 3.4 %copy-start.6 = (bf16[1024,32]{0,1:T(8,128)(2,1)S(1)}, bf16[1024,32]{0,1:T(8,128)(2,1)}, u32[]{:S(2)}) copy-start(bf16[1024,32]{0,1:T(8,128)(2,1)} %param.19) | copy-start | bytes 196612
  0.0 3.5 %copy-start.11 = (f32[96]{0:T(128)S(1)}, f32[96]{0:T(128)}, u32[]{:S(2)}) copy-start(f32[96]{0:T(128)} %param.24) | copy-start | bytes 1156
  0.0 3.6 %copy-start.3 = (bf16[1024,96]{0,1:T(8,128)(2,1)S(1)}, bf16[1024,96]{0,1:T(8,128)(2,1)}, u32[]{:S(2)}) copy-start(bf16[1024,96]{0,1:T(8,128)(2,1)} %param.17) | copy-start | bytes 589828
  0.0 3.7 %copy-start.12 = (f32[96]{0:T(128)S(1)}, f32[96]{0:T(128)}, u32[]{:S(2)}) copy-start(f32[96]{0:T(128)} %param.23) | copy-start | bytes 1156
  3.4 1.2 copy-start.2
  3.4 1.2 copy-start.13
  3.4 1.2 copy-start.14
  6.1 68.7 %copy-start.5 = (bf16[64,2048]{1,0:T(8,128)(2,1)S(1)}, bf16[64,2048]{1,0:T(8,128)(2,1)}, u32[]{:S(2)}) copy-start(bf16[64,2048]{1,0:T(8,128)(2,1)} %param.27) | copy-start | bytes 786436
  6.2 68.7 %copy-start.8 = (f32[1024]{0:T(1024)S(1)}, f32[1024]{0:T(1024)}, u32[]{:S(2)}) copy-start(f32[1024]{0:T(1024)} %param.25) | copy-start | bytes 12292
  72.7 1.8 copy-start.4
  74.9 3.3 %copy-start.7 = (f32[2048]{0:T(1024)S(1)}, f32[2048]{0:T(1024)}, u32[]{:S(2)}) copy-start(f32[2048]{0:T(1024)} %param.28) | copy-start | bytes 24580
  74.9 4.1 %copy-start.9 = (s32[64,2]{0,1:T(2,128)S(1)}, s32[64,2]{0,1:T(2,128)}, u32[]{:S(2)}) copy-start(s32[64,2]{0,1:T(2,128)} %param.29) | copy-start | bytes 1540
  74.9 5.0 %copy-start.10 = (f32[64,2]{0,1:T(2,128)S(1)}, f32[64,2]{0,1:T(2,128)}, u32[]{:S(2)}) copy-start(f32[64,2]{0,1:T(2,128)} %param.30) | copy-start | bytes 1540
  78.1 3.4 %copy-start.1 = (f32[64,2048]{1,0:T(8,128)}, f32[64,2048]{1,0:T(8,128)S(1)}, u32[]{:S(2)}) copy-start(f32[64,2048]{1,0:T(8,128)S(1)} %get-tuple-element.19.middle_ref) | copy-start | bytes 1572868

commit v6 on v0

v6 whole, which is shorter than its diff:
```python
import jax
import jax.numpy as jnp
from jax import lax
from jax.experimental import pallas as pl
from jax.experimental.pallas import tpu as pltpu
from jax.sharding import PartitionSpec as P

D = 2048
NOPE = 64
ROPE = 32
VH = 64
TOPK = 2
QK = 96


epsilon = 1e-06
rope_base = 10000.0


def rms_scale(values):
    return lax.rsqrt(jnp.mean(values * values, axis=-1, keepdims=True) + epsilon)


def rotate_half(values, angles):
    half_dims = values.shape[-1] // 2
    first_half = values[..., :half_dims]
    second_half = values[..., half_dims:]
    cosine = jnp.cos(angles)
    sine_val = jnp.sin(angles)
    return jnp.concatenate(
        [
            first_half * cosine - second_half * sine_val,
            second_half * cosine + first_half * sine_val,
        ],
        axis=-1,
    )


def head_prepare(raw_rows, gain_vec, angles):
    normed_rows = raw_rows * rms_scale(raw_rows) * gain_vec
    turned_rows = rotate_half(normed_rows[..., NOPE:], angles[:, None, :])
    return jnp.concatenate([normed_rows[..., :NOPE], turned_rows], axis=-1).astype(jnp.bfloat16)


def slot_targets(route_rows, expert_total, slot_cap):
    flat_routes = route_rows.reshape(-1)
    one_hot = (flat_routes[:, None] == jnp.arange(expert_total, dtype=jnp.int32)[None, :]).astype(
        jnp.int32
    )
    earlier = jnp.cumsum(one_hot, axis=0) - one_hot
    rank_in = jnp.sum(earlier * one_hot, axis=1)
    return (flat_routes * slot_cap + rank_in).reshape(route_rows.shape)


SCORE_EXP = 1.4426950408889634 * QK ** (-0.5)
Q_TILE = 256
SIDE = 4
VISITS = (
    (0, 0), (1, 0), (3, 0), (0, 1), (0, 3), (1, 1), (1, 3), (3, 1),
    (3, 3), (2, 0), (0, 2), (2, 1), (2, 3), (1, 2), (3, 2), (2, 2),
)


WEIGHT_STEPS = (1, 3, 6, 8, 11, 13)


def chunk_order(chips):
    far = chips // 2
    return [(1 + n // 2, n % 2) for n in range(2 * far - 1)]


def attention_phase(
    q_ref, own_ref, down_ref, project_hbm, res_ref, out_gain_ref, ffn_gain_ref,
    out_ref, middle_ref, all_ref, project_ref, project_sem, att_ref,
    kv_ref, pair_ref, peak_ref, acc_ref, val_ref, done_ref, tok_ref,
    kv_send, kv_recv, q_send, q_recv, out_send, out_recv,
    w_send, w_recv, twin_send, twin_recv, meet,
):
    shard_len = q_ref.shape[0]
    half = shard_len // 2
    block_count = lax.axis_size("sp")
    tp_count = lax.axis_size("tp")
    tok = shard_len // tp_count
    chips = tp_count // 2
    pack = tok // 2
    groups = tp_count // 4
    hidden = down_ref.shape[0]
    share_rows = hidden // 2
    part_rows = own_ref.shape[0] // 2
    mine = lax.axis_index("sp")
    head = lax.axis_index("tp")
    mirror = block_count - 1 - mine
    low = jnp.minimum(mine, mirror)
    high = jnp.maximum(mine, mirror)
    early = mine < block_count // 2
    shift = pl.multiple_of(jnp.where(early, 0, 2 * tok), 2 * tok)
    own_slot = pl.multiple_of(jnp.where(early, 0, half), half)
    far_slot = pl.multiple_of(half - own_slot, half)
    chip, core = head // 2, head % 2
    twin = chip * 2 + 1 - core
    row, col = mine // SIDE, mine % SIDE

    def block_at(dx, dy):
        return ((row + dy) % SIDE) * SIDE + (col + dx) % SIDE

    project_load = pltpu.make_async_copy(project_hbm, project_ref, project_sem.at[0])
    project_load.start()
    own_load = pltpu.make_async_copy(down_ref, all_ref.at[head], project_sem.at[1])
    own_load.start()
    meet()
    def remote(source, target, send, recv, place, lane):
        return pltpu.make_async_remote_copy(
            src_ref=source,
            dst_ref=target,
            send_sem=send,
            recv_sem=recv,
            device_id={"sp": place, "tp": lane},
            device_id_type=pl.DeviceIdType.MESH,
        )

    def queries_of(group, offset):
        return q_ref.at[pl.ds(pl.multiple_of(group * 4 * tok + offset, 2 * tok), 2 * tok)]

    def trade(group, slot):
        target = pair_ref.at[pl.ds(pl.multiple_of(slot + group * 2 * tok, 2 * tok), 2 * tok)]
        return remote(queries_of(group, 2 * tok - shift), target,
                      q_send.at[group], q_recv.at[group], mirror, head)

    def lane_of(way, distance):
        return ((chip + (chips - distance if way == 0 else distance)) % chips) * 2 + core

    early_chunks = chunk_order(chips)

    def weight(way, distance, part):
        lane = lane_of(way, distance - 1)
        rows = pl.ds(part * share_rows, share_rows)
        source = down_ref.at[rows] if distance == 1 else all_ref.at[lane, rows]
        index = (way * chips + distance) * 2 + part
        return remote(source, all_ref.at[lane, rows], w_send.at[index], w_recv.at[index],
                      mine, ((chip + (1 if way == 0 else chips - 1)) % chips) * 2 + core)

    def share(way, distance, part):
        lane = lane_of(way, distance)
        rows = pl.ds(part * share_rows, share_rows)
        source = down_ref.at[rows] if distance == 0 else all_ref.at[lane, rows]
        index = (way * chips + distance) * 2 + part
        return remote(source, all_ref.at[lane, rows],
                      twin_send.at[index], twin_recv.at[index], mine, twin)

    def weights_arrive(distance, turn):
        for way in (0, 1):
            part = turn ^ way
            weight(way, distance, part).wait_recv()
            if (distance + 1, turn) in early_chunks:
                weight(way, distance + 1, part).start()
            share(way, distance, part).start()

    def at(part, along, across):
        return (along, across) if part == 0 else (across, along)

    def piece(part, where, way, own=False, side=None):
        block = block_at(*where)
        rows = pl.ds(part * part_rows, part_rows)
        cols = slice(None) if side is None else pl.ds(side * half, half)
        index = (part * block_count + block) * 2
        source = own_ref.at[rows] if own else kv_ref.at[block, rows, cols]
        compass = ((1, 0), (3, 0), (0, 1), (0, 3)).index(way)
        return remote(source, kv_ref.at[block, rows, cols],
                      kv_send.at[index * 2 + compass],
                      kv_recv.at[index + (0 if side is None else side)],
                      block_at(*way), head)

    def landed(part, where, side=None):
        piece(part, where, (1, 0), side=side).wait_recv()

    sent = []

    def push(part, where, way, own=False, side=None):
        piece(part, where, way, own, side).start()
        sent.append((part, where, way, own, side))

    def spread(part, where):
        push(part, where, at(part, 0, 1))
        push(part, where, at(part, 0, 3))

    def neighbours_first():
        for part in (0, 1):
            for along, side, way in ((3, 0, 1), (1, 1, 3)):
                landed(part, at(part, along, 0))
                push(part, at(part, along, 0), at(part, way, 0), side=side)
                spread(part, at(part, along, 0))

    def pass_across(alongs):
        for part in (0, 1):
            for along in alongs:
                for across, side, way in ((3, 0, 1), (1, 1, 3)):
                    landed(part, at(part, along, across))
                    push(part, at(part, along, across), at(part, 0, way), side=side)

    def far_first():
        for part in (0, 1):
            landed(part, at(part, 2, 0), 0)
            landed(part, at(part, 2, 0), 1)
            spread(part, at(part, 2, 0))

    def far_across(alongs):
        for part in (0, 1):
            for along in alongs:
                landed(part, at(part, along, 2), 0)
                landed(part, at(part, along, 2), 1)

    for group in range(groups):
        trade(group, own_slot).start()
    for part in (0, 1):
        for way in (0, 1):
            weight(way, 1, part ^ way).start()
        share(0, 0, part).start()
    for part in (0, 1):
        push(part, (0, 0), at(part, 1, 0), own=True)
        push(part, (0, 0), at(part, 3, 0), own=True)
    for part in (0, 1):
        push(part, (0, 0), at(part, 0, 1), own=True)
        push(part, (0, 0), at(part, 0, 3), own=True)
    kv_ref[mine] = own_ref[...]
    for group in range(groups):
        target = pl.ds(pl.multiple_of(own_slot + group * 2 * tok, 2 * tok), 2 * tok)
        pair_ref[target, :] = queries_of(group, shift)[...]
    peak_ref[...] = jnp.full_like(peak_ref, -1e30)
    acc_ref[...] = jnp.zeros_like(acc_ref)
    lane = lax.broadcasted_iota(jnp.int32, (shard_len, 128), 1)
    val_ref[...] = jnp.where(lane == VH, 1.0, 0.0).astype(jnp.bfloat16)

    def attend(block, parts):
        keys = kv_ref[block, :QK, :]
        val_ref[:, :VH] = kv_ref[block, QK:, :].T
        values = val_ref[...]
        for start, masked in parts:
            for first in range(start, start + half, Q_TILE):
                rows = pl.ds(first, Q_TILE)
                scores = jnp.dot(
                    pair_ref[rows, :QK], keys, preferred_element_type=jnp.float32
                )
                if masked:
                    q_pos = lax.broadcasted_iota(jnp.int32, scores.shape, 0)
                    k_pos = lax.broadcasted_iota(jnp.int32, scores.shape, 1)
                    q_pos = q_pos + (first - start)
                    q_pos = q_pos + (q_pos // (2 * tok)) * (2 * tok)
                    scores = jnp.where(k_pos - q_pos <= shift, scores, -1e30)
                old = peak_ref[rows, :]
                new = jnp.maximum(old, jnp.max(scores, axis=1, keepdims=True))
                weights = jnp.exp2((scores - new[:, :1]) * SCORE_EXP).astype(jnp.bfloat16)
                factor = jnp.exp2((old - new) * SCORE_EXP)
                peak_ref[rows, :] = new
                acc_ref[rows, :] = acc_ref[rows, :] * factor + jnp.dot(
                    weights, values, preferred_element_type=jnp.float32
                )

    def visit(step, _):
        @pl.when(step == 0)
        def _():
            neighbours_first()
            for group in range(groups):
                trade(group, far_slot).wait_recv()

        @pl.when(step == 1)
        def _():
            pass_across((0,))

        for turn_at, chunk in zip(WEIGHT_STEPS, early_chunks):

            @pl.when(step == turn_at)
            def _(chunk=chunk):
                weights_arrive(*chunk)

        @pl.when(step == 2)
        def _():
            far_first()

        @pl.when(step == 5)
        def _():
            pass_across((1, 3))

        @pl.when(step == 9)
        def _():
            far_across((0,))
            pass_across((2,))

        @pl.when(step == 11)
        def _():
            far_across((1, 3))

        @pl.when(step == 15)
        def _():
            far_across((2,))

        dx = sum(jnp.where(step == k, v[0], 0) for k, v in enumerate(VISITS) if v[0])
        dy = sum(jnp.where(step == k, v[1], 0) for k, v in enumerate(VISITS) if v[1])
        block = block_at(dx, dy)

        @pl.when(block < low)
        def _():
            attend(block, ((0, False), (half, False)))

        @pl.when(block == low)
        def _():
            attend(block, ((0, True), (half, False)))

        @pl.when((block > low) & (block < high))
        def _():
            attend(block, ((half, False),))

        @pl.when(block == high)
        def _():
            attend(block, ((half, True),))

    lax.fori_loop(0, block_count, visit, None)
    shares = (acc_ref[...] / acc_ref[:, VH : VH + 1]).reshape(tp_count, 2, pack, 128)
    lanes = lax.broadcasted_iota(jnp.int32, (tp_count, pack, 128), 2)
    done_ref[...] = (
        jnp.where(lanes < VH, shares[:, 0], pltpu.roll(shares[:, 1], VH, 2))
        .reshape(tp_count * pack, 128)
        .astype(jnp.bfloat16)
    )

    per_slot = tp_count // 2

    def piece_of(slot, order):
        return pl.ds(pl.multiple_of((slot // tok + order) * pack, pack), pack)

    def result(index):
        side, order = index // per_slot, index % per_slot
        slot = jnp.where(side == 0, own_slot, far_slot)
        return remote(done_ref.at[piece_of(slot, order)], tok_ref.at[head],
                      out_send.at[index], out_recv.at[head],
                      jnp.where(side == 0, mine, mirror),
                      (order // 2) * 4 + shift // tok + order % 2)

    here = (chip % 2) * 2 * tok == shift
    self_order = (head // 4) * 2 + core
    self_index = jnp.where(here, self_order, tp_count)

    def send_result(index, _):
        @pl.when(index != self_index)
        def _():
            result(index).start()

    lax.fori_loop(0, tp_count, send_result, None)

    @pl.when(here)
    def _():
        tok_ref[head] = done_ref[piece_of(own_slot, self_order), :]

    def take_result(index, _):
        @pl.when(jnp.logical_not(here & (index == head)))
        def _():
            remote(done_ref.at[pl.ds(0, pack)], tok_ref.at[index],
                   out_send.at[index], out_recv.at[index], mirror, head).wait_recv()

    lax.fori_loop(0, tp_count, take_result, None)
    token_heads = tok_ref[...].astype(jnp.float32)
    squares = jnp.sum(token_heads * token_heads, axis=0)
    lane_id = lax.broadcasted_iota(jnp.int32, (pack, 128), 1)
    left = lane_id < VH
    scales = [
        lax.rsqrt(
            jnp.sum(jnp.where(side, squares, 0.0), axis=1, keepdims=True)
            * (1.0 / (tp_count * VH))
            + epsilon
        )
        for side in (left, lane_id >= VH)
    ]
    for pair in range(tp_count // 2):
        columns = pl.ds(pair * 128, 128)
        one, two = token_heads[2 * pair], token_heads[2 * pair + 1]
        top = jnp.where(left, one, pltpu.roll(two, VH, 1)) * scales[0]
        bottom = jnp.where(left, pltpu.roll(one, VH, 1), two) * scales[1]
        att_ref[:pack, columns] = (top * out_gain_ref[:, columns]).astype(jnp.bfloat16)
        att_ref[pack:, columns] = (bottom * out_gain_ref[:, columns]).astype(jnp.bfloat16)
    project_load.wait()
    middle = res_ref[...].astype(jnp.float32) + jnp.dot(
        att_ref[...], project_ref[...], preferred_element_type=jnp.float32
    )
    middle_ref[...] = middle
    out_ref[...] = (middle * rms_scale(middle) * ffn_gain_ref[...]).astype(jnp.bfloat16)

    def late():
        for chunk in early_chunks[len(WEIGHT_STEPS) :]:
            weights_arrive(*chunk)

    def finish():
        own_load.wait()
        for part in (0, 1):
            share(0, 0, part).wait()
        for distance, turn in early_chunks:
            for way in (0, 1):
                weight(way, distance, turn ^ way).wait_send()
                share(way, distance, turn ^ way).wait()
        for group in range(groups):
            trade(group, own_slot).wait_send()
        for message in sent:
            piece(*message).wait_send()

        def drain(index, _):
            @pl.when(index != self_index)
            def _():
                result(index).wait_send()

        lax.fori_loop(0, tp_count, drain, None)

    return late, finish


ROW_CUT = 80


def expert_loads(gate_ref, up_ref, both_ref, load_sem):
    hidden = gate_ref.shape[1]
    return (
        pltpu.make_async_copy(gate_ref, both_ref.at[:, pl.ds(0, hidden)], load_sem.at[0]),
        pltpu.make_async_copy(up_ref, both_ref.at[:, pl.ds(hidden, hidden)], load_sem.at[1]),
    )


def expert_phase(
    choose_ref, token_ref, down_ref, mix_ref, middle_ref, out_ref, loads, late, finish,
    wide_ref, away_ref, got_ref, home_ref, back_ref, ret_ref, x_ref,
    away_send, away_recv, home_send, home_recv, both_ref, seen, inner_ref, hid_ref, served_ref,
    hop_send, hop_recv, twin_send, twin_recv, hid_send, hid_recv,
):
    count = choose_ref.shape[0]
    width = token_ref.shape[1]
    places = lax.axis_size("sp")
    chunks = width // 128
    slab = (count // places) * chunks
    hidden = down_ref.shape[1]
    chips = lax.axis_size("tp") // 2
    place = lax.axis_index("tp")
    chip, core = place // 2, place % 2
    toward = jnp.where(core == 0, 1, chips - 1)
    ahead = ((chip + toward) % chips) * 2 + core
    behind = ((chip + chips - toward) % chips) * 2 + core
    twin = chip * 2 + 1 - core

    mine = lax.axis_index("sp")

    def peer(turn):
        return (mine + turn) % places

    chosen = jnp.dot(choose_ref[...], token_ref[...], preferred_element_type=jnp.float32)
    for chunk in range(chunks):
        wide_ref[pl.ds(chunk, count, stride=chunks), :] = chosen[
            :, chunk * 128 : (chunk + 1) * 128
        ]
    away_ref[...] = wide_ref[...].astype(jnp.bfloat16)

    def slab_of(place):
        return pl.ds(pl.multiple_of(place * slab, slab), slab)

    def swap(source, target, send, recv, turn):
        return pltpu.make_async_remote_copy(
            src_ref=source.at[slab_of(peer(turn))],
            dst_ref=target.at[slab_of(mine)],
            send_sem=send.at[turn],
            recv_sem=recv.at[turn],
            device_id={"sp": peer(turn)},
            device_id_type=pl.DeviceIdType.MESH,
        )

    def exchange(source, target, send, recv):
        def start(turn, _):
            swap(source, target, send, recv, turn).start()

        lax.fori_loop(1, places, start, None)
        target[slab_of(mine), :] = source[slab_of(mine), :]

        def finish(turn, _):
            swap(source, target, send, recv, turn).wait_recv()

        lax.fori_loop(1, places, finish, None)

    def narrow(target):
        for chunk in range(chunks):
            target[:, pl.ds(chunk * 128, 128)] = wide_ref[
                pl.ds(chunk, count, stride=chunks), :
            ].astype(jnp.bfloat16)

    exchange(away_ref, got_ref, away_send, away_recv)
    wide_ref[...] = got_ref[...].astype(jnp.float32)
    narrow(x_ref)

    def remote(source, target, send, recv, other):
        return pltpu.make_async_remote_copy(
            src_ref=source,
            dst_ref=target,
            send_sem=send,
            recv_sem=recv,
            device_id={"tp": other},
            device_id_type=pl.DeviceIdType.MESH,
        )

    first, second = pl.ds(0, ROW_CUT), pl.ds(ROW_CUT, count - ROW_CUT)
    front, rear = pl.ds(0, count), pl.ds(count, count)

    cuts = ((0, 48), (80, 32), (48, 32), (112, 32))

    def forward(step, source=None):
        copies = []
        for index, (start, size) in enumerate(cuts):
            rows = pl.ds(start, size)
            copies.append(
                remote(
                    seen.at[step, rows] if source is None else source.at[rows],
                    seen.at[step + 1, rows],
                    hop_send.at[step * 4 + index],
                    hop_recv.at[step * 4 + index],
                    ahead if start < ROW_CUT else behind,
                )
            )
        return copies

    def share(step):
        return remote(seen.at[step, front], seen.at[step, rear],
                      twin_send.at[step], twin_recv.at[step], twin)

    def share_own():
        return remote(x_ref, seen.at[0, rear], twin_send.at[0], twin_recv.at[0], twin)

    def chip_at(distance):
        return (chip + chips + distance) % chips

    def tell(step):
        away, near = toward * step, (chips - toward) * step
        parts = (
            (first, 0, chip_at(near) * 2 + core, 0),
            (second, ROW_CUT, chip_at(away) * 2 + core, 1),
            (first, count, chip_at(away) * 2 + 1 - core, 0),
            (second, count + ROW_CUT, chip_at(near) * 2 + 1 - core, 1),
        )
        columns = pl.ds(pl.multiple_of(place * hidden, hidden), hidden)
        return [
            remote(inner_ref.at[step, pl.ds(start, rows.size)], hid_ref.at[rows, columns],
                   hid_send.at[step * 4 + order], hid_recv.at[place * 2 + half], owner)
            for order, (rows, start, owner, half) in enumerate(parts)
        ]

    def hear(lane):
        columns = pl.ds(pl.multiple_of(lane * hidden, hidden), hidden)
        return [
            remote(inner_ref.at[0, pl.ds(0, rows.size)], hid_ref.at[rows, columns],
                   hid_send.at[half], hid_recv.at[lane * 2 + half], twin)
            for half, rows in enumerate((first, second))
        ]

    def experts(step):
        pre = jnp.dot(seen[step], both_ref[...], preferred_element_type=jnp.float32)
        inner_ref[step] = (jax.nn.silu(pre[:, :hidden]) * pre[:, hidden:]).astype(
            jnp.bfloat16
        )

    for copy in (*forward(0, x_ref), share_own()):
        copy.start()
    for load in loads:
        load.wait()
    seen[0, front, :] = x_ref[...]
    share_own().wait_recv()
    experts(0)
    hid_ref[:, pl.ds(pl.multiple_of(place * hidden, hidden), hidden)] = inner_ref[0, front, :]
    for copy in tell(0)[2:]:
        copy.start()

    def finish_step(step):
        share(step).wait_recv()
        experts(step)
        for copy in tell(step):
            copy.start()

    def step_of(step, _):
        for arrived, onward in zip(forward(step - 1), forward(step)):
            arrived.wait_recv()

            @pl.when(step < chips - 1)
            def _():
                onward.start()

        share(step).start()

        @pl.when(step == 2)
        def _():
            late()

        @pl.when(step > 1)
        def _():
            finish_step(step - 1)

    lax.fori_loop(1, chips, step_of, None)
    finish_step(chips - 1)

    def gathered(lane, _):
        @pl.when(lane != place)
        def _():
            for copy in hear(lane):
                copy.wait_recv()

    lax.fori_loop(0, 2 * chips, gathered, None)
    finish()

    def project(index, _):
        columns = pl.ds(pl.multiple_of(index * 512, 512), 512)
        served_ref[:, columns] = jnp.dot(
            hid_ref[...], down_ref[:, :, columns].reshape(2 * chips * hidden, 512),
            preferred_element_type=jnp.float32
        )

    lax.fori_loop(0, width // 512, project, None)
    for chunk in range(chunks):
        wide_ref[pl.ds(chunk, count, stride=chunks), :] = served_ref[
            :, chunk * 128 : (chunk + 1) * 128
        ]
    home_ref[...] = wide_ref[...].astype(jnp.bfloat16)
    exchange(home_ref, back_ref, home_send, home_recv)
    wide_ref[...] = back_ref[...].astype(jnp.float32)
    narrow(ret_ref)
    returned = ret_ref[...]
    out_ref[...] = (
        middle_ref[...]
        + jnp.dot(mix_ref[0], returned, preferred_element_type=jnp.float32)
        + jnp.dot(mix_ref[1], returned, preferred_element_type=jnp.float32)
        + jnp.dot(mix_ref[2], returned, preferred_element_type=jnp.float32)
    ).astype(jnp.bfloat16)

    def settle(turn, _):
        swap(away_ref, got_ref, away_send, away_recv, turn).wait_send()
        swap(home_ref, back_ref, home_send, home_recv, turn).wait_send()

    lax.fori_loop(1, places, settle, None)

    for copy in (*forward(0, x_ref), share_own(), *tell(0)[2:]):
        copy.wait_send()

    def drain(step, _):
        @pl.when(step < chips - 1)
        def _():
            for copy in forward(step):
                copy.wait_send()

        share(step).wait_send()
        for copy in tell(step):
            copy.wait_send()

    lax.fori_loop(1, chips, drain, None)


def layer(
    query_rows, bundle, down, project, residual, out_gain, ffn_gain, chooser, gate, up, mix_parts
):
    shard_len = query_rows.shape[0]
    block_count = lax.axis_size("sp")
    tp_count = lax.axis_size("tp")
    tok = shard_len // tp_count
    chips = tp_count // 2
    pack = tok // 2
    groups = tp_count // 4
    hidden, width = down.shape
    count = chooser.shape[0]
    rows = count * (width // 128)
    attention_scratch = [
        pltpu.VMEM((tok, width), jnp.bfloat16),
        pltpu.VMEM((tok, width), jnp.float32),
        pltpu.VMEM((tp_count, hidden, width), jnp.bfloat16),
        pltpu.VMEM(project.shape, jnp.bfloat16),
        pltpu.SemaphoreType.DMA((2,)),
        pltpu.VMEM((tok, tp_count * VH), jnp.bfloat16),
        pltpu.VMEM((block_count, *bundle.shape), jnp.bfloat16),
        pltpu.VMEM((shard_len, 128), jnp.bfloat16),
        pltpu.VMEM((shard_len, 128), jnp.float32),
        pltpu.VMEM((shard_len, 128), jnp.float32),
        pltpu.VMEM((shard_len, 128), jnp.bfloat16),
        pltpu.VMEM((tp_count * pack, 128), jnp.bfloat16),
        pltpu.VMEM((tp_count, pack, 128), jnp.bfloat16),
        pltpu.SemaphoreType.DMA((block_count * 8,)),
        pltpu.SemaphoreType.DMA((block_count * 4,)),
        pltpu.SemaphoreType.DMA((groups,)),
        pltpu.SemaphoreType.DMA((groups,)),
        pltpu.SemaphoreType.DMA((tp_count,)),
        pltpu.SemaphoreType.DMA((tp_count,)),
        *[pltpu.SemaphoreType.DMA((4 * chips,)) for _ in range(4)],
    ]
    expert_scratch = [
        pltpu.VMEM((rows, 128), jnp.float32),
        *[pltpu.VMEM((rows, 128), jnp.bfloat16) for _ in range(4)],
        pltpu.VMEM((count, width), jnp.bfloat16),
        pltpu.VMEM((count, width), jnp.bfloat16),
        *[pltpu.SemaphoreType.DMA((block_count,)) for _ in range(4)],
        pltpu.VMEM((width, 2 * hidden), jnp.bfloat16),
        pltpu.VMEM((chips, 2 * count, width), jnp.bfloat16),
        pltpu.VMEM((chips, 2 * count, hidden), jnp.bfloat16),
        pltpu.VMEM((count, tp_count * hidden), jnp.bfloat16),
        pltpu.VMEM((count, width), jnp.float32),
        *[pltpu.SemaphoreType.DMA((4 * chips,)) for _ in range(6)],
    ]
    split = len(attention_scratch)

    def kernel(
        q_ref, own_ref, down_ref, project_hbm, res_ref, out_gain_ref, ffn_gain_ref,
        choose_ref, gate_ref, up_ref, mix_ref, out_ref, load_sem, *scratch,
    ):
        attention_refs, expert_refs = scratch[:split], scratch[split:]
        token_ref, middle_ref, all_ref = attention_refs[:3]
        loads = expert_loads(gate_ref, up_ref, expert_refs[11], load_sem)
        for load in loads:
            load.start()

        def meet():
            mine = lax.axis_index("sp")
            head = lax.axis_index("tp")
            mirror = block_count - 1 - mine
            row, col = mine // SIDE, mine % SIDE

            def block_at(dx, dy):
                return ((row + dy) % SIDE) * SIDE + (col + dx) % SIDE

            barrier = pltpu.get_barrier_semaphore()

            def greet(place, lane):
                pl.semaphore_signal(
                    barrier,
                    inc=1,
                    device_id={"sp": place, "tp": lane},
                    device_id_type=pl.DeviceIdType.MESH,
                )

            for dx, dy in ((1, 0), (3, 0), (0, 1), (0, 3)):
                greet(block_at(dx, dy), head)
            for other in range(tp_count):
                greet(mirror, other)

                @pl.when(other != head)
                def _():
                    greet(mine, other)

            def greet_place(turn, _):
                greet((mine + turn) % block_count, head)

            lax.fori_loop(1, block_count, greet_place, None)
            pl.semaphore_wait(barrier, 4 + 2 * tp_count - 1 + block_count - 1)

        late, finish = attention_phase(
            q_ref, own_ref, down_ref, project_hbm, res_ref, out_gain_ref, ffn_gain_ref,
            *attention_refs, meet,
        )
        expert_phase(
            choose_ref, token_ref, all_ref, mix_ref, middle_ref, out_ref, loads, late, finish,
            *expert_refs,
        )

    vmem, hbm = pl.BlockSpec(memory_space=pltpu.VMEM), pl.BlockSpec(memory_space=pltpu.HBM)
    return pl.pallas_call(
        kernel,
        out_shape=jax.ShapeDtypeStruct(residual.shape, jnp.bfloat16),
        in_specs=[vmem, vmem, hbm, hbm, vmem, vmem, vmem, vmem, hbm, hbm, vmem],
        out_specs=vmem,
        scratch_shapes=[pltpu.SemaphoreType.DMA((2,)), *attention_scratch, *expert_scratch],
        compiler_params=pltpu.CompilerParams(
            collective_id=5, has_side_effects=True, vmem_limit_bytes=56 * 1024 * 1024
        ),
    )(query_rows, bundle, down, project, residual, out_gain, ffn_gain, chooser, gate, up, mix_parts)


def shards(
    queries,
    latent,
    rot_key,
    latent_gain,
    key_up,
    value_up,
    query_gain,
    key_gain,
    out_gain,
    out_weight,
    residual,
    ffn_gain,
    routes,
    route_weights,
    expert_gate,
    expert_up,
    expert_down,
):
    shard_len = queries.shape[0]
    local_heads = key_up.shape[1] // NOPE
    sp_count = lax.axis_size("sp")
    my_first = lax.axis_index("sp") * shard_len
    positions = my_first + jnp.arange(shard_len, dtype=jnp.int32)
    inverse = rope_base ** (-jnp.arange(0, ROPE, 2, dtype=jnp.float32) / ROPE)
    angles = positions.astype(jnp.float32)[:, None] * inverse[None, :]
    lat_f32 = latent.astype(jnp.float32)
    normed_latent = (lat_f32 * rms_scale(lat_f32) * latent_gain).astype(jnp.bfloat16)
    key_nope = jnp.dot(normed_latent, key_up, preferred_element_type=jnp.float32).astype(
        jnp.bfloat16
    )
    value_rows = jnp.dot(normed_latent, value_up, preferred_element_type=jnp.float32).astype(
        jnp.bfloat16
    )
    shared = rot_key.astype(jnp.float32)[:, None, :]
    raw_keys = jnp.concatenate(
        [key_nope.astype(jnp.float32).reshape(shard_len, local_heads, NOPE), shared], axis=-1
    )
    key_rows = head_prepare(raw_keys, key_gain, angles)
    query_rows = head_prepare(
        queries.astype(jnp.float32).reshape(shard_len, local_heads, QK), query_gain, angles
    )
    bundle = jnp.concatenate([key_rows.reshape(shard_len, QK).T, value_rows.T], axis=0)
    tok_count = residual.shape[0]
    slot_cap = max(2, 9 * tok_count * TOPK // (8 * sp_count))
    slot_total = sp_count * slot_cap
    targets = slot_targets(routes, sp_count, slot_cap)
    slot_ids = jnp.arange(slot_total, dtype=jnp.int32)
    hits = targets[:, :, None] == slot_ids[None, None, :]
    chooser = jnp.any(slot_ids[:, None, None] == targets[None, :, :], axis=2).astype(jnp.bfloat16)
    mix = jnp.sum(jnp.where(hits, route_weights[:, :, None], 0.0), axis=1)
    mix_high = lax.reduce_precision(mix, 8, 7)
    mix_mid = lax.reduce_precision(mix - mix_high, 8, 7)
    mix_low = mix - mix_high - mix_mid
    mix_parts = jnp.stack([mix_high, mix_mid, mix_low]).astype(jnp.bfloat16)
    return layer(
        jnp.pad(query_rows.reshape(shard_len, QK), ((0, 0), (0, 128 - QK))),
        bundle,
        expert_down[0],
        out_weight,
        residual,
        out_gain[None, :],
        ffn_gain[None, :],
        chooser,
        expert_gate[0],
        expert_up[0],
        mix_parts,
    )


def solution(mesh):
    return jax.shard_map(
        shards,
        mesh=mesh,
        in_specs=(
            P("sp", "tp"),
            P("sp", None),
            P("sp", None),
            P(),
            P(None, "tp"),
            P(None, "tp"),
            P(),
            P(),
            P(),
            P(),
            P(("sp", "tp"), None),
            P(),
            P(("sp", "tp"), None),
            P(("sp", "tp"), None),
            P("sp", None, "tp"),
            P("sp", None, "tp"),
            P("sp", "tp", None),
        ),
        out_specs=P(("sp", "tp"), None),
        check_vma=False,
    )
```

time: 452 us -> 172 us (0.38)
  waiting for transfers between devices: 209 us -> 0 us
  Pallas kernels: 0 us -> 161 us
  blocking collectives: 157 us -> 0 us
  matrix products: 31.3 us -> 2.33 us
  starting transfers between devices: 14.7 us -> 0 us
  between operations: 13.5 us -> 0.26 us
  other arithmetic: 12 us -> 4.33 us
  local copies, waits for them, and re-layouts: 9.85 us -> 4.17 us
    pallas_call x0 -> x1, Pallas kernels: none -> 161 us  [layer(): pl.pallas_call(kernel, out_shape=jax.ShapeDtypeStruct(residual.shape, jnp...]
    all_to_all x1 -> x0, blocking collectives: 157 us -> none  [shards(): lax.all_to_all(outbound, 'sp', split_axis=0, concat_axis=0, tiled=True)]
    all_gather x2 -> x0, waiting for transfers between devices: 119 us -> none  [the longest x1 63.8 us: shards(): key_piece = lax.all_gather(bundle, 'sp', axis=2, tiled=True)]
    reduce_scatter x1 -> x0, waiting for transfers between devices: 68.3 us -> none  [shards(): lax.psum_scatter(jnp.dot(hidden, expert_down[0], preferred_element_type=j...]
    dot_general x6 -> x0, matrix products: 28.9 us -> none  [the longest x1 14.2 us: shards(): jnp.dot(hidden, expert_down[0], preferred_element_type=jnp.float32)]
    all_to_all x2 -> x0, waiting for transfers between devices: 22 us -> none  [the longest x1 13.2 us: shards(): lax.all_to_all(served, 'sp', split_axis=0, concat_axis=0, tiled=True)]
    all_to_all x2 -> x0, starting transfers between devices: 14.4 us -> none  [the longest x1 7.87 us: shards(): lax.all_to_all(head_major, 'tp', split_axis=0, concat_axis=1, tiled=True)]
    reduce_sum x4 -> x1, other arithmetic: 4.68 us -> 0.12 us  [shards(): mix = jnp.sum(jnp.where(hits, route_weights[:, :, None], 0.0), axis=1)]
  transfers between devices with their start and end apart: 5 -> 0, of which waited for: 5 -> 0; matrix products, arithmetic and copies ran while one was open for 0% -> 0% of each run, Pallas kernels for 0% -> 0%
where the time goes in v6:
time: 172 us
  Pallas kernels  161 us (94%)
  other arithmetic  4.33 us (3%)
  local copies, waits for them, and re-layouts  4.17 us (2%)
  matrix products  2.33 us (1%)
    pallas_call x1, Pallas kernels, layer(): pl.pallas_call(kernel, out_shape=jax.ShapeDtypeStruct(residual.shape, jnp...  161 us

profile of v6, /device:TPU:1, one launch (start us, length us, event | category | flops | bytes accessed | tf_op | source)
XLA Modules:
  0.0 172.1 jit_solution(9809309338363143129)
XLA Ops:
  0.0 0.0 copy-start
  0.0 0.0 copy-start.3
  0.0 0.0 copy-start.6
  0.0 0.0 copy-start.2
  0.0 0.0 copy-start.7
  0.0 1.6 fusion
  1.6 0.0 copy-done
  1.6 1.8 %fusion.3 = bf16[1024,1,64]{0,2,1:T(8,128)(2,1)S(1)} fusion(bf16[512,64]{0,1:T(8,128)(2,1)S(1)} %copy-done, bf16[1024,512]{1,0:T(8,128)(2,1)} %param.18, f32[512]{0:T(512)} %param.20, f32[1024]{0:T(1024)S(1)} %add_rsqrt_fusion.1), kind=kOutput, calls=%fused_computation.7 | convolution fusion | flops 69271552 | bytes 1251328 | tf_op jit(solution)/shard_map/dot_general | solution.py:797
  3.4 0.0 copy-start.1
  3.4 0.0 copy-start.8
  3.4 0.0 copy-start.9
  3.4 0.0 copy-done.3
  3.4 0.1 fusion.8
  3.5 0.0 copy-done.6
  3.5 0.1 fusion.9
  3.6 0.0 copy-done.2
  3.6 0.1 fusion.5
  3.7 0.0 copy-done.7
  3.7 0.1 fusion.7
  3.8 0.3 fusion.34
  4.2 0.0 copy-start.4
  4.3 0.0 copy-start.5
  4.3 0.3 copy-done.1
  4.6 0.0 copy-done.8
  4.6 0.0 copy-done.9
  4.6 0.6 fusion.4
  5.2 0.7 pad_maximum_fusion.own_ref
  5.9 0.2 copy.39
  6.1 0.8 pad.4.clone.q_ref
  6.9 0.0 copy-done.4
  6.9 0.1 copy.35
  7.0 0.1 eq.42
  7.1 0.1 fusion.32
  7.2 0.2 reduce_window_sum.11
  7.4 0.2 select_reduce_fusion.1
  7.5 0.1 reduce_sum.53
  7.7 0.1 copy.36
  7.8 0.0 copy-done.5
  7.8 0.1 select_reduce_fusion
  7.9 0.7 pad_maximum_fusion.3.mix_ref
  8.6 0.1 fusion.14
  8.7 0.7 copy.38.choose_ref
  9.4 161.0 %shard_map.163 = bf16[64,2048]{1,0:T(8,128)(2,1)} custom-call(bf16[1024,128]{1,0:T(8,128)(2,1)} %pad.4.clone.q_ref, bf16[160,1024]{1,0:T(8,128)(2,1)} %pad_maximum_fusion.own_ref, bf16[128,2048]{1,0:T(8,128)(2,1)} %bitcast.35, bf16[1024,2048]{1,0:T(8,128)(2,1)} %project_hbm.1, bf16[64,2048]{1,0:T(8,128)(2,1)} %res_ref.1, f32[1,1024]{1,0:T(1,128)} %bitcast.41, ...), custom_call_target="tpu_custom_call" | custom-call | tf_op jit(solution)/shard_map/pallas_call | solution.py:757
  170.4 1.7 copy.41
  (11 shorter events, 0.1 us)
Async XLA Ops:
  0.0 1.6 copy-start
  0.0 3.4 %copy-start.3 = (bf16[1024,32]{0,1:T(8,128)(2,1)S(1)}, bf16[1024,32]{0,1:T(8,128)(2,1)}, u32[]{:S(2)}) copy-start(bf16[1024,32]{0,1:T(8,128)(2,1)} %param.19) | copy-start | bytes 196612
  0.0 3.5 %copy-start.6 = (f32[96]{0:T(128)S(1)}, f32[96]{0:T(128)}, u32[]{:S(2)}) copy-start(f32[96]{0:T(128)} %param.24) | copy-start | bytes 1156
  0.0 3.6 %copy-start.2 = (bf16[1024,96]{0,1:T(8,128)(2,1)S(1)}, bf16[1024,96]{0,1:T(8,128)(2,1)}, u32[]{:S(2)}) copy-start(bf16[1024,96]{0,1:T(8,128)(2,1)} %param.17) | copy-start | bytes 589828
  0.0 3.7 %copy-start.7 = (f32[96]{0:T(128)S(1)}, f32[96]{0:T(128)}, u32[]{:S(2)}) copy-start(f32[96]{0:T(128)} %param.23) | copy-start | bytes 1156
  3.4 1.2 copy-start.1
  3.4 1.2 copy-start.8
  3.4 1.2 copy-start.9
  4.2 2.6 %copy-start.4 = (s32[64,2]{0,1:T(2,128)S(1)}, s32[64,2]{0,1:T(2,128)}, u32[]{:S(2)}) copy-start(s32[64,2]{0,1:T(2,128)} %param.29) | copy-start | bytes 1540
  4.3 3.5 %copy-start.5 = (f32[64,2]{0,1:T(2,128)S(1)}, f32[64,2]{0,1:T(2,128)}, u32[]{:S(2)}) copy-start(f32[64,2]{0,1:T(2,128)} %param.30) | copy-start | bytes 1540

commit v7 on v6

--- a/solution.py
+++ b/solution.py
@@ -53,7 +53,7 @@
 
 
 SCORE_EXP = 1.4426950408889634 * QK ** (-0.5)
-Q_TILE = 256
+Q_TILE = 128
 SIDE = 4
 VISITS = (
     (0, 0), (1, 0), (3, 0), (0, 1), (0, 3), (1, 1), (1, 3), (3, 1),
@@ -235,11 +235,15 @@
         val_ref[:, :VH] = kv_ref[block, QK:, :].T
         values = val_ref[...]
         for start, masked in parts:
-            for first in range(start, start + half, Q_TILE):
+            tiles = range(start, start + half, Q_TILE)
+            all_scores = [
+                jnp.dot(
+                    pair_ref[pl.ds(first, Q_TILE), :QK], keys, preferred_element_type=jnp.float32
+                )
+                for first in tiles
+            ]
+            for first, scores in zip(tiles, all_scores):
                 rows = pl.ds(first, Q_TILE)
-                scores = jnp.dot(
-                    pair_ref[rows, :QK], keys, preferred_element_type=jnp.float32
-                )
                 if masked:
                     q_pos = lax.broadcasted_iota(jnp.int32, scores.shape, 0)
                     k_pos = lax.broadcasted_iota(jnp.int32, scores.shape, 1)
@@ -248,7 +252,8 @@
                     scores = jnp.where(k_pos - q_pos <= shift, scores, -1e30)
                 old = peak_ref[rows, :]
                 new = jnp.maximum(old, jnp.max(scores, axis=1, keepdims=True))
-                weights = jnp.exp2((scores - new[:, :1]) * SCORE_EXP).astype(jnp.bfloat16)
+                spread_peak = jnp.tile(new, (1, shard_len // 128))
+                weights = jnp.exp2((scores - spread_peak) * SCORE_EXP).astype(jnp.bfloat16)
                 factor = jnp.exp2((old - new) * SCORE_EXP)
                 peak_ref[rows, :] = new
                 acc_ref[rows, :] = acc_ref[rows, :] * factor + jnp.dot(

time: 172 us -> 169 us (0.983)
  Pallas kernels: 161 us -> 158 us
    pallas_call x1, Pallas kernels: 161 us -> 158 us  [layer(): pl.pallas_call(kernel, out_shape=jax.ShapeDtypeStruct(residual.shape, jnp...]
where the time goes in v7:
time: 169 us
  Pallas kernels  158 us (93%)
  other arithmetic  4.33 us (3%)
  local copies, waits for them, and re-layouts  4.17 us (2%)
  matrix products  2.33 us (1%)
    pallas_call x1, Pallas kernels, layer(): pl.pallas_call(kernel, out_shape=jax.ShapeDtypeStruct(residual.shape, jnp...  158 us

profile of v7, /device:TPU:1, one launch (start us, length us, event | category | flops | bytes accessed | tf_op | source)
XLA Modules:
  0.0 168.8 jit_solution(17013768405093587261)
XLA Ops:
  0.0 0.0 copy-start
  0.0 0.0 copy-start.3
  0.0 0.0 copy-start.6
  0.0 0.0 copy-start.2
  0.0 0.0 copy-start.7
  0.0 1.6 fusion
  1.6 0.0 copy-done
  1.6 1.8 %fusion.3 = bf16[1024,1,64]{0,2,1:T(8,128)(2,1)S(1)} fusion(bf16[512,64]{0,1:T(8,128)(2,1)S(1)} %copy-done, bf16[1024,512]{1,0:T(8,128)(2,1)} %param.18, f32[512]{0:T(512)} %param.20, f32[1024]{0:T(1024)S(1)} %add_rsqrt_fusion.1), kind=kOutput, calls=%fused_computation.7 | convolution fusion | flops 69271552 | bytes 1251328 | tf_op jit(solution)/shard_map/dot_general | solution.py:802
  3.4 0.0 copy-start.1
  3.4 0.0 copy-start.8
  3.4 0.0 copy-start.9
  3.4 0.0 copy-done.3
  3.4 0.1 fusion.8
  3.5 0.0 copy-done.6
  3.5 0.1 fusion.9
  3.6 0.0 copy-done.2
  3.6 0.1 fusion.5
  3.7 0.0 copy-done.7
  3.7 0.1 fusion.7
  3.8 0.3 fusion.34
  4.2 0.0 copy-start.4
  4.3 0.0 copy-start.5
  4.3 0.3 copy-done.1
  4.6 0.0 copy-done.8
  4.6 0.0 copy-done.9
  4.6 0.6 fusion.4
  5.2 0.7 pad_maximum_fusion.own_ref
  5.9 0.2 copy.39
  6.1 0.8 pad.4.clone.q_ref
  6.9 0.0 copy-done.4
  6.9 0.1 copy.35
  7.0 0.1 eq.42
  7.1 0.1 fusion.32
  7.2 0.2 reduce_window_sum.11
  7.4 0.2 select_reduce_fusion.1
  7.5 0.1 reduce_sum.53
  7.7 0.1 copy.36
  7.8 0.0 copy-done.5
  7.8 0.1 select_reduce_fusion
  7.9 0.7 pad_maximum_fusion.3.mix_ref
  8.6 0.1 fusion.14
  8.7 0.7 copy.38.choose_ref
  9.4 157.7 %shard_map.163 = bf16[64,2048]{1,0:T(8,128)(2,1)} custom-call(bf16[1024,128]{1,0:T(8,128)(2,1)} %pad.4.clone.q_ref, bf16[160,1024]{1,0:T(8,128)(2,1)} %pad_maximum_fusion.own_ref, bf16[128,2048]{1,0:T(8,128)(2,1)} %bitcast.35, bf16[1024,2048]{1,0:T(8,128)(2,1)} %project_hbm.1, bf16[64,2048]{1,0:T(8,128)(2,1)} %res_ref.1, f32[1,1024]{1,0:T(1,128)} %bitcast.41, ...), custom_call_target="tpu_custom_call" | custom-call | tf_op jit(solution)/shard_map/pallas_call | solution.py:762
  167.1 1.7 copy.41
  (11 shorter events, 0.1 us)
Async XLA Ops:
  0.0 1.6 copy-start
  0.0 3.4 %copy-start.3 = (bf16[1024,32]{0,1:T(8,128)(2,1)S(1)}, bf16[1024,32]{0,1:T(8,128)(2,1)}, u32[]{:S(2)}) copy-start(bf16[1024,32]{0,1:T(8,128)(2,1)} %param.19) | copy-start | bytes 196612
  0.0 3.5 %copy-start.6 = (f32[96]{0:T(128)S(1)}, f32[96]{0:T(128)}, u32[]{:S(2)}) copy-start(f32[96]{0:T(128)} %param.24) | copy-start | bytes 1156
  0.0 3.6 %copy-start.2 = (bf16[1024,96]{0,1:T(8,128)(2,1)S(1)}, bf16[1024,96]{0,1:T(8,128)(2,1)}, u32[]{:S(2)}) copy-start(bf16[1024,96]{0,1:T(8,128)(2,1)} %param.17) | copy-start | bytes 589828
  0.0 3.7 %copy-start.7 = (f32[96]{0:T(128)S(1)}, f32[96]{0:T(128)}, u32[]{:S(2)}) copy-start(f32[96]{0:T(128)} %param.23) | copy-start | bytes 1156
  3.4 1.2 copy-start.1
  3.4 1.2 copy-start.8
  3.4 1.2 copy-start.9
  4.2 2.6 %copy-start.4 = (s32[64,2]{0,1:T(2,128)S(1)}, s32[64,2]{0,1:T(2,128)}, u32[]{:S(2)}) copy-start(s32[64,2]{0,1:T(2,128)} %param.29) | copy-start | bytes 1540
  4.3 3.5 %copy-start.5 = (f32[64,2]{0,1:T(2,128)S(1)}, f32[64,2]{0,1:T(2,128)}, u32[]{:S(2)}) copy-start(f32[64,2]{0,1:T(2,128)} %param.30) | copy-start | bytes 1540

commit v8 on v7

--- a/solution.py
+++ b/solution.py
@@ -766,7 +766,7 @@
         out_specs=vmem,
         scratch_shapes=[pltpu.SemaphoreType.DMA((2,)), *attention_scratch, *expert_scratch],
         compiler_params=pltpu.CompilerParams(
-            collective_id=5, has_side_effects=True, vmem_limit_bytes=56 * 1024 * 1024
+            collective_id=5, has_side_effects=True, vmem_limit_bytes=50 * 1024 * 1024
         ),
     )(query_rows, bundle, down, project, residual, out_gain, ffn_gain, chooser, gate, up, mix_parts)
 

time: 169 us -> 164 us (0.970)
  local copies, waits for them, and re-layouts: 4.17 us -> 1.92 us
where the time goes in v8:
time: 164 us
  Pallas kernels  157 us (96%)
  other arithmetic  2.97 us (2%)
  matrix products  2.33 us (1%)
  local copies, waits for them, and re-layouts  1.92 us (1%)
    pallas_call x1, Pallas kernels, layer(): pl.pallas_call(kernel, out_shape=jax.ShapeDtypeStruct(residual.shape, jnp...  157 us

profile of v8, /device:TPU:1, one launch (start us, length us, event | category | flops | bytes accessed | tf_op | source)
XLA Modules:
  0.0 164.1 jit_solution(14331297384113522217)
XLA Ops:
  0.0 0.0 copy-start
  0.0 0.0 copy-start.9
  0.0 0.0 copy-start.12
  0.0 0.0 copy-start.8
  0.0 0.0 copy-start.13
  0.0 1.6 fusion
  1.6 0.0 copy-done
  1.6 1.8 %fusion.3 = bf16[1024,1,64]{0,2,1:T(8,128)(2,1)S(1)} fusion(bf16[512,64]{0,1:T(8,128)(2,1)S(1)} %copy-done, bf16[1024,512]{1,0:T(8,128)(2,1)} %param.18, f32[512]{0:T(512)} %param.20, f32[1024]{0:T(1024)S(1)} %add_rsqrt_fusion.1), kind=kOutput, calls=%fused_computation.7 | convolution fusion | flops 69271552 | bytes 1251328 | tf_op jit(solution)/shard_map/dot_general | solution.py:802
  3.4 0.0 copy-start.7
  3.4 0.0 copy-start.14
  3.4 0.0 copy-start.15
  3.4 0.0 copy-done.9
  3.4 0.1 fusion.8
  3.5 0.0 copy-done.12
  3.5 0.1 fusion.9
  3.6 0.0 copy-done.8
  3.6 0.1 fusion.5
  3.7 0.0 copy-done.13
  3.7 0.1 fusion.7
  3.8 0.3 fusion.34
  4.2 0.0 copy-start.10
  4.3 0.0 copy-start.11
  4.3 0.3 copy-done.7
  4.6 0.0 copy-done.14
  4.6 0.0 copy-done.15
  4.6 0.0 copy-start.1
  4.6 0.0 copy-start.2
  4.6 0.0 copy-start.3
  4.7 0.0 copy-start.4
  4.7 0.0 copy-start.5
  4.7 0.0 copy-start.6
  4.7 0.6 fusion.4
  5.3 0.2 copy.39
  5.5 0.1 pad.4.clone.q_ref
  5.5 0.0 copy-done.10
  5.5 0.1 copy.35
  5.6 0.1 eq.42
  5.8 0.1 fusion.32
  5.9 0.2 reduce_window_sum.11
  6.0 0.2 select_reduce_fusion.1
  6.2 0.1 reduce_sum.53
  6.4 0.1 copy.36
  6.4 0.0 copy-done.11
  6.4 0.1 select_reduce_fusion
  6.6 0.1 fusion.14
  6.7 0.1 copy.38.choose_ref
  6.8 0.0 copy-done.1
  6.8 0.0 copy-done.2
  6.9 0.0 copy-done.3
  6.9 0.0 copy-done.4
  6.9 0.0 copy-done.5
  6.9 0.0 copy-done.6
  6.9 156.5 %shard_map.163 = bf16[64,2048]{1,0:T(8,128)(2,1)S(1)} custom-call(bf16[1024,128]{1,0:T(8,128)(2,1)S(1)} %pad.4.clone.q_ref, bf16[160,1024]{1,0:T(8,128)(2,1)S(1)} %pad_maximum_fusion.own_ref, bf16[128,2048]{1,0:T(8,128)(2,1)S(1)} %bitcast.35, bf16[1024,2048]{1,0:T(8,128)(2,1)} %project_hbm.1, bf16[64,2048]{1,0:T(8,128)(2,1)S(1)} %copy-done.4, ...), custom_call_target="tpu_custom_call" | custom-call | tf_op jit(solution)/shard_map/pallas_call | solution.py:762
  163.4 0.7 copy.41
  (13 shorter events, 0.2 us)
Async XLA Ops:
  0.0 1.6 copy-start
  0.0 3.4 %copy-start.9 = (bf16[1024,32]{0,1:T(8,128)(2,1)S(1)}, bf16[1024,32]{0,1:T(8,128)(2,1)}, u32[]{:S(2)}) copy-start(bf16[1024,32]{0,1:T(8,128)(2,1)} %param.19) | copy-start | bytes 196612
  0.0 3.5 %copy-start.12 = (f32[96]{0:T(128)S(1)}, f32[96]{0:T(128)}, u32[]{:S(2)}) copy-start(f32[96]{0:T(128)} %param.24) | copy-start | bytes 1156
  0.0 3.6 %copy-start.8 = (bf16[1024,96]{0,1:T(8,128)(2,1)S(1)}, bf16[1024,96]{0,1:T(8,128)(2,1)}, u32[]{:S(2)}) copy-start(bf16[1024,96]{0,1:T(8,128)(2,1)} %param.17) | copy-start | bytes 589828
  0.0 3.7 %copy-start.13 = (f32[96]{0:T(128)S(1)}, f32[96]{0:T(128)}, u32[]{:S(2)}) copy-start(f32[96]{0:T(128)} %param.23) | copy-start | bytes 1156
  3.4 1.2 copy-start.7
  3.4 1.2 copy-start.14
  3.4 1.2 copy-start.15
  4.2 1.3 copy-start.10
  4.3 2.2 %copy-start.11 = (f32[64,2]{0,1:T(2,128)S(1)}, f32[64,2]{0,1:T(2,128)}, u32[]{:S(2)}) copy-start(f32[64,2]{0,1:T(2,128)} %param.30) | copy-start | bytes 1540
  4.6 2.2 %copy-start.1 = (bf16[1,128,2048]{2,1,0:T(8,128)(2,1)S(1)}, bf16[1,128,2048]{2,1,0:T(8,128)(2,1)}, u32[]{:S(2)}) copy-start(bf16[1,128,2048]{2,1,0:T(8,128)(2,1)} %param.33) | copy-start | bytes 1572868
  4.6 2.2 %copy-start.2 = (bf16[1,2048,128]{2,1,0:T(8,128)(2,1)S(1)}, bf16[1,2048,128]{2,1,0:T(8,128)(2,1)}, u32[]{:S(2)}) copy-start(bf16[1,2048,128]{2,1,0:T(8,128)(2,1)} %param.31) | copy-start | bytes 1572868
  4.6 2.2 %copy-start.3 = (bf16[1,2048,128]{2,1,0:T(8,128)(2,1)S(1)}, bf16[1,2048,128]{2,1,0:T(8,128)(2,1)}, u32[]{:S(2)}) copy-start(bf16[1,2048,128]{2,1,0:T(8,128)(2,1)} %param.32) | copy-start | bytes 1572868
  4.7 2.2 %copy-start.4 = (bf16[64,2048]{1,0:T(8,128)(2,1)S(1)}, bf16[64,2048]{1,0:T(8,128)(2,1)}, u32[]{:S(2)}) copy-start(bf16[64,2048]{1,0:T(8,128)(2,1)} %res_ref.1) | copy-start | bytes 786436
  4.7 2.2 %copy-start.5 = (f32[2048]{0:T(1024)S(1)}, f32[2048]{0:T(1024)}, u32[]{:S(2)}) copy-start(f32[2048]{0:T(1024)} %param.28) | copy-start | bytes 24580
  4.7 2.2 %copy-start.6 = (f32[1024]{0:T(1024)S(1)}, f32[1024]{0:T(1024)}, u32[]{:S(2)}) copy-start(f32[1024]{0:T(1024)} %param.25) | copy-start | bytes 12292
